TPU v7x, 256 devices: a whole 4x4x8 slice. The times are simulated.
256 devices in a mesh: ep: 32 (over z, x), tp: 8 (over y, core).
Axes of the slice: x: 4, y: 4, z: 8, core: 2. Of those that a mesh axis runs over, the one named last changes fastest.
Arguments:
- tokens: bfloat16 [1536, 2048], P('ep'), may hold values from -6 to 6
- state: float32 [1536, 8, 128, 128], P('ep', 'tp'), may hold values from -4 to 4
- norm_gain: float32 [2048], replicated, may hold values from 0.1 to 1.9
- w_query: bfloat16 [2048, 1024], P('ep', 'tp'), may hold values from -0.125 to 0.125
- w_forget: bfloat16 [2048, 1024], P('ep', 'tp'), may hold values from -0.125 to 0.125
- w_input: bfloat16 [2048, 1024], P('ep', 'tp'), may hold values from -0.125 to 0.125
- w_outgate: bfloat16 [2048, 1024], P('ep', 'tp'), may hold values from -0.125 to 0.125
- lower_bound: float32 [1024], P('tp'), may hold values from 0 to 0.9
- head_gain: float32 [1024], P('tp'), may hold values from 0.1 to 1.9
- w_output: bfloat16 [1024, 2048], P('tp'), may hold values from -0.1875 to 0.1875
- ffn_gain: float32 [2048], replicated, may hold values from 0.1 to 1.9
- route_ids: int32 [1536, 4], P('ep'), may hold values from 0 to 63, all different within a row; in each aligned block of 48 rows (0 to 47, 48 to 95, ...) at most 6 rows name the same one
- route_weight: float32 [1536, 4], P('ep'), may hold values from 0.2 to 1
- expert_gate: bfloat16 [64, 2048, 1024], P('ep', None, 'tp'), may hold values from -0.125 to 0.125
- expert_up: bfloat16 [64, 2048, 1024], P('ep', None, 'tp'), may hold values from -0.125 to 0.125
- expert_down: bfloat16 [64, 1024, 2048], P('ep', 'tp'), may hold values from -0.1875 to 0.1875
- shared_gate: bfloat16 [2048, 1024], P(None, 'tp'), may hold values from -0.125 to 0.125
- shared_up: bfloat16 [2048, 1024], P(None, 'tp'), may hold values from -0.125 to 0.125
- shared_down: bfloat16 [1024, 2048], P('tp'), may hold values from -0.1875 to 0.1875
- dense_gate: bfloat16 [2048, 8192], P('tp', 'ep'), may hold values from -0.125 to 0.125
- dense_up: bfloat16 [2048, 8192], P('tp', 'ep'), may hold values from -0.125 to 0.125
- dense_down: bfloat16 [8192, 2048], P('ep', 'tp'), may hold values from -0.0625 to 0.0625
- dense_mix: float32 [2048], P('tp'), may hold values from -6 to 6
Outputs:
- mixed: bfloat16 [1536, 2048], P('ep', 'tp')
- new_state: float32 [1536, 8, 128, 128], P('ep', 'tp')
Inputs may be any that keep to these rules, and one draw needn't show every extreme that they name: `route_ids`: each row names 4 different experts. Among the rows of one device no expert is named more than 6 times, and in every draw some expert is named exactly 6 times by some device's rows.
All inputs are finite; a program needn't handle non-finite values.
Results may differ from a plain program's by a relative error of at most 0.025.
Values may be sent and summed in bfloat16 or wider, within the bound.
A program may use at most 64 MiB of HBM per device.

v0:
```python
import jax
import jax.numpy as jnp
from jax import lax
from jax.sharding import Mesh
from jax.sharding import PartitionSpec as P

EP = ("ep_0", "ep_1")


EPS = 1e-06


def side_by_side(arrays, axis, dim, along):
    ends, at = ([], 0)
    for a in arrays[:-1]:
        at += a.shape[along]
        ends.append(at)
    both = jnp.concatenate(arrays, axis=along)
    return tuple(jnp.split(lax.all_gather(both, axis, axis=dim, tiled=True), ends, axis=along))


def from_everyone(x, axis):
    copies = jnp.broadcast_to(x, (lax.axis_size(axis), *x.shape))
    return lax.all_to_all(copies, axis, split_axis=0, concat_axis=0, tiled=True)


def over_copies(x, axis):
    return from_everyone(x, axis).astype(jnp.float32).sum(axis=0)


def split_up(x, dim, size):
    shape = x.shape
    parts = x.reshape(*shape[:dim], size, shape[dim] // size, *shape[dim + 1 :])
    return jnp.moveaxis(parts, dim, 0)


def sum_at_owner(x, axis, dim):
    parts = split_up(x, dim, lax.axis_size(axis))
    arrived = lax.all_to_all(parts, axis, split_axis=0, concat_axis=0, tiled=True)
    return arrived.astype(jnp.float32).sum(axis=0)


def joined_along(parts, dim):
    shape = list(parts.shape[1:])
    shape[dim] *= parts.shape[0]
    return jnp.moveaxis(parts, 0, dim).reshape(shape)


def collect(x, axis, dim):
    return joined_along(from_everyone(x, axis), dim)


def padded_to(lines, size):
    spare = -len(lines) % size
    return jnp.pad(lines, [(0, spare)] + [(0, 0)] * (lines.ndim - 1))


def total_of(x, axis):
    lines = x.reshape(-1, *x.shape[1:][-1:])
    own = lax.psum_scatter(
        padded_to(lines, lax.axis_size(axis)), axis, scatter_dimension=0, tiled=True
    )
    whole = lax.all_gather(own, axis).reshape(-1, *lines.shape[1:])
    return lax.slice_in_dim(whole, 0, len(lines)).reshape(x.shape)


def sum_by_axis(terms, axes):
    subtotal = terms.astype(jnp.bfloat16)
    for axis in axes:
        subtotal = lax.psum_scatter(subtotal, axis, scatter_dimension=0, tiled=True)
    return subtotal.astype(jnp.float32)


def rms_scale(values, gain):
    values = values.astype(jnp.float32)
    return values * lax.rsqrt(jnp.mean(values * values, axis=-1, keepdims=True) + EPS) * gain


def rounded(values):
    return lax.optimization_barrier(values.astype(jnp.bfloat16)).astype(jnp.float32)


def local(
    tokens,
    state,
    norm_gain,
    w_query,
    w_forget,
    w_input,
    w_outgate,
    lower_bound,
    head_gain,
    w_output,
    ffn_gain,
    route_ids,
    route_weight,
    expert_gate,
    expert_up,
    expert_down,
    shared_gate,
    shared_up,
    shared_down,
    dense_gate,
    dense_up,
    dense_down,
    dense_mix,
):
    ep_size = lax.axis_size(EP)
    tp_size = lax.axis_size("tp")
    seq_local, width = tokens.shape
    mix_local = w_query.shape[1]
    heads_local = state.shape[1]
    head_dim = state.shape[2]
    width_local = width // tp_size
    tp_index = lax.axis_index("tp")
    normed = rms_scale(tokens, norm_gain).astype(jnp.bfloat16)
    block = normed
    joined = jnp.concatenate(
        side_by_side((w_query, w_forget, w_input, w_outgate), EP, 0, 1), axis=1
    )
    projected = jnp.dot(block, joined, preferred_element_type=jnp.float32)
    projected = rounded(projected)
    query, forget_pre, values, out_gate = jnp.split(projected, 4, axis=1)
    shape = (seq_local, heads_local, head_dim)
    forget_sig = jax.nn.sigmoid(forget_pre)
    decay = (lower_bound + (1.0 - lower_bound) * forget_sig).reshape(shape)
    keygate = ((1.0 - lower_bound) * (1.0 - forget_sig)).reshape(shape)
    new_state = decay[..., None] * state + keygate[..., None] * values.reshape(shape)[:, :, None, :]
    readout = jnp.einsum("bhk,bhkv->bhv", query.reshape(shape), new_state)
    readout = readout * lax.rsqrt(jnp.mean(readout * readout, axis=-1, keepdims=True) + EPS)
    head_out = (readout.reshape(seq_local, mix_local) * head_gain * jax.nn.silu(out_gate)).astype(
        jnp.bfloat16
    )
    head_part = rounded(jnp.dot(head_out, w_output, preferred_element_type=jnp.float32))
    resid = tokens.astype(jnp.float32) + over_copies(head_part.astype(jnp.bfloat16), "tp").astype(
        jnp.float32
    )
    moe_in = rms_scale(resid, ffn_gain).astype(jnp.bfloat16)
    exp_local = expert_gate.shape[0]
    experts = exp_local * ep_size
    topk = route_ids.shape[1]
    capacity = max(2, 2 * seq_local * topk // experts)
    flat_ids = route_ids.reshape(-1)
    onehot = (flat_ids[:, None] == jnp.arange(experts, dtype=jnp.int32)[None, :]).astype(jnp.int32)
    slot_rank = jnp.sum((jnp.cumsum(onehot, axis=0) - onehot) * onehot, axis=1)
    slot_index = (flat_ids * capacity + slot_rank).reshape(seq_local, topk)
    slot_ids = jnp.arange(experts * capacity, dtype=jnp.int32)
    slot_hits = slot_index[None, :, :] == slot_ids[:, None, None]
    dispatch = jnp.sum(slot_hits.astype(jnp.bfloat16), axis=2)
    outgoing = jnp.dot(dispatch, moe_in, preferred_element_type=jnp.float32).astype(jnp.bfloat16)
    outgoing = outgoing.reshape(experts, capacity, width)
    incoming = lax.all_to_all(outgoing, EP, split_axis=0, concat_axis=0, tiled=True)
    count = incoming.shape[1]
    grouped = incoming.reshape(ep_size, exp_local, count, width)
    gate_pre = jnp.einsum(
        "sexd,edf->sexf", grouped, expert_gate, preferred_element_type=jnp.float32
    )
    up_pre = jnp.einsum("sexd,edf->sexf", grouped, expert_up, preferred_element_type=jnp.float32)
    hidden = (jax.nn.silu(gate_pre) * up_pre).astype(jnp.bfloat16)
    partial_value = rounded(
        jnp.einsum("sexf,efd->sexd", hidden, expert_down, preferred_element_type=jnp.float32)
    )
    summed = sum_at_owner(partial_value.astype(jnp.bfloat16), "tp", 3).astype(jnp.bfloat16)
    results = lax.all_to_all(
        summed.reshape(experts, count, width_local), EP, split_axis=0, concat_axis=0, tiled=True
    )
    combine = jnp.sum(
        jnp.where(
            slot_index[:, :, None] == slot_ids[None, None, :],
            route_weight[:, :, None],
            jnp.float32(0.0),
        ),
        axis=1,
    )
    routed = jnp.dot(combine, results.reshape(experts * capacity, width_local).astype(jnp.float32))
    shared_hidden = (
        jax.nn.silu(jnp.dot(moe_in, shared_gate, preferred_element_type=jnp.float32))
        * jnp.dot(moe_in, shared_up, preferred_element_type=jnp.float32)
    ).astype(jnp.bfloat16)
    shared_part = rounded(jnp.dot(shared_hidden, shared_down, preferred_element_type=jnp.float32))
    shared_out = sum_at_owner(shared_part.astype(jnp.bfloat16), "tp", 1)
    own_columns = lax.dynamic_slice_in_dim(moe_in, tp_index * width_local, width_local, 1)
    dense_joined = jnp.concatenate([dense_gate, dense_up], axis=1)
    dense_pre = jnp.dot(
        collect(own_columns, EP, 0), dense_joined, preferred_element_type=jnp.float32
    )
    dense_pre = total_of(rounded(dense_pre).astype(jnp.bfloat16), "tp").astype(jnp.float32)
    dense_pre_gate, dense_pre_up = jnp.split(dense_pre, 2, axis=1)
    dense_hidden = (jax.nn.silu(dense_pre_gate) * dense_pre_up).astype(jnp.bfloat16)
    block = dense_hidden
    dense_out = sum_by_axis(jnp.dot(block, dense_down, preferred_element_type=jnp.float32), EP)
    own_resid = lax.dynamic_slice_in_dim(resid, tp_index * width_local, width_local, 1)
    mixed = (own_resid + routed + shared_out + jax.nn.sigmoid(dense_mix) * dense_out).astype(
        jnp.bfloat16
    )
    return (mixed, new_state)


def solution(mesh):
    torus = Mesh(mesh.devices.reshape(8, 4, mesh.shape["tp"]), ("ep_0", "ep_1", "tp"))
    return jax.shard_map(
        local,
        mesh=torus,
        in_specs=(
            P(EP, None),
            P(EP, "tp", None, None),
            P(),
            P(EP, "tp"),
            P(EP, "tp"),
            P(EP, "tp"),
            P(EP, "tp"),
            P("tp"),
            P("tp"),
            P("tp", None),
            P(),
            P(EP, None),
            P(EP, None),
            P(EP, None, "tp"),
            P(EP, None, "tp"),
            P(EP, "tp", None),
            P(None, "tp"),
            P(None, "tp"),
            P("tp", None),
            P("tp", EP),
            P("tp", EP),
            P(EP, "tp"),
            P("tp"),
        ),
        out_specs=(P(EP, "tp"), P(EP, "tp", None, None)),
        check_vma=False,
    )
```

profile of v0, /device:TPU:1, one launch (start us, length us, event | category | flops | bytes accessed | tf_op | source)
XLA Modules:
  0.0 299.8 jit_solution(5604684566299326197)
XLA Ops:
  7.2 0.0 copy-start
  7.2 0.0 copy-start.11
  7.2 0.0 all-gather.4.cloned.1.call-start
  7.2 1.5 pad_maximum_fusion
  8.7 0.0 all-gather.4.cloned.1.call-update
  8.7 1.1 fusion.18
  9.8 0.7 broadcast_subtract_fusion
  10.5 77.7 %all-gather.4.cloned.1.call-done = bf16[2048,512]{1,0:T(8,128)(2,1)} async-done(((bf16[64,512]{1,0:T(8,128)(2,1)}), bf16[2048,512]{1,0:T(8,128)(2,1)}) %all-gather.4.cloned.1.call-update) | async-done | bytes 2097168 | tf_op jit(solution)/shard_map/all_gather | solution.py:19
  88.2 2.2 convolution_convert_fusion.6
  90.5 0.0 copy-start.12
  90.6 3.5 %fusion = f32[48,1,128]{2,1,0:T(1,128)S(1)} fusion(bf16[48,128,1]{1,0,2:T(8,128)(2,1)S(1)} %slice_bitcast_fusion, f32[48,128]{1,0:T(8,128)S(1)} %split.30, f32[48,128]{1,0:T(8,128)S(1)} %get-tuple-element.5, f32[48,1,128,128]{3,2,1,0:T(8,128)} %param.24, f32[48,128]{1,0:T(8,128)S(1)} %get-tuple-element.4), kind=kOutput, calls=%fused_computation | convolution fusion | flops 3932160 | bytes 3256320 | tf_op jit(solution)/shard_map/bhk,bhkv->bhv/dot_general | solution.py:129
  94.1 0.1 multiply_reduce_fusion.1
  94.2 0.3 convolution_convert_fusion.5
  94.5 1.3 broadcast_in_dim.12
  95.8 9.7 %all-to-all-start = ((bf16[8,48,2048]{2,1,0:T(8,128)(2,1)}), bf16[8,48,2048]{2,1,0:T(8,128)(2,1)S(1)}, u32[]{:S(2)}, u32[]{:S(2)}) async-start(bf16[8,48,2048]{2,1,0:T(8,128)(2,1)} %broadcast_in_dim.12), calls=%async_computation | async-start | bytes 3145728 | tf_op jit(solution)/shard_map/all_to_all | solution.py:24
  105.5 20.6 %all-to-all-done = bf16[8,48,2048]{2,1,0:T(8,128)(2,1)S(1)} async-done(((bf16[8,48,2048]{2,1,0:T(8,128)(2,1)}), bf16[8,48,2048]{2,1,0:T(8,128)(2,1)S(1)}, u32[]{:S(2)}, u32[]{:S(2)}) %all-to-all-start) | async-done | bytes 1572896 | tf_op jit(solution)/shard_map/all_to_all | solution.py:24
  126.1 0.2 convert_reduce_fusion
  126.3 0.0 copy-start.5
  126.4 0.0 copy-start.6
  126.4 0.2 multiply_reduce_fusion
  126.6 0.1 multiply_convert_fusion
  126.7 0.6 copy-done.1
  127.3 0.1 broadcast_in_dim.15
  127.3 26.4 %all_to_all.30 = bf16[32,48,256]{2,1,0:T(8,128)(2,1)S(1)} all-to-all(bf16[32,48,256]{2,1,0:T(8,128)(2,1)S(1)} %broadcast_in_dim.15), channel_id=1, replica_groups=mesh['ep_0'=8,'ep_1'=4,'tp'=8] {'ep_0','ep_1'}, dimensions={0} | all-to-all | bytes 1572864 | tf_op jit(solution)/shard_map/all_to_all | solution.py:24
  153.7 1.7 convolution_convert_fusion
  155.5 0.0 reduce-scatter.4.cloned.1.call-update
  155.5 0.1 copy.91
  155.6 0.1 eq.48
  155.7 0.6 reduce-window.6
  156.4 0.2 slice_reduce_fusion
  156.6 0.1 bitcast_bitcast_fusion.2
  156.7 0.1 reduce_sum.93
  156.8 0.1 copy.94
  156.9 0.1 fusion.33
  157.0 0.6 convolution_convert_fusion.1
  157.6 1.6 reshape.116
  159.2 5.8 %all-to-all-start.1 = ((bf16[64,6,2048]{2,1,0:T(8,128)(2,1)}), bf16[64,6,2048]{2,1,0:T(8,128)(2,1)S(1)}, u32[]{:S(2)}, u32[]{:S(2)}) async-start(bf16[64,6,2048]{2,1,0:T(8,128)(2,1)} %reshape.116), calls=%async_computation.1 | async-start | bytes 4194304 | tf_op jit(solution)/shard_map/all_to_all | solution.py:152
  165.0 0.0 all-gather.6.cloned.1.call-start
  165.1 21.0 %reduce-scatter.4.cloned.1.call-done = bf16[192,512]{1,0:T(8,128)(2,1)} async-done(((bf16[1536,512]{1,0:T(8,128)(2,1)}), bf16[192,512]{1,0:T(8,128)(2,1)}) %reduce-scatter.4.cloned.1.call-update) | async-done | bytes 196624 | tf_op jit(solution)/shard_map/reduce_scatter | solution.py:60
  186.1 0.0 all-gather.6.cloned.1.call-update
  186.1 26.0 %all-to-all-done.1 = bf16[64,6,2048]{2,1,0:T(8,128)(2,1)S(1)} async-done(((bf16[64,6,2048]{2,1,0:T(8,128)(2,1)}), bf16[64,6,2048]{2,1,0:T(8,128)(2,1)S(1)}, u32[]{:S(2)}, u32[]{:S(2)}) %all-to-all-start.1) | async-done | bytes 1572896 | tf_op jit(solution)/shard_map/all_to_all | solution.py:152
  212.1 3.0 %convolution_bitcast_fusion.1 = f32[32,2,6,128]{3,0,2,1:T(8,128)} fusion(bf16[32,2,6,2048]{3,2,1,0:T(8,128)(2,1)S(1)} %bitcast.86, bf16[2,2048,128]{2,1,0:T(8,128)(2,1)} %param.36), kind=kOutput, calls=%fused_computation.16 | convolution fusion | flops 201326592 | bytes 2818048 | tf_op jit(solution)/shard_map/sexd,edf->sexf/dot_general | solution.py:155
  215.2 4.0 %fusion.2 = bf16[32,2,6,2048]{3,0,2,1:T(8,128)(2,1)} fusion(bf16[32,2,6,2048]{3,2,1,0:T(8,128)(2,1)S(1)} %bitcast.87, bf16[2,128,2048]{2,1,0:T(8,128)(2,1)S(1)} %copy-done, bf16[2,2048,128]{2,1,0:T(8,128)(2,1)} %param.37, f32[32,2,6,128]{3,0,2,1:T(8,128)} %convolution_bitcast_fusion.1), kind=kOutput, calls=%fused_computation.7 | convolution fusion | flops 403734528 | bytes 5439488 | tf_op jit(solution)/shard_map/sexf,efd->sexd/dot_general | solution.py:161
  219.2 2.8 copy.129
  221.9 7.5 %all-to-all-start.2 = ((bf16[8,32,2,6,256]{4,1,3,2,0:T(8,128)(2,1)}), bf16[8,32,2,6,256]{4,1,3,2,0:T(8,128)(2,1)S(1)}, u32[]{:S(2)}, u32[]{:S(2)}) async-start(bf16[8,32,2,6,256]{4,1,3,2,0:T(8,128)(2,1)} %bitcast.88), calls=%async_computation.2 | async-start | bytes 3145728 | tf_op jit(solution)/shard_map/all_to_all | solution.py:39
  229.4 1.8 convert_element_type.112
  231.3 2.4 convolution_convert_fusion.3
  233.7 0.0 reduce-scatter.6.cloned.1.call-update
  233.7 0.2 fusion.58
  234.0 1.6 convolution_convert_fusion.4
  235.6 0.7 copy.130
  236.3 13.8 %all-to-all-done.2 = bf16[8,32,2,6,256]{4,1,3,2,0:T(8,128)(2,1)S(1)} async-done(((bf16[8,32,2,6,256]{4,1,3,2,0:T(8,128)(2,1)}), bf16[8,32,2,6,256]{4,1,3,2,0:T(8,128)(2,1)S(1)}, u32[]{:S(2)}, u32[]{:S(2)}) %all-to-all-start.2) | async-done | bytes 1572896 | tf_op jit(solution)/shard_map/all_to_all | solution.py:39
  250.1 4.3 %all-to-all-start.4 = ((bf16[8,48,256]{2,1,0:T(8,128)(2,1)}), bf16[8,48,256]{2,1,0:T(8,128)(2,1)S(1)}, u32[]{:S(2)}, u32[]{:S(2)}) async-start(bf16[8,48,256]{2,1,0:T(8,128)(2,1)} %bitcast.85), calls=%async_computation.4 | async-start | bytes 393216 | tf_op jit(solution)/shard_map/all_to_all | solution.py:39
  254.3 0.1 select_reduce_fusion
  254.5 0.3 reduce_sum.97
  254.8 0.8 copy.111
  255.6 9.0 %reduce-scatter.6.cloned.1.call-done = bf16[192,256]{1,0:T(8,128)(2,1)} async-done(((bf16[1536,256]{1,0:T(8,128)(2,1)}), bf16[192,256]{1,0:T(8,128)(2,1)}) %reduce-scatter.6.cloned.1.call-update) | async-done | bytes 98320 | tf_op jit(solution)/shard_map/reduce_scatter | solution.py:70
  264.5 0.0 reduce-scatter.8.cloned.1.call-update
  264.6 7.3 %all-to-all-start.3 = ((bf16[64,6,256]{2,1,0:T(8,128)(2,1)}), bf16[64,6,256]{2,1,0:T(8,128)(2,1)S(1)}, u32[]{:S(2)}, u32[]{:S(2)}) async-start(bf16[64,6,256]{2,1,0:T(8,128)(2,1)} %bitcast.16), calls=%async_computation.3 | async-start | bytes 524288 | tf_op jit(solution)/shard_map/all_to_all | solution.py:164
  271.9 5.1 %multiply_add_fusion = f32[48,1,128,128]{3,2,1,0:T(8,128)} fusion(f32[48,1,128,128]{3,2,1,0:T(8,128)} %param.24, f32[48,128]{1,0:T(8,128)S(1)} %split.30, f32[48,128]{1,0:T(8,128)S(1)} %get-tuple-element.5, f32[48,128]{1,0:T(8,128)S(1)} %get-tuple-element.4), kind=kLoop, calls=%fused_computation.3 | loop fusion | flops 2359296 | bytes 6365184 | tf_op jit(solution)/shard_map/add | solution.py:128
  277.0 5.3 %all-to-all-done.3 = bf16[64,6,256]{2,1,0:T(8,128)(2,1)S(1)} async-done(((bf16[64,6,256]{2,1,0:T(8,128)(2,1)}), bf16[64,6,256]{2,1,0:T(8,128)(2,1)S(1)}, u32[]{:S(2)}, u32[]{:S(2)}) %all-to-all-start.3) | async-done | bytes 196640 | tf_op jit(solution)/shard_map/all_to_all | solution.py:164
  282.3 0.1 reshape.120
  282.3 9.4 %reduce-scatter.8.cloned.1.call-done = bf16[48,256]{1,0:T(8,128)(2,1)} async-done(((bf16[192,256]{1,0:T(8,128)(2,1)}), bf16[48,256]{1,0:T(8,128)(2,1)}) %reduce-scatter.8.cloned.1.call-update) | async-done | bytes 24592 | tf_op jit(solution)/shard_map/reduce_scatter | solution.py:70
  291.7 1.6 fusion.11
  (41 shorter events, 0.3 us)
Async XLA Ops:
  7.2 208.0 %copy-start = (bf16[2,128,2048]{2,1,0:T(8,128)(2,1)S(1)}, bf16[2,128,2048]{2,1,0:T(8,128)(2,1)}, u32[]{:S(2)}) copy-start(bf16[2,128,2048]{2,1,0:T(8,128)(2,1)} %param.38) | copy-start | bytes 3145732
  7.2 83.4 %copy-start.11 = (f32[128]{0:T(128)S(1)}, f32[128]{0:T(128)}, u32[]{:S(2)}) copy-start(f32[128]{0:T(128)} %param.30) | copy-start | bytes 1540
  7.2 81.0 %all-gather.4.cloned.1.call-start = ((), (), s32[]{:S(2)}) async-start(), calls=%async_computation.9 | async-start | bytes 2162688 | tf_op jit(solution)/shard_map/all_gather | solution.py:19
  90.5 3.7 %copy-start.3 = (bf16[128,2048]{1,0:T(8,128)(2,1)S(1)}, bf16[128,2048]{1,0:T(8,128)(2,1)}, u32[]{:S(2)}) copy-start(bf16[128,2048]{1,0:T(8,128)(2,1)} %param.32) | copy-start | bytes 1572868
  90.5 3.7 %copy-start.12 = (f32[128]{0:T(128)S(1)}, f32[128]{0:T(128)}, u32[]{:S(2)}) copy-start(f32[128]{0:T(128)} %param.31) | copy-start | bytes 1540
  95.8 30.5 %copy-start.2 = (bf16[48,2048]{1,0:T(8,128)(2,1)S(1)}, bf16[48,2048]{1,0:T(8,128)(2,1)}, u32[]{:S(2)}) copy-start(bf16[48,2048]{1,0:T(8,128)(2,1)} %param.23) | copy-start | bytes 589828
  95.8 30.3 %all-to-all-start = ((bf16[8,48,2048]{2,1,0:T(8,128)(2,1)}), bf16[8,48,2048]{2,1,0:T(8,128)(2,1)S(1)}, u32[]{:S(2)}, u32[]{:S(2)}) async-start(bf16[8,48,2048]{2,1,0:T(8,128)(2,1)} %broadcast_in_dim.12), calls=%async_computation | async-start | bytes 3145728 | tf_op jit(solution)/shard_map/all_to_all | solution.py:24
  105.5 21.0 %copy-start.7 = (f32[2048]{0:T(1024)S(1)}, f32[2048]{0:T(1024)}, u32[]{:S(2)}) copy-start(f32[2048]{0:T(1024)} %param.33) | copy-start | bytes 24580
  105.5 80.5 %reduce-scatter.4.cloned.1.call-start = ((), (), s32[]{:S(2)}) async-start(), calls=%async_computation.10 | async-start | bytes 1769472 | tf_op jit(solution)/shard_map/reduce_scatter | solution.py:60
  126.3 27.4 %copy-start.5 = (bf16[256,256]{1,0:T(8,128)(2,1)S(1)}, bf16[256,256]{1,0:T(8,128)(2,1)}, u32[]{:S(2)}) copy-start(bf16[256,256]{1,0:T(8,128)(2,1)} %param.43) | copy-start | bytes 393220
  126.4 27.4 %copy-start.6 = (bf16[256,256]{1,0:T(8,128)(2,1)S(1)}, bf16[256,256]{1,0:T(8,128)(2,1)}, u32[]{:S(2)}) copy-start(bf16[256,256]{1,0:T(8,128)(2,1)} %param.42) | copy-start | bytes 393220
  126.5 0.7 copy-start.1
  153.7 1.8 copy-start.8
  159.2 52.9 %all-to-all-start.1 = ((bf16[64,6,2048]{2,1,0:T(8,128)(2,1)}), bf16[64,6,2048]{2,1,0:T(8,128)(2,1)S(1)}, u32[]{:S(2)}, u32[]{:S(2)}) async-start(bf16[64,6,2048]{2,1,0:T(8,128)(2,1)} %reshape.116), calls=%async_computation.1 | async-start | bytes 4194304 | tf_op jit(solution)/shard_map/all_to_all | solution.py:152
  165.0 64.4 %all-gather.6.cloned.1.call-start = ((), (), s32[]{:S(2)}) async-start(), calls=%async_computation.13 | async-start | bytes 1769472 | tf_op jit(solution)/shard_map/all_gather | solution.py:63
  221.9 28.1 %all-to-all-start.2 = ((bf16[8,32,2,6,256]{4,1,3,2,0:T(8,128)(2,1)}), bf16[8,32,2,6,256]{4,1,3,2,0:T(8,128)(2,1)S(1)}, u32[]{:S(2)}, u32[]{:S(2)}) async-start(bf16[8,32,2,6,256]{4,1,3,2,0:T(8,128)(2,1)} %bitcast.88), calls=%async_computation.2 | async-start | bytes 3145728 | tf_op jit(solution)/shard_map/all_to_all | solution.py:39
  229.4 35.1 %reduce-scatter.6.cloned.1.call-start = ((), (), s32[]{:S(2)}) async-start(), calls=%async_computation.11 | async-start | bytes 884736 | tf_op jit(solution)/shard_map/reduce_scatter | solution.py:70
  231.3 2.4 copy-start.4
  233.7 20.6 %copy-start.10 = (f32[256]{0:T(256)S(1)}, f32[256]{0:T(256)}, u32[]{:S(2)}) copy-start(f32[256]{0:T(256)} %param.45) | copy-start | bytes 3076
  233.7 20.6 %copy-start.9 = (f32[48,4]{0,1:T(4,128)S(1)}, f32[48,4]{0,1:T(4,128)}, u32[]{:S(2)}) copy-start(f32[48,4]{0,1:T(4,128)} %param.35) | copy-start | bytes 2308
  250.1 14.5 %all-to-all-start.4 = ((bf16[8,48,256]{2,1,0:T(8,128)(2,1)}), bf16[8,48,256]{2,1,0:T(8,128)(2,1)S(1)}, u32[]{:S(2)}, u32[]{:S(2)}) async-start(bf16[8,48,256]{2,1,0:T(8,128)(2,1)} %bitcast.85), calls=%async_computation.4 | async-start | bytes 393216 | tf_op jit(solution)/shard_map/all_to_all | solution.py:39
  254.3 37.4 %reduce-scatter.8.cloned.1.call-start = ((), (), s32[]{:S(2)}) async-start(), calls=%async_computation.12 | async-start | bytes 122880 | tf_op jit(solution)/shard_map/reduce_scatter | solution.py:70
  264.6 17.7 %all-to-all-start.3 = ((bf16[64,6,256]{2,1,0:T(8,128)(2,1)}), bf16[64,6,256]{2,1,0:T(8,128)(2,1)S(1)}, u32[]{:S(2)}, u32[]{:S(2)}) async-start(bf16[64,6,256]{2,1,0:T(8,128)(2,1)} %bitcast.16), calls=%async_computation.3 | async-start | bytes 524288 | tf_op jit(solution)/shard_map/all_to_all | solution.py:164
Sparse Core Ops, SparseCore 0:
  11.2 77.0 all-gather.3
  155.6 30.3 reduce-scatter.3
  187.9 28.7 all-gather.5
  233.8 30.6 reduce-scatter.5
  266.9 24.7 reduce-scatter.7
where the time goes:
time: 302 us; the launch traced here: 300 us
  waiting for transfers between devices  183 us (61%)
  starting transfers between devices  34.6 us (11%)
  blocking collectives  26.4 us (9%)
  matrix products  21.1 us (7%)
  between operations  14.1 us (5%)
  other arithmetic  12.1 us (4%)
  local copies, waits for them, and re-layouts  8.57 us (3%)
    all_gather x1, waiting for transfers between devices, side_by_side(): lax.all_gather(both, axis, axis=dim, tiled=True)  77.7 us
    all_to_all x1, blocking collectives, from_everyone(): return lax.all_to_all(copies, axis, split_axis=0, concat_axis=0, tiled=True)  26.4 us
    all_to_all x1, waiting for transfers between devices, local(): lax.all_to_all(outgoing, EP, split_axis=0, concat_axis=0, tiled=True)  26 us
    reduce_scatter x1, waiting for transfers between devices, total_of(): lax.psum_scatter(padded_to(lines, lax.axis_size(axis)), axis, scatter_dim...  21 us
    all_to_all x1, waiting for transfers between devices, from_everyone(): return lax.all_to_all(copies, axis, split_axis=0, concat_axis=0, tiled=True)  20.6 us
    reduce_scatter x2, waiting for transfers between devices, sum_by_axis(): subtotal = lax.psum_scatter(subtotal, axis, scatter_dimension=0, tiled=True)  18.3 us
    all_to_all x2, waiting for transfers between devices, sum_at_owner(): lax.all_to_all(parts, axis, split_axis=0, concat_axis=0, tiled=True)  13.8 us
    all_to_all x2, starting transfers between devices, sum_at_owner(): lax.all_to_all(parts, axis, split_axis=0, concat_axis=0, tiled=True)  11.8 us
  transfers between devices with their start and end apart: 10, of which 8 were waited for; matrix products, arithmetic and copies ran while one was open for 9% of the time, Pallas kernels for 0%

commit v1 on v0

v1 whole, which is shorter than its diff:
```python
import functools

import jax
import jax.numpy as jnp
from jax import lax
from jax.experimental import pallas as pl
from jax.experimental.pallas import tpu as pltpu
from jax.sharding import Mesh
from jax.sharding import PartitionSpec as P

EP = ("z", "x")
TP = ("y", "c")
NZ, NX, NY, NC = 8, 4, 4, 2
NE, NT = NZ * NX, NY * NC
MESH = pl.DeviceIdType.MESH
EPS = 1e-06

Z_ORDER = (1, 7, 2, 6, 3, 5, 4)
Y_ORDER = (1, 3, 2)


def whole(ref, index):
    return ref.at[index]


def lanes(width):
    def view(ref, index):
        start = pl.multiple_of(index * width, width)
        return ref.at[(slice(None),) * (len(ref.shape) - 1) + (pl.ds(start, width),)]

    return view


class Links:
    def __init__(self, send_sem, recv_sem):
        self.send_sem, self.recv_sem = send_sem, recv_sem
        self.sent = self.received = 0
        self.z, self.x = lax.axis_index("z"), lax.axis_index("x")
        self.y, self.c = lax.axis_index("y"), lax.axis_index("c")
        self.e = self.z * NX + self.x
        self.t = self.y * NC + self.c
        self.copies = []

    def reserve(self, number):
        first = self.received
        self.received += number
        return first

    def send(self, src, dst, slot, **device):
        copy = pltpu.make_async_remote_copy(
            src_ref=src,
            dst_ref=dst,
            send_sem=self.send_sem.at[self.sent],
            recv_sem=self.recv_sem.at[slot],
            device_id=device,
            device_id_type=MESH,
        )
        self.sent += 1
        copy.start()
        self.copies.append(copy)

    def wait(self, dst, slot):
        pltpu.make_async_remote_copy(
            src_ref=dst,
            dst_ref=dst,
            send_sem=self.send_sem.at[0],
            recv_sem=self.recv_sem.at[slot],
            device_id={"c": 1 - self.c},
            device_id_type=MESH,
        ).wait_recv()

    def finish(self):
        for copy in self.copies:
            copy.wait_send()


class GatherEp:
    peers = "zx"
    sends, receives = 7 + 3 * 8, 32

    def __init__(self, dst_view=whole):
        self.view = dst_view

    def begin(self, n, src, dst):
        self.base = n.reserve(32)
        mine = self.view(dst, n.e)
        for dz in Z_ORDER:
            n.send(src, mine, self.base + n.e, z=(n.z + dz) % NZ)
        for dx in (1, 3, 2):
            n.send(src, mine, self.base + n.e, x=(n.x + dx) % NX)
        mine[...] = src[...]

    def stages(self, n, src, dst):
        for dz in Z_ORDER:
            e = ((n.z + dz) % NZ) * NX + n.x
            block = self.view(dst, e)
            n.wait(block, self.base + e)
            for dx in (1, 3, 2):
                n.send(block, block, self.base + e, x=(n.x + dx) % NX)
            yield
        for dz in (0,) + Z_ORDER:
            for dx in (1, 3, 2):
                e = ((n.z + dz) % NZ) * NX + (n.x + dx) % NX
                n.wait(self.view(dst, e), self.base + e)


class GatherTp:
    peers = "yc"
    sends, receives = 3 + 1 + 3, 8

    def __init__(self, dst_view=whole):
        self.view = dst_view

    def begin(self, n, src, dst):
        self.base = n.reserve(8)
        mine = self.view(dst, n.t)
        for dy in Y_ORDER:
            n.send(src, mine, self.base + n.t, y=(n.y + dy) % NY)
        n.send(src, mine, self.base + n.t, c=1 - n.c)
        mine[...] = src[...]

    def stages(self, n, src, dst):
        for dy in Y_ORDER:
            t = ((n.y + dy) % NY) * NC + n.c
            block = self.view(dst, t)
            n.wait(block, self.base + t)
            n.send(block, block, self.base + t, c=1 - n.c)
            yield
        for dy in (0,) + Y_ORDER:
            t = ((n.y + dy) % NY) * NC + 1 - n.c
            n.wait(self.view(dst, t), self.base + t)


class SwapTp:
    peers = "yct"
    sends, receives = 7, 8

    def __init__(self, src_view=whole, dst_view=whole):
        self.src_view, self.view = src_view, dst_view

    def begin(self, n, src, dst):
        self.base = n.reserve(8)
        mine = self.view(dst, n.t)
        for dy in Y_ORDER:
            for dc in (0, 1):
                y, c = (n.y + dy) % NY, (n.c + dc) % NC
                n.send(self.src_view(src, y * NC + c), mine, self.base + n.t, y=y, c=c)
        other = n.y * NC + 1 - n.c
        n.send(self.src_view(src, other), mine, self.base + n.t, c=1 - n.c)
        mine[...] = self.src_view(src, n.t)[...]

    def stages(self, n, src, dst):
        yield
        for dy in (0,) + Y_ORDER:
            for dc in (0, 1):
                if dy or dc:
                    t = ((n.y + dy) % NY) * NC + (n.c + dc) % NC
                    n.wait(self.view(dst, t), self.base + t)


class SwapEp:
    peers = "e"
    sends, receives = 31, 32

    def begin(self, n, src, dst):
        self.base = n.reserve(32)
        for dz in (4, 3, 5, 2, 6, 1, 7, 0):
            for dx in (2, 1, 3, 0):
                if dz or dx:
                    z, x = (n.z + dz) % NZ, (n.x + dx) % NX
                    n.send(src.at[z * NX + x], dst.at[n.e], self.base + n.e, z=z, x=x)
        dst.at[n.e][...] = src.at[n.e][...]

    def stages(self, n, src, dst):
        yield
        for dz in range(NZ):
            for dx in range(NX):
                if dz or dx:
                    e = ((n.z + dz) % NZ) * NX + (n.x + dx) % NX
                    n.wait(dst.at[e], self.base + e)


def greet(n, kinds):
    barrier = pltpu.get_barrier_semaphore()
    peers = []
    if "e" in kinds:
        for dz in range(NZ):
            for dx in range(NX):
                if dz or dx:
                    peers.append(dict(z=(n.z + dz) % NZ, x=(n.x + dx) % NX))
    elif "z" in kinds:
        peers += [dict(z=(n.z + dz) % NZ) for dz in range(1, NZ)]
        peers += [dict(x=(n.x + dx) % NX) for dx in range(1, NX)]
    if "t" in kinds:
        for dy in range(1, NY):
            for dc in (0, 1):
                peers.append(dict(y=(n.y + dy) % NY, c=(n.c + dc) % NC))
    elif "y" in kinds:
        peers += [dict(y=(n.y + dy) % NY) for dy in range(1, NY)]
    if "c" in kinds:
        peers.append(dict(c=1 - n.c))
    for peer in peers:
        pl.semaphore_signal(barrier, inc=1, device_id=peer, device_id_type=MESH)
    pl.semaphore_wait(barrier, len(peers))


def mover(plans, *refs):
    count = len(plans)
    srcs, dsts = refs[:count], refs[count : 2 * count]
    n = Links(*refs[2 * count :])
    greet(n, "".join(plan.peers for plan in plans))
    for plan, src, dst in zip(plans, srcs, dsts):
        plan.begin(n, src, dst)
    running = [plan.stages(n, src, dst) for plan, src, dst in zip(plans, srcs, dsts)]
    while running:
        running = [stage for stage in running if next(stage, running) is not running]
    n.finish()


def move(ident, name, *jobs):
    plans = [job[0] for job in jobs]
    arrays = [job[1] for job in jobs]
    shapes = [jax.ShapeDtypeStruct(job[2], job[1].dtype) for job in jobs]
    vmem = pl.BlockSpec(memory_space=pltpu.VMEM)
    return pl.pallas_call(
        functools.partial(mover, plans),
        out_shape=shapes,
        in_specs=[vmem] * len(jobs),
        out_specs=[vmem] * len(jobs),
        scratch_shapes=[
            pltpu.SemaphoreType.DMA((sum(plan.sends for plan in plans),)),
            pltpu.SemaphoreType.DMA((sum(plan.receives for plan in plans),)),
        ],
        compiler_params=pltpu.CompilerParams(collective_id=ident, has_side_effects=True),
        name=name,
    )(*arrays)


def rms_scale(values, gain):
    values = values.astype(jnp.float32)
    return values * lax.rsqrt(jnp.mean(values * values, axis=-1, keepdims=True) + EPS) * gain


def rounded(values):
    return lax.optimization_barrier(values.astype(jnp.bfloat16)).astype(jnp.float32)


def dot(left, right):
    return jnp.dot(left, right, preferred_element_type=jnp.float32)


def local(
    tokens,
    state,
    norm_gain,
    w_query,
    w_forget,
    w_input,
    w_outgate,
    lower_bound,
    head_gain,
    w_output,
    ffn_gain,
    route_ids,
    route_weight,
    expert_gate,
    expert_up,
    expert_down,
    shared_gate,
    shared_up,
    shared_down,
    dense_gate,
    dense_up,
    dense_down,
    dense_mix,
):
    bf16, f32 = jnp.bfloat16, jnp.float32
    seq, width = tokens.shape
    batch = seq * NE
    wide = width // NT
    topk = route_ids.shape[1]
    exp_local = expert_gate.shape[0]
    capacity = max(2, 2 * seq * topk // (exp_local * NE))
    slots = NE * capacity
    e_index = lax.axis_index(EP)
    t_index = lax.axis_index(TP)

    joined = jnp.concatenate((w_query, w_forget, w_input, w_outgate), axis=1)
    dense_joined = jnp.concatenate((dense_gate, dense_up), axis=1)
    routes = jnp.stack([route_ids.astype(f32).T, route_weight.T]).reshape(2 * topk, seq)
    routes = jnp.pad(routes, ((0, 0), (0, 128 - seq)))
    down_blocks = expert_down.reshape(exp_local * expert_down.shape[1], width)
    w_all, routes_all, dense_all, down_all = move(
        0,
        "gather_weights",
        (GatherEp(), joined, (NE, *joined.shape)),
        (GatherEp(), routes, (NE, *routes.shape)),
        (GatherTp(), dense_joined, (NT, *dense_joined.shape)),
        (SwapTp(lanes(wide)), down_blocks, (NT, down_blocks.shape[0], wide)),
    )

    normed = rms_scale(tokens, norm_gain).astype(bf16)
    projected = rounded(dot(normed, w_all.reshape(width, -1)))
    query, forget_pre, values, out_gate = jnp.split(projected, 4, axis=1)
    shape = (seq, 1, query.shape[1])
    forget_sig = jax.nn.sigmoid(forget_pre)
    decay = (lower_bound + (1.0 - lower_bound) * forget_sig).reshape(shape)
    keygate = ((1.0 - lower_bound) * (1.0 - forget_sig)).reshape(shape)
    new_state = decay[..., None] * state + keygate[..., None] * values.reshape(shape)[:, :, None, :]
    readout = jnp.einsum("bhk,bhkv->bhv", query.reshape(shape), new_state)
    readout = readout * lax.rsqrt(jnp.mean(readout * readout, axis=-1, keepdims=True) + EPS)
    head_out = (readout.reshape(seq, -1) * head_gain * jax.nn.silu(out_gate)).astype(bf16)
    head_part = dot(head_out, w_output).astype(bf16)

    (head_parts,) = move(1, "swap_heads", (SwapTp(lanes(wide)), head_part, (NT, seq, wide)))
    own_tokens = lax.dynamic_slice_in_dim(tokens, t_index * wide, wide, 1)
    own_resid = own_tokens.astype(f32) + head_parts.astype(f32).sum(axis=0)
    resid_cols = own_resid.astype(bf16)

    cols_all, resid_rows = move(
        2,
        "gather_resid",
        (GatherEp(), resid_cols, (NE, seq, wide)),
        (GatherTp(lanes(wide)), resid_cols, (seq, width)),
    )
    cols_all = cols_all.reshape(batch, wide)

    ids = routes_all[:, :topk, :seq].astype(jnp.int32)
    weights = routes_all[:, topk:, :seq]
    experts = e_index * exp_local + jnp.arange(exp_local, dtype=jnp.int32)
    named = ids[None] == experts[:, None, None, None]
    token_weight = jnp.sum(jnp.where(named, weights[None], 0.0), axis=2)
    hit = jnp.any(named, axis=2)
    earlier = jnp.triu(jnp.ones((seq, seq), bf16), 1)
    rank = jnp.einsum("jeb,bc->jec", hit.astype(bf16), earlier, preferred_element_type=f32)
    slot = jnp.arange(NE, dtype=jnp.int32)[None, :, None] * capacity + rank.astype(jnp.int32)
    slot = jnp.where(hit, slot, -1).reshape(exp_local, 1, batch)
    pick = (slot == jnp.arange(slots, dtype=jnp.int32)[None, :, None]).astype(bf16)
    chosen = dot(pick.reshape(exp_local * slots, batch), cols_all).astype(bf16)

    dense_rows, chosen_rows = move(
        3,
        "swap_rows",
        (SwapTp(dst_view=lanes(wide)), cols_all.reshape(NT, batch // NT, wide), (batch // NT, width)),
        (GatherTp(lanes(wide)), chosen, (exp_local * slots, width)),
    )

    dense_in = rms_scale(dense_rows, ffn_gain).astype(bf16)
    dense_pre = dot(dense_in, dense_all.reshape(width, -1))
    dense_gate_pre, dense_up_pre = jnp.split(dense_pre, 2, axis=1)
    dense_hidden = (jax.nn.silu(dense_gate_pre) * dense_up_pre).astype(bf16)

    expert_in = rms_scale(chosen_rows, ffn_gain).astype(bf16).reshape(exp_local, slots, width)
    gate_pre = jnp.einsum("jsd,jdf->jsf", expert_in, expert_gate, preferred_element_type=f32)
    up_pre = jnp.einsum("jsd,jdf->jsf", expert_in, expert_up, preferred_element_type=f32)
    hidden = (jax.nn.silu(gate_pre) * up_pre).astype(bf16).reshape(exp_local * slots, -1)

    shared_in = rms_scale(resid_rows, ffn_gain).astype(bf16)
    shared_hidden = (jax.nn.silu(dot(shared_in, shared_gate)) * dot(shared_in, shared_up)).astype(bf16)
    shared_part = dot(shared_hidden, shared_down).astype(bf16)

    dense_hidden_all, hidden_all, shared_parts = move(
        4,
        "gather_hidden",
        (GatherTp(), dense_hidden, (NT, *dense_hidden.shape)),
        (GatherTp(lanes(hidden.shape[1])), hidden, (hidden.shape[0], NT * hidden.shape[1])),
        (SwapTp(lanes(wide)), shared_part, (NT, seq, wide)),
    )
    shared_out = shared_parts.astype(f32).sum(axis=0)
    dense_out = dot(dense_hidden_all.reshape(batch, -1), dense_down) * jax.nn.sigmoid(dense_mix)
    hidden_all = hidden_all.reshape(exp_local, slots, -1)
    down = down_all.reshape(NT, exp_local, -1, wide).transpose(1, 0, 2, 3)
    down = down.reshape(exp_local, -1, wide)
    expert_out = jnp.einsum("jsf,jfd->jsd", hidden_all, down, preferred_element_type=f32)
    expert_out = expert_out.astype(bf16)
    back = jnp.einsum("jsb,jsd->jbd", pick, expert_out, preferred_element_type=f32)
    routed = jnp.sum(back * token_weight.reshape(exp_local, batch, 1), axis=0)
    partial = (dense_out + routed).astype(bf16).reshape(NE, seq, wide)

    (partials,) = move(5, "swap_partials", (SwapEp(), partial, (NE, seq, wide)))
    mixed = own_resid + shared_out + partials.astype(f32).sum(axis=0)
    return mixed.astype(bf16), new_state


def solution(mesh):
    torus = Mesh(mesh.devices.reshape(NZ, NX, NY, NC), ("z", "x", "y", "c"))
    return jax.shard_map(
        local,
        mesh=torus,
        in_specs=(
            P(EP, None),
            P(EP, TP, None, None),
            P(),
            P(EP, TP),
            P(EP, TP),
            P(EP, TP),
            P(EP, TP),
            P(TP),
            P(TP),
            P(TP, None),
            P(),
            P(EP, None),
            P(EP, None),
            P(EP, None, TP),
            P(EP, None, TP),
            P(EP, TP, None),
            P(None, TP),
            P(None, TP),
            P(TP, None),
            P(TP, EP),
            P(TP, EP),
            P(EP, TP),
            P(TP),
        ),
        out_specs=(P(EP, TP), P(EP, TP, None, None)),
        check_vma=False,
    )
```

time: 302 us -> 199 us (0.66)
  waiting for transfers between devices: 183 us -> 0 us
  Pallas kernels: 0 us -> 155 us
  starting transfers between devices: 34.6 us -> 0 us
  blocking collectives: 26.4 us -> 0 us
  between operations: 14.1 us -> 1.12 us
  other arithmetic: 12.1 us -> 18 us
  local copies, waits for them, and re-layouts: 8.57 us -> 3.77 us
    pallas_call x0 -> x6, Pallas kernels: none -> 155 us  [move(): pl.pallas_call(functools.partial(mover, plans), out_shape=shapes, in_spec...]
    all_gather x2 -> x0, waiting for transfers between devices: 77.7 us -> none  [the longest x1 77.7 us: side_by_side(): lax.all_gather(both, axis, axis=dim, tiled=True)]
    all_to_all x5 -> x0, waiting for transfers between devices: 65.7 us -> none  [the longest x1 26 us: local(): lax.all_to_all(outgoing, EP, split_axis=0, concat_axis=0, tiled=True)]
    reduce_scatter x3 -> x0, waiting for transfers between devices: 39.4 us -> none  [the longest x1 21 us: total_of(): lax.psum_scatter(padded_to(lines, lax.axis_size(axis)), axis, scatter_dim...]
    all_to_all x5 -> x0, starting transfers between devices: 34.5 us -> none  [the longest x2 11.8 us: sum_at_owner(): lax.all_to_all(parts, axis, split_axis=0, concat_axis=0, tiled=True)]
    all_to_all x1 -> x0, blocking collectives: 26.4 us -> none  [from_everyone(): return lax.all_to_all(copies, axis, split_axis=0, concat_axis=0, tiled=True)]
    reshape x5 -> x1, local copies, waits for them, and re-layouts: 5.94 us -> 1.04 us  [local(): down = down_all.reshape(NT, exp_local, -1, wide).transpose(1, 0, 2, 3)]
    dot_general x10 -> x11, matrix products: 17.7 us -> 17.4 us  [the longest x7 12.6 us: dot(): return jnp.dot(left, right, preferred_element_type=jnp.float32)]
  transfers between devices with their start and end apart: 10 -> 0, of which waited for: 8 -> 0; matrix products, arithmetic and copies ran while one was open for 9% -> 0% of each run, Pallas kernels for 0% -> 0%
where the time goes in v1:
time: 199 us
  Pallas kernels  155 us (78%)
  matrix products  20.8 us (10%)
  other arithmetic  18 us (9%)
  local copies, waits for them, and re-layouts  3.77 us (2%)
    pallas_call x6, Pallas kernels, move(): pl.pallas_call(functools.partial(mover, plans), out_shape=shapes, in_spec...  155 us
    dot_general x7, matrix products, dot(): return jnp.dot(left, right, preferred_element_type=jnp.float32)  12.6 us
    add x1, other arithmetic, local(): decay[..., None] * state  5.07 us

profile of v1, /device:TPU:1, one launch (start us, length us, event | category | flops | bytes accessed | tf_op | source)
XLA Modules:
  0.0 198.7 jit_solution(12141004106329647248)
XLA Ops:
  0.6 0.0 copy-start
  0.6 0.0 copy-start.4
  0.7 0.0 copy-start.23
  0.7 1.5 pad_maximum_fusion.1.refs_0_
  2.2 0.7 convert_bitcast_fusion
  2.8 0.7 pad_maximum_fusion.2
  3.5 0.6 pad.4.refs_1_
  4.1 1.7 pad_maximum_fusion.refs_2_
  5.8 57.8 %gather_weights.1 = (bf16[32,64,512]{2,1,0:T(8,128)(2,1)}, f32[32,8,128]{2,1,0:T(8,128)}, bf16[8,256,512]{2,1,0:T(8,128)(2,1)}, bf16[8,256,256]{2,1,0:T(8,128)(2,1)}) custom-call(bf16[64,512]{1,0:T(8,128)(2,1)} %pad_maximum_fusion.1.refs_0_, f32[8,128]{1,0:T(8,128)} %pad.4.refs_1_, bf16[256,512]{1,0:T(8,128)(2,1)} %pad_maximum_fusion.refs_2_, ...), custom_call_target="tpu_custom_call" | custom-call | tf_op jit(solution)/shard_map/gather_weights/pallas_call | solution.py:225
  63.7 0.0 copy-start.25
  63.7 1.0 slice_convert_fusion
  64.7 0.1 fusion.29
  64.8 0.7 mul.257
  65.5 0.0 copy-done.4
  65.5 0.1 fusion.19
  65.7 0.0 copy-done.23
  65.7 2.1 %convolution_convert_fusion.4 = bf16[48,512]{1,0:T(8,128)(2,1)S(1)} fusion(bf16[2048,512]{1,0:T(8,128)(2,1)} %bitcast.62, bf16[48,2048]{1,0:T(8,128)(2,1)S(1)} %copy-done.4, f32[2048]{0:T(1024)S(1)} %copy-done.23, f32[48]{0:T(128)S(1)} %add_rsqrt_fusion.4), kind=kOutput, calls=%fused_computation.26 | convolution fusion | flops 101081088 | bytes 2351296 | tf_op jit(solution)/shard_map/dot_general | solution.py:249
  67.8 0.0 copy-start.5
  67.8 0.0 copy-start.26
  67.8 0.0 copy-done.25
  67.9 0.0 copy-start.11
  67.9 0.5 copy-done.11
  68.5 3.4 %fusion.3 = f32[48,1,128]{2,1,0:T(1,128)S(1)} fusion(bf16[48,128,1]{1,0,2:T(8,128)(2,1)S(1)} %slice_bitcast_fusion, f32[48,128]{1,0:T(8,128)S(1)} %split.26, f32[48,128]{1,0:T(8,128)S(1)} %get-tuple-element.27, f32[48,1,128,128]{3,2,1,0:T(8,128)} %param.24, f32[48,128]{1,0:T(8,128)S(1)} %get-tuple-element.26), kind=kOutput, calls=%fused_computation.6 | convolution fusion | flops 3932160 | bytes 3256320 | tf_op jit(solution)/shard_map/bhk,bhkv->bhv/dot_general | solution.py:310
  71.9 0.0 copy-done.13
  71.9 0.1 multiply_reduce_fusion
  72.0 0.9 convolution_convert_fusion.1.refs_0_
  73.0 8.1 %swap_heads.1 = bf16[8,48,256]{2,1,0:T(8,128)(2,1)} custom-call(bf16[48,2048]{1,0:T(8,128)(2,1)} %convolution_convert_fusion.1.refs_0_), custom_call_target="tpu_custom_call" | custom-call | tf_op jit(solution)/shard_map/swap_heads/pallas_call | solution.py:225
  81.0 1.0 convert_reduce_fusion.2
  82.0 0.6 fusion.34.refs_0_.refs_1_
  82.6 16.8 %gather_resid.1 = (bf16[32,48,256]{2,1,0:T(8,128)(2,1)}, bf16[48,2048]{1,0:T(8,128)(2,1)}) custom-call(bf16[48,256]{1,0:T(8,128)(2,1)} %fusion.34.refs_0_.refs_1_, bf16[48,256]{1,0:T(8,128)(2,1)} %fusion.34.refs_0_.refs_1_), custom_call_target="tpu_custom_call" | custom-call | tf_op jit(solution)/shard_map/gather_resid/pallas_call | solution.py:225
  99.4 0.1 compare_reduce_fusion
  99.5 0.1 fusion.13
  99.6 0.1 eq.41
  99.8 0.0 copy-start.19
  99.8 0.0 copy-start.27
  99.8 0.3 iota_compare_fusion
  100.1 2.5 %convolution_convert_fusion.3.refs_1_ = bf16[384,256]{1,0:T(8,128)(2,1)} fusion(pred[384,1536]{1,0:T(32,128)(4,1)S(1)} %bitcast.69, bf16[1536,256]{1,0:T(8,128)(2,1)} %bitcast.66), kind=kOutput, calls=%fused_computation.23 | convolution fusion | flops 302088192 | bytes 1572864 | tf_op jit(solution)/shard_map/dot_general | solution.py:249
  102.6 26.2 %swap_rows.1 = (bf16[192,2048]{1,0:T(8,128)(2,1)}, bf16[384,2048]{1,0:T(8,128)(2,1)}) custom-call(bf16[8,192,256]{2,1,0:T(8,128)(2,1)} %bitcast.67, bf16[384,256]{1,0:T(8,128)(2,1)} %convolution_convert_fusion.3.refs_1_), custom_call_target="tpu_custom_call" | custom-call | tf_op jit(solution)/shard_map/swap_rows/pallas_call | solution.py:225
  128.8 1.4 fusion.8
  130.2 1.9 fusion.15
  132.1 0.7 fusion.26.refs_0_
  132.8 0.4 fusion
  133.2 0.4 fusion.2
  133.6 0.0 copy-start.28
  133.6 0.0 copy-done
  133.6 0.6 fusion.60
  134.2 0.6 copy-done.28
  134.8 1.2 fusion.11
  136.1 0.1 fusion.22
  136.2 0.0 copy-done.6
  136.2 0.9 fusion.32
  137.1 1.9 convolution_convert_fusion.refs_2_
  139.0 18.6 %gather_hidden.1 = (bf16[8,192,256]{2,1,0:T(8,128)(2,1)}, bf16[384,1024]{1,0:T(8,128)(2,1)}, bf16[8,48,256]{2,1,0:T(8,128)(2,1)}) custom-call(bf16[192,256]{1,0:T(8,128)(2,1)} %fusion.26.refs_0_, bf16[384,128]{1,0:T(8,128)(2,1)} %bitcast.72, bf16[48,2048]{1,0:T(8,128)(2,1)} %convolution_convert_fusion.refs_2_), custom_call_target="tpu_custom_call" | custom-call | tf_op jit(solution)/shard_map/gather_hidden/pallas_call | solution.py:225
  157.6 0.0 copy-done.3
  157.7 1.0 copy.30
  158.7 2.9 %fusion.7 = f32[1536,256]{1,0:T(8,128)S(1)} fusion(f32[2,1536]{1,0:T(2,128)S(1)} %copy-done.22, bf16[2,192,1024]{2,1,0:T(8,128)(2,1)} %bitcast.76, bf16[2,1024,256]{2,1,0:T(8,128)(2,1)} %bitcast.65, s32[2,1536]{1,0:T(2,128)S(1)} %copy-done.21), kind=kOutput, calls=%fused_computation.17 | convolution fusion | flops 505184256 | bytes 3432448 | tf_op jit(solution)/shard_map/jsb,jsd->jbd/dot_general | solution.py:376
  161.7 0.0 copy-done.18
  161.7 0.0 copy-start.17
  161.7 2.4 %fusion.6 = bf16[1536,256]{1,0:T(8,128)(2,1)} fusion(f32[1536,256]{1,0:T(8,128)S(1)} %fusion.7, bf16[1536,256]{1,0:T(8,128)(2,1)} %bitcast.68, bf16[256,256]{1,0:T(8,128)(2,1)S(1)} %copy-done.18, f32[256]{0:T(256)S(1)} %add_divide_fusion), kind=kOutput, calls=%fused_computation.11 | convolution fusion | flops 202506240 | bytes 3277824 | tf_op jit(solution)/shard_map/dot_general | solution.py:249
  164.1 27.5 %swap_partials.1 = bf16[32,48,256]{2,1,0:T(8,128)(2,1)} custom-call(bf16[32,48,256]{2,1,0:T(8,128)(2,1)} %bitcast.61), custom_call_target="tpu_custom_call" | custom-call | tf_op jit(solution)/shard_map/swap_partials/pallas_call | solution.py:225
  191.7 1.3 convert_reduce_fusion
  193.0 0.6 add_convert_fusion
  193.6 0.0 copy-done.16
  193.6 5.1 %multiply_add_fusion = f32[48,1,128,128]{3,2,1,0:T(8,128)} fusion(f32[48,1,128,128]{3,2,1,0:T(8,128)} %param.24, f32[48,128]{1,0:T(8,128)S(1)} %copy-done.12, f32[48,128]{1,0:T(8,128)S(1)} %copy-done.16, f32[48,128]{1,0:T(8,128)S(1)} %copy-done.14), kind=kLoop, calls=%fused_computation.8 | loop fusion | flops 2359296 | bytes 6365184 | tf_op jit(solution)/shard_map/add | solution.py:309
  (52 shorter events, 0.2 us)
Async XLA Ops:
  0.6 133.0 %copy-start = (bf16[2,2048,128]{2,1,0:T(8,128)(2,1)S(1)}, bf16[2,2048,128]{2,1,0:T(8,128)(2,1)}, u32[]{:S(2)}) copy-start(bf16[2,2048,128]{2,1,0:T(8,128)(2,1)} %param.36) | copy-start | bytes 3145732
  0.6 64.9 %copy-start.4 = (bf16[48,2048]{1,0:T(8,128)(2,1)S(1)}, bf16[48,2048]{1,0:T(8,128)(2,1)}, u32[]{:S(2)}) copy-start(bf16[48,2048]{1,0:T(8,128)(2,1)} %param.23) | copy-start | bytes 589828
  0.7 65.0 %copy-start.23 = (f32[2048]{0:T(1024)S(1)}, f32[2048]{0:T(1024)}, u32[]{:S(2)}) copy-start(f32[2048]{0:T(1024)} %param.25) | copy-start | bytes 24580
  63.7 4.2 %copy-start.25 = (f32[128]{0:T(128)S(1)}, f32[128]{0:T(128)}, u32[]{:S(2)}) copy-start(f32[128]{0:T(128)} %param.30) | copy-start | bytes 1540
  67.8 4.2 %copy-start.5 = (bf16[128,2048]{1,0:T(8,128)(2,1)S(1)}, bf16[128,2048]{1,0:T(8,128)(2,1)}, u32[]{:S(2)}) copy-start(bf16[128,2048]{1,0:T(8,128)(2,1)} %param.32) | copy-start | bytes 1572868
  67.8 4.2 %copy-start.26 = (f32[128]{0:T(128)S(1)}, f32[128]{0:T(128)}, u32[]{:S(2)}) copy-start(f32[128]{0:T(128)} %param.31) | copy-start | bytes 1540
  67.9 0.6 copy-start.11
  67.9 4.0 %copy-start.13 = (f32[48,128]{1,0:T(8,128)}, f32[48,128]{1,0:T(8,128)S(1)}, u32[]{:S(2)}) copy-start(f32[48,128]{1,0:T(8,128)S(1)} %get-tuple-element.26) | copy-start | bytes 73732
  67.9 4.0 %copy-start.15 = (f32[48,128]{1,0:T(8,128)}, f32[48,128]{1,0:T(8,128)S(1)}, u32[]{:S(2)}) copy-start(f32[48,128]{1,0:T(8,128)S(1)} %get-tuple-element.27) | copy-start | bytes 73732
  82.0 48.1 %copy-start.9 = (f32[48,256]{1,0:T(8,128)}, f32[48,256]{1,0:T(8,128)S(1)}, u32[]{:S(2)}) copy-start(f32[48,256]{1,0:T(8,128)S(1)} %convert_reduce_fusion.2) | copy-start | bytes 147460
  99.8 30.4 %copy-start.20 = (s32[2,1536]{1,0:T(2,128)}, s32[2,1536]{1,0:T(2,128)S(1)}, u32[]{:S(2)}) copy-start(s32[2,1536]{1,0:T(2,128)S(1)} %eq.41) | copy-start | bytes 36868
  99.8 30.4 %copy-start.19 = (f32[2048]{0:T(1024)S(1)}, f32[2048]{0:T(1024)}, u32[]{:S(2)}) copy-start(f32[2048]{0:T(1024)} %param.33) | copy-start | bytes 24580
  99.8 30.4 %copy-start.27 = (bf16[8,256,512]{2,1,0:T(8,128)(2,1)S(1)}, bf16[8,256,512]{2,1,0:T(8,128)(2,1)}, u32[]{:S(2)}) copy-start(bf16[8,256,512]{2,1,0:T(8,128)(2,1)} %get-tuple-element.17) | copy-start | bytes 6291460
  130.2 2.6 %copy-start.1 = (bf16[384,2048]{1,0:T(8,128)(2,1)S(1)}, bf16[384,2048]{1,0:T(8,128)(2,1)}, u32[]{:S(2)}) copy-start(bf16[384,2048]{1,0:T(8,128)(2,1)} %get-tuple-element.18) | copy-start | bytes 4718596
  133.6 1.2 copy-start.28
  134.8 1.2 copy-start.2
  134.8 1.4 copy-start.6
  134.8 2.3 %copy-start.7 = (bf16[128,2048]{1,0:T(8,128)(2,1)S(1)}, bf16[128,2048]{1,0:T(8,128)(2,1)}, u32[]{:S(2)}) copy-start(bf16[128,2048]{1,0:T(8,128)(2,1)} %param.41) | copy-start | bytes 1572868
  134.8 2.3 %copy-start.8 = (bf16[2048,128]{1,0:T(8,128)(2,1)S(1)}, bf16[2048,128]{1,0:T(8,128)(2,1)}, u32[]{:S(2)}) copy-start(bf16[2048,128]{1,0:T(8,128)(2,1)} %param.40) | copy-start | bytes 1572868
  136.1 21.6 %copy-start.3 = (bf16[8,256,256]{2,1,0:T(8,128)(2,1)S(1)}, bf16[8,256,256]{2,1,0:T(8,128)(2,1)}, u32[]{:S(2)}) copy-start(bf16[8,256,256]{2,1,0:T(8,128)(2,1)} %get-tuple-element.23) | copy-start | bytes 3145732
  139.0 19.7 %copy-start.21 = (s32[2,1536]{1,0:T(2,128)S(1)}, s32[2,1536]{1,0:T(2,128)}, u32[]{:S(2)}) copy-start(s32[2,1536]{1,0:T(2,128)} %copy-done.20) | copy-start | bytes 36868
  139.0 19.7 %copy-start.22 = (f32[2,1536]{1,0:T(2,128)S(1)}, f32[2,1536]{1,0:T(2,128)}, u32[]{:S(2)}) copy-start(f32[2,1536]{1,0:T(2,128)} %mul.257) | copy-start | bytes 36868
  158.7 2.9 %copy-start.24 = (f32[256]{0:T(256)S(1)}, f32[256]{0:T(256)}, u32[]{:S(2)}) copy-start(f32[256]{0:T(256)} %param.45) | copy-start | bytes 3076
  158.7 3.0 %copy-start.18 = (bf16[256,256]{1,0:T(8,128)(2,1)S(1)}, bf16[256,256]{1,0:T(8,128)(2,1)}, u32[]{:S(2)}) copy-start(bf16[256,256]{1,0:T(8,128)(2,1)} %param.44) | copy-start | bytes 393220
  161.7 31.2 %copy-start.17 = (bf16[8,48,256]{2,1,0:T(8,128)(2,1)S(1)}, bf16[8,48,256]{2,1,0:T(8,128)(2,1)}, u32[]{:S(2)}) copy-start(bf16[8,48,256]{2,1,0:T(8,128)(2,1)} %get-tuple-element.20) | copy-start | bytes 589828
  164.1 28.9 %copy-start.10 = (f32[48,256]{1,0:T(8,128)S(1)}, f32[48,256]{1,0:T(8,128)}, u32[]{:S(2)}) copy-start(f32[48,256]{1,0:T(8,128)} %copy-done.9) | copy-start | bytes 147460
  164.1 29.5 %copy-start.12 = (f32[48,128]{1,0:T(8,128)S(1)}, f32[48,128]{1,0:T(8,128)}, u32[]{:S(2)}) copy-start(f32[48,128]{1,0:T(8,128)} %copy-done.11) | copy-start | bytes 73732
  164.1 29.5 %copy-start.14 = (f32[48,128]{1,0:T(8,128)S(1)}, f32[48,128]{1,0:T(8,128)}, u32[]{:S(2)}) copy-start(f32[48,128]{1,0:T(8,128)} %copy-done.13) | copy-start | bytes 73732
  164.1 29.5 %copy-start.16 = (f32[48,128]{1,0:T(8,128)S(1)}, f32[48,128]{1,0:T(8,128)}, u32[]{:S(2)}) copy-start(f32[48,128]{1,0:T(8,128)} %copy-done.15) | copy-start | bytes 73732

commit v2 on v0

v2 whole, which is shorter than its diff:
```python
import jax
import jax.numpy as jnp
from jax import lax
from jax.experimental import pallas as pl
from jax.experimental.pallas import tpu as pltpu
from jax.sharding import Mesh
from jax.sharding import PartitionSpec as P

EP = ("z", "x")
TP = ("y", "c")
NZ, NX, NY, NC = 8, 4, 4, 2
NE, NT = NZ * NX, NY * NC
MESH = pl.DeviceIdType.MESH
EPS = 1e-06
SEQ, WIDTH, HEAD, WIDE, TOPK = 48, 2048, 128, 256, 4
PAIR, CAP, PAD = 2, 6, 16
SLOTS, PADDED = NE * CAP, NE * PAD
ROWS = SEQ * NE // NT
FF = 128

BF, F32 = jnp.bfloat16, jnp.float32
Z_ORDER = (1, 7, 2, 6, 3, 5, 4)
Y_ORDER = (1, 3, 2)
X_ORDER = (1, 3, 2)
SENDS, ARRIVALS, LOCALS = 119, 134, 20


def cols_at(ref, index, width):
    start = pl.multiple_of(index * width, width)
    return ref.at[(slice(None),) * (len(ref.shape) - 1) + (pl.ds(start, width),)]


def dot(left, right):
    return jnp.dot(left, right, preferred_element_type=F32)


def iota(shape, dim):
    return lax.broadcasted_iota(jnp.int32, shape, dim)


def scaled(values, gain):
    values = values.astype(F32)
    return values * lax.rsqrt(jnp.mean(values * values, axis=-1, keepdims=True) + EPS) * gain


class Links:
    def __init__(self, send_sem, recv_sem, local_sem):
        self.send_sem, self.recv_sem, self.local_sem = send_sem, recv_sem, local_sem
        self.sent = self.received = self.locals = 0
        self.z, self.x = lax.axis_index("z"), lax.axis_index("x")
        self.y, self.c = lax.axis_index("y"), lax.axis_index("c")
        self.e = self.z * NX + self.x
        self.t = self.y * NC + self.c
        self.pending = []

    def load(self, src, dst):
        copy = pltpu.make_async_copy(src, dst, self.local_sem.at[self.locals])
        self.locals += 1
        copy.start()
        return copy

    def reserve(self, number):
        first = self.received
        self.received += number
        return first

    def new_send(self):
        self.sent += 1
        return self.sent - 1

    def copy(self, src, dst, sent, slot, **device):
        return pltpu.make_async_remote_copy(
            src_ref=src,
            dst_ref=dst,
            send_sem=self.send_sem.at[sent],
            recv_sem=self.recv_sem.at[slot],
            device_id=device,
            device_id_type=MESH,
        )

    def send(self, src, dst, slot, **device):
        copy = self.copy(src, dst, self.new_send(), slot, **device)
        copy.start()
        self.pending.append(copy)

    def wait(self, dst, slot):
        self.copy(dst, dst, 0, slot, c=1 - self.c).wait_recv()

    def finish(self):
        for copy in self.pending:
            copy.wait_send()
        assert (self.sent, self.received, self.locals) == (SENDS, ARRIVALS, LOCALS)

    def greet(self):
        barrier = pltpu.get_barrier_semaphore()
        peers = []
        for dz in range(NZ):
            for dx in range(NX):
                if dz or dx:
                    peers.append(dict(z=(self.z + dz) % NZ, x=(self.x + dx) % NX))
        for dy in range(NY):
            for dc in range(NC):
                if dy or dc:
                    peers.append(dict(y=(self.y + dy) % NY, c=(self.c + dc) % NC))
        for peer in peers:
            pl.semaphore_signal(barrier, inc=1, device_id=peer, device_id_type=MESH)
        return lambda: pl.semaphore_wait(barrier, len(peers))

    def gather_tp(self, view):
        base = self.reserve(NT)
        mine = view(self.t)
        for dy in Y_ORDER:
            self.send(mine, mine, base + self.t, y=(self.y + dy) % NY)
        self.send(mine, mine, base + self.t, c=1 - self.c)

        def relay():
            for dy in Y_ORDER:
                t = ((self.y + dy) % NY) * NC + self.c
                block = view(t)
                self.wait(block, base + t)
                self.send(block, block, base + t, c=1 - self.c)

        def rest():
            for dy in (0,) + Y_ORDER:
                t = ((self.y + dy) % NY) * NC + 1 - self.c
                self.wait(view(t), base + t)

        return relay, rest

    def swap_tp(self, src_view, dst_view):
        base = self.reserve(NT)
        mine = dst_view(self.t)
        others = []
        for dy in Y_ORDER + (0,):
            for dc in range(NC):
                if dy or dc:
                    others.append(((self.y + dy) % NY, (self.c + dc) % NC))
        for y, c in others:
            self.send(src_view(y * NC + c), mine, base + self.t, y=y, c=c)

        def rest():
            for y, c in others:
                t = y * NC + c
                self.wait(dst_view(t), base + t)

        return rest

    def swap_ep(self, src, dst):
        slot, sent = self.reserve(1), self.new_send()
        for dz in (4, 3, 5, 2, 6, 1, 7, 0):
            for dx in (2, 1, 3, 0):
                if dz or dx:
                    z, x = (self.z + dz) % NZ, (self.x + dx) % NX
                    self.copy(src.at[z * NX + x], dst.at[self.e], sent, slot, z=z, x=x).start()
        self.pending.append(self.copy(src.at[pl.ds(0, NE - 1)], dst.at[pl.ds(0, NE - 1)], sent, slot, c=1 - self.c))
        return lambda: self.wait(dst.at[pl.ds(0, NE - 1)], slot)


def layer(
    tokens,
    state,
    norm_gain,
    w_query,
    w_forget,
    w_input,
    w_outgate,
    lower_bound,
    head_gain,
    w_output,
    ffn_gain,
    route_ids,
    route_weight,
    expert_gate,
    expert_up,
    expert_down,
    shared_gate,
    shared_up,
    shared_down,
    dense_gate,
    dense_up,
    dense_down,
    dense_mix,
    mixed,
    new_state,
    tok,
    wz,
    dense_w,
    down_own,
    down_all,
    held,
    expert_w,
    shared_w,
    shared_d,
    out_w,
    dense_d,
    tok_out,
    tok_in,
    part_out,
    part_in,
    head_part,
    head_in,
    cols,
    resid_rows,
    slot_out,
    slot_in,
    chosen,
    chosen_in,
    dense_rows,
    dense_in,
    dense_hidden,
    hidden,
    shared_part,
    shared_in,
    sum_out,
    sum_in,
    sum2_out,
    sum2_in,
    back_out,
    back_in,
    readout,
    combine,
    dispatch,
    squeeze,
    expand,
    decay_t,
    keygate_t,
    value_f,
    resid,
    send_sem,
    recv_sem,
    local_sem,
):
    n = Links(send_sem, recv_sem, local_sem)
    met = n.greet()
    own_down = cols_at(expert_down, n.t, WIDE)
    load_tok = n.load(tokens, tok)
    load_w = [
        n.load(w, wz.at[n.z, :, pl.ds(i * HEAD, HEAD)])
        for i, w in enumerate((w_query, w_forget, w_input, w_outgate))
    ]
    load_dense = [
        n.load(w, dense_w.at[n.t, :, pl.ds(i * WIDE, WIDE)]) for i, w in enumerate((dense_gate, dense_up))
    ]
    load_down = n.load(expert_down, down_own)
    load_mine = n.load(own_down, down_all.at[:, n.t])
    load_state = n.load(state, held)
    load_out = n.load(w_output, out_w)
    load_shared = [
        n.load(shared_gate, shared_w.at[:, pl.ds(0, FF)]),
        n.load(shared_up, shared_w.at[:, pl.ds(FF, FF)]),
        n.load(shared_down, shared_d),
    ]
    load_expert = [
        n.load(w.at[j], expert_w.at[:, pl.ds((2 * j + i) * FF, FF)])
        for j in range(PAIR)
        for i, w in enumerate((expert_gate, expert_up))
    ]
    load_dense_d = n.load(dense_down, dense_d)

    load_tok.wait()
    normed = scaled(tok[...], norm_gain[...]).astype(BF)
    for x in range(NX):
        for z in range(NZ):
            start = (z * NX + x) * 64
            tok_out[x, :, z * 64 : (z + 1) * 64] = normed[:, start : start + 64]
    tok_in[pl.ds(n.x, 1)] = tok_out[pl.ds(n.x, 1)]

    met()
    for copy in load_w:
        copy.wait()
    base_w = n.reserve(NZ)
    for dz in Z_ORDER:
        n.send(wz.at[n.z], wz.at[n.z], base_w + n.z, z=(n.z + dz) % NZ)
    base_t = n.reserve(NX)
    for dx in X_ORDER:
        x = (n.x + dx) % NX
        n.send(tok_out.at[x], tok_in.at[n.x], base_t + n.x, x=x)
    for copy in load_dense:
        copy.wait()
    dense_relay, dense_rest = n.gather_tp(lambda t: dense_w.at[t])
    load_down.wait()
    down_rest = n.swap_tp(lambda t: cols_at(down_own, t, WIDE), lambda t: down_all.at[:, t])

    lane = iota((SEQ, 128), 1)
    named = [route_ids[:, k : k + 1] for k in range(TOPK)]
    equal = [(lane == ids).astype(F32) for ids in named]
    earlier = (iota((SEQ, SEQ), 1) < iota((SEQ, SEQ), 0)).astype(BF)
    rank = dot(earlier, sum(equal).astype(BF))
    places = []
    for ids, same in zip(named, equal):
        first = (ids // 2) * PAD + (ids % 2) * CAP
        places.append(first.astype(F32) + jnp.sum(same * rank, axis=1, keepdims=True))
    slot_lane = iota((SEQ, PADDED), 1).astype(F32)
    total = jnp.zeros((SEQ, PADDED), F32)
    table = jnp.full((SEQ, 128), -1.0, F32)
    for k, place in enumerate(places):
        total = total + jnp.where(slot_lane == place, route_weight[:, k : k + 1], 0.0)
        table = jnp.where(lane == k, place, table)
    combine[...] = total
    table = table.T
    slot_row = iota((PADDED, SEQ), 0).astype(F32)
    picked = jnp.zeros((PADDED, SEQ), F32)
    for k in range(TOPK):
        picked = picked + (slot_row == table[k : k + 1, :]).astype(F32)
    dispatch[...] = picked.astype(BF)

    def row_of(slot):
        inside = slot % PAD
        second = (inside >= CAP).astype(jnp.int32)
        row = second * SLOTS + (slot // PAD) * CAP + inside - second * CAP
        return jnp.where(inside < PAIR * CAP, row, -1)

    squeeze[...] = (iota((PAIR * SLOTS, PADDED), 0) == row_of(iota((1, PADDED), 1))).astype(F32).astype(BF)
    expand[...] = (iota((PADDED, PAIR * SLOTS), 1) == row_of(iota((PADDED, 1), 0))).astype(F32).astype(BF)

    for dx in X_ORDER:
        x = (n.x + dx) % NX
        n.wait(tok_in.at[x], base_t + x)
    for dz in Z_ORDER:
        z = (n.z + dz) % NZ
        n.wait(wz.at[z], base_w + z)
    part = dot(tok_in[...].reshape(NX * SEQ, 512), wz[...].reshape(512, 512))
    part_out[...] = part.astype(BF).reshape(NX, SEQ, 512)
    base_p = n.reserve(NX)
    for dx in X_ORDER:
        x = (n.x + dx) % NX
        n.send(part_out.at[x], part_in.at[n.x], base_p + n.x, x=x)
    part_in[pl.ds(n.x, 1)] = part_out[pl.ds(n.x, 1)]
    dense_relay()
    for dx in X_ORDER:
        x = (n.x + dx) % NX
        n.wait(part_in.at[x], base_p + x)
    projected = part_in[0].astype(F32)
    for x in range(1, NX):
        projected = projected + part_in[x].astype(F32)
    projected = projected.astype(BF).astype(F32)
    query, forget_pre = projected[:, :HEAD], projected[:, HEAD : 2 * HEAD]
    values, out_gate = projected[:, 2 * HEAD : 3 * HEAD], projected[:, 3 * HEAD :]
    low = lower_bound[...]
    forget_sig = jax.nn.sigmoid(forget_pre)
    decay = low + (1.0 - low) * forget_sig
    keygate = (1.0 - low) * (1.0 - forget_sig)
    mixed_q = (query * decay).T
    decay_t[...] = decay.T
    keygate_t[...] = keygate.T
    value_f[...] = values
    load_state.wait()
    for b in range(SEQ):
        readout[b : b + 1, :] = jnp.sum(mixed_q[:, b : b + 1] * held[b, 0], axis=0, keepdims=True)
    read = readout[...] + jnp.sum(query * keygate, axis=1, keepdims=True) * values
    read = read * lax.rsqrt(jnp.mean(read * read, axis=-1, keepdims=True) + EPS)
    head_out = (read * head_gain[...] * jax.nn.silu(out_gate)).astype(BF)
    load_out.wait()
    head_part[...] = dot(head_out, out_w[...]).astype(BF)
    head_rest = n.swap_tp(lambda t: cols_at(head_part, t, WIDE), lambda t: head_in.at[t])
    head_in[pl.ds(n.t, 1)] = cols_at(head_part, n.t, WIDE)[...][None]
    head_rest()
    own = cols_at(tok, n.t, WIDE)[...].astype(F32)
    for t in range(NT):
        own = own + head_in[t].astype(F32)
    resid[...] = own
    own_cols = own.astype(BF)
    cols[pl.ds(n.e, 1)] = own_cols[None]

    base_c = n.reserve(NE)
    mine = cols.at[n.e]
    for dz in Z_ORDER:
        n.send(mine, mine, base_c + n.e, z=(n.z + dz) % NZ)
    for dx in X_ORDER:
        n.send(mine, mine, base_c + n.e, x=(n.x + dx) % NX)
    cols_at(resid_rows, n.t, WIDE)[...] = own_cols
    rows_relay, rows_rest = n.gather_tp(lambda t: cols_at(resid_rows, t, WIDE))
    slot_out[...] = dot(dispatch[...], own_cols).astype(BF).reshape(NE, PAD, WIDE)
    slots_rest = n.swap_ep(slot_out, slot_in)
    slot_in[pl.ds(n.e, 1)] = slot_out[pl.ds(n.e, 1)]
    for dz in Z_ORDER:
        e = ((n.z + dz) % NZ) * NX + n.x
        n.wait(cols.at[e], base_c + e)
        for dx in X_ORDER:
            n.send(cols.at[e], cols.at[e], base_c + e, x=(n.x + dx) % NX)
    rows_relay()

    slots_rest()
    picked_rows = dot(squeeze[...], slot_in[...].reshape(PADDED, WIDE)).astype(BF)
    cols_at(chosen, n.t, WIDE)[...] = picked_rows
    chosen_relay, chosen_rest = n.gather_tp(lambda t: cols_at(chosen, t, WIDE))

    for b in range(SEQ):
        held[b, 0] = decay_t[:, b : b + 1] * held[b, 0] + keygate_t[:, b : b + 1] * value_f[b : b + 1, :]
    store_state = n.load(held, new_state)

    for dz in (0,) + Z_ORDER:
        for dx in X_ORDER:
            e = ((n.z + dz) % NZ) * NX + (n.x + dx) % NX
            n.wait(cols.at[e], base_c + e)
    per = NE // NT
    dense_swap = n.swap_tp(
        lambda t: cols.at[pl.ds(t * per, per)],
        lambda t: dense_rows.at[:, :, pl.ds(pl.multiple_of(t * WIDE, WIDE), WIDE)],
    )
    dense_rows[:, :, pl.ds(pl.multiple_of(n.t * WIDE, WIDE), WIDE)] = cols[pl.ds(n.t * per, per)]

    rows_rest()
    for copy in load_shared:
        copy.wait()
    shared_x = scaled(resid_rows[...], ffn_gain[...]).astype(BF)
    shared_pre = dot(shared_x, shared_w[...])
    shared_hidden = (jax.nn.silu(shared_pre[:, :FF]) * shared_pre[:, FF:]).astype(BF)
    shared_part[...] = dot(shared_hidden, shared_d[...]).astype(BF)
    shared_rest = n.swap_tp(lambda t: cols_at(shared_part, t, WIDE), lambda t: shared_in.at[t])
    shared_in[pl.ds(n.t, 1)] = cols_at(shared_part, n.t, WIDE)[...][None]

    chosen_relay()
    chosen_rest()
    for copy in load_expert:
        copy.wait()
    gain = ffn_gain[...]
    for j in range(PAIR):
        for i in range(4):
            rows = pl.ds(j * SLOTS + i * SEQ, SEQ)
            chosen_in[rows] = scaled(chosen[rows], gain).astype(BF)
        pre = dot(chosen_in[pl.ds(j * SLOTS, SLOTS)], expert_w[:, 2 * j * FF : 2 * (j + 1) * FF])
        unit = (jax.nn.silu(pre[:, :FF]) * pre[:, FF:]).astype(BF)
        cols_at(hidden, n.t, FF).at[pl.ds(j * SLOTS, SLOTS)][...] = unit
    hidden_relay, hidden_rest = n.gather_tp(lambda t: cols_at(hidden, t, FF))

    dense_rest()
    dense_swap()
    for i in range(per):
        dense_in[pl.ds(i * SEQ, SEQ)] = scaled(dense_rows[i], gain).astype(BF)
    pre = dot(dense_in[...], dense_w[...].reshape(WIDTH, 2 * WIDE))
    dense_hidden[pl.ds(n.t, 1)] = (jax.nn.silu(pre[:, :WIDE]) * pre[:, WIDE:]).astype(BF)[None]
    units_relay, units_rest = n.gather_tp(lambda t: dense_hidden.at[t])

    hidden_relay()
    units_relay()
    down_rest()
    load_mine.wait()
    hidden_rest()
    outs = [
        dot(hidden[pl.ds(j * SLOTS, SLOTS)], down_all[j].reshape(NT * FF, WIDE)).astype(BF) for j in range(PAIR)
    ]
    spread = dot(expand[:, :SLOTS], outs[0]) + dot(expand[:, SLOTS:], outs[1])
    back_out[...] = spread.astype(BF).reshape(NE, PAD, WIDE)
    back_rest = n.swap_ep(back_out, back_in)
    back_in[pl.ds(n.e, 1)] = back_out[pl.ds(n.e, 1)]

    units_rest()
    load_dense_d.wait()
    scale = jax.nn.sigmoid(dense_mix[...])
    for t in range(NT):
        block = dot(dense_hidden[t], dense_d[...]) * scale
        sum_out[t] = block.astype(BF).reshape(NX, SEQ, WIDE)
    base_x = n.reserve(NX)
    for dx in X_ORDER:
        x = (n.x + dx) % NX
        n.send(sum_out.at[:, x], sum_in.at[n.x], base_x + n.x, x=x)
    back_rest()
    shared_rest()
    result = resid[...] + jnp.dot(
        combine[...],
        back_in[...].reshape(PADDED, WIDE).astype(F32),
        preferred_element_type=F32,
        precision=lax.Precision.HIGHEST,
    )
    for t in range(NT):
        result = result + shared_in[t].astype(F32)
    resid[...] = result
    for dx in X_ORDER:
        x = (n.x + dx) % NX
        n.wait(sum_in.at[x], base_x + x)
    for z in range(NZ):
        block = sum_out[z, pl.ds(n.x, 1)][0].astype(F32)
        for dx in X_ORDER:
            block = block + sum_in[pl.ds((n.x + dx) % NX, 1), z][0].astype(F32)
        sum2_out[z] = block.astype(BF)
    base_z = n.reserve(NZ)
    for dz in (4, 3, 5, 2, 6, 1, 7):
        z = (n.z + dz) % NZ
        n.send(sum2_out.at[z], sum2_in.at[n.z], base_z + n.z, z=z)
    sum2_in[pl.ds(n.z, 1)] = sum2_out[pl.ds(n.z, 1)]
    for dz in Z_ORDER:
        z = (n.z + dz) % NZ
        n.wait(sum2_in.at[z], base_z + z)
    result = resid[...]
    for z in range(NZ):
        result = result + sum2_in[z].astype(F32)
    mixed[...] = result.astype(BF)
    store_state.wait()
    n.finish()


def local(*args):
    args = list(args)
    for i in (2, 7, 8, 10, 22):
        args[i] = args[i].reshape(1, -1)
    vmem = pl.BlockSpec(memory_space=pltpu.VMEM)
    hbm = pl.BlockSpec(memory_space=pl.ANY)
    small = (2, 7, 8, 10, 11, 12, 22)
    scratch = [
        ((SEQ, WIDTH), BF),
        ((NZ, 64, 512), BF),
        ((NT, WIDE, 2 * WIDE), BF),
        ((PAIR, FF, WIDTH), BF),
        ((PAIR, NT, FF, WIDE), BF),
        ((SEQ, 1, HEAD, HEAD), F32),
        ((WIDTH, 2 * PAIR * FF), BF),
        ((WIDTH, 2 * FF), BF),
        ((FF, WIDTH), BF),
        ((HEAD, WIDTH), BF),
        ((WIDE, WIDE), BF),
        ((NX, SEQ, 512), BF),
        ((NX, SEQ, 512), BF),
        ((NX, SEQ, 512), BF),
        ((NX, SEQ, 512), BF),
        ((SEQ, WIDTH), BF),
        ((NT, SEQ, WIDE), BF),
        ((NE, SEQ, WIDE), BF),
        ((SEQ, WIDTH), BF),
        ((NE, PAD, WIDE), BF),
        ((NE, PAD, WIDE), BF),
        ((PAIR * SLOTS, WIDTH), BF),
        ((PAIR * SLOTS, WIDTH), BF),
        ((NE // NT, SEQ, WIDTH), BF),
        ((ROWS, WIDTH), BF),
        ((NT, ROWS, WIDE), BF),
        ((PAIR * SLOTS, NT * FF), BF),
        ((SEQ, WIDTH), BF),
        ((NT, SEQ, WIDE), BF),
        ((NZ, NX, SEQ, WIDE), BF),
        ((NX, NZ, SEQ, WIDE), BF),
        ((NZ, SEQ, WIDE), BF),
        ((NZ, SEQ, WIDE), BF),
        ((NE, PAD, WIDE), BF),
        ((NE, PAD, WIDE), BF),
        ((SEQ, HEAD), F32),
        ((SEQ, PADDED), F32),
        ((PADDED, SEQ), BF),
        ((PAIR * SLOTS, PADDED), BF),
        ((PADDED, PAIR * SLOTS), BF),
        ((HEAD, SEQ), F32),
        ((HEAD, SEQ), F32),
        ((SEQ, HEAD), F32),
        ((SEQ, WIDE), F32),
    ]
    return pl.pallas_call(
        layer,
        out_shape=[
            jax.ShapeDtypeStruct((SEQ, WIDE), BF),
            jax.ShapeDtypeStruct((SEQ, 1, HEAD, HEAD), F32),
        ],
        in_specs=[vmem if i in small else hbm for i in range(len(args))],
        out_specs=[vmem, hbm],
        scratch_shapes=[pltpu.VMEM(shape, kind) for shape, kind in scratch]
        + [
            pltpu.SemaphoreType.DMA((SENDS,)),
            pltpu.SemaphoreType.DMA((ARRIVALS,)),
            pltpu.SemaphoreType.DMA((LOCALS,)),
        ],
        compiler_params=pltpu.CompilerParams(collective_id=0, has_side_effects=True),
        name="layer",
    )(*args)


def solution(mesh):
    torus = Mesh(mesh.devices.reshape(NZ, NX, NY, NC), ("z", "x", "y", "c"))
    return jax.shard_map(
        local,
        mesh=torus,
        in_specs=(
            P(EP, None),
            P(EP, TP, None, None),
            P(),
            P(EP, TP),
            P(EP, TP),
            P(EP, TP),
            P(EP, TP),
            P(TP),
            P(TP),
            P(TP, None),
            P(),
            P(EP, None),
            P(EP, None),
            P(EP, None, TP),
            P(EP, None, TP),
            P(EP, TP, None),
            P(None, TP),
            P(None, TP),
            P(TP, None),
            P(TP, EP),
            P(TP, EP),
            P(EP, TP),
            P(TP),
        ),
        out_specs=(P(EP, TP), P(EP, TP, None, None)),
        check_vma=False,
    )
```

time: 302 us -> 114 us (0.38)
  waiting for transfers between devices: 183 us -> 0 us
  Pallas kernels: 0 us -> 105 us
  starting transfers between devices: 34.6 us -> 0 us
  blocking collectives: 26.4 us -> 0 us
  matrix products: 21.1 us -> 0 us
  between operations: 14.1 us -> 0.64 us
  other arithmetic: 12.1 us -> 0 us
    pallas_call x0 -> x1, Pallas kernels: none -> 105 us  [local(): pl.pallas_call(layer, out_shape=[jax.ShapeDtypeStruct((SEQ, WIDE), BF), j...]
    all_gather x2 -> x0, waiting for transfers between devices: 77.7 us -> none  [the longest x1 77.7 us: side_by_side(): lax.all_gather(both, axis, axis=dim, tiled=True)]
    all_to_all x5 -> x0, waiting for transfers between devices: 65.7 us -> none  [the longest x1 26 us: local(): lax.all_to_all(outgoing, EP, split_axis=0, concat_axis=0, tiled=True)]
    reduce_scatter x3 -> x0, waiting for transfers between devices: 39.4 us -> none  [the longest x1 21 us: total_of(): lax.psum_scatter(padded_to(lines, lax.axis_size(axis)), axis, scatter_dim...]
    all_to_all x5 -> x0, starting transfers between devices: 34.5 us -> none  [the longest x2 11.8 us: sum_at_owner(): lax.all_to_all(parts, axis, split_axis=0, concat_axis=0, tiled=True)]
    all_to_all x1 -> x0, blocking collectives: 26.4 us -> none  [from_everyone(): return lax.all_to_all(copies, axis, split_axis=0, concat_axis=0, tiled=True)]
    dot_general x11 -> x0, matrix products: 21.1 us -> none  [the longest x1 4.01 us: local(): jnp.einsum('sexf,efd->sexd', hidden, expert_down, preferred_element_type=...]
    unnamed x27 -> x4, local copies, waits for them, and re-layouts: 0.77 us -> 8 us
  transfers between devices with their start and end apart: 10 -> 0, of which waited for: 8 -> 0; matrix products, arithmetic and copies ran while one was open for 9% -> 0% of each run, Pallas kernels for 0% -> 0%
where the time goes in v2:
time: 114 us
  Pallas kernels  105 us (92%)
  local copies, waits for them, and re-layouts  8 us (7%)
    pallas_call x1, Pallas kernels, local(): pl.pallas_call(layer, out_shape=[jax.ShapeDtypeStruct((SEQ, WIDE), BF), j...  105 us
    unnamed x4, local copies, waits for them, and re-layouts  8 us

profile of v2, /device:TPU:1, one launch (start us, length us, event | category | flops | bytes accessed | tf_op | source)
XLA Modules:
  0.0 113.9 jit_solution(1558716826692201440)
XLA Ops:
  0.6 1.4 %copy.25.route_ids = s32[48,4]{1,0:T(8,128)} copy(s32[48,4]{0,1:T(4,128)} %param.34) | data formatting | bytes 1536 | tf_op args[11]
  2.0 1.4 %copy.26.route_weight = f32[48,4]{1,0:T(8,128)} copy(f32[48,4]{0,1:T(4,128)} %param.35) | data formatting | bytes 1536 | tf_op args[12]
  3.4 105.2 %layer.1 = (bf16[48,256]{1,0:T(8,128)(2,1)}, f32[48,1,128,128]{3,2,1,0:T(8,128)}) custom-call(bf16[48,2048]{1,0:T(8,128)(2,1)} %tokens.1, f32[48,1,128,128]{3,2,1,0:T(8,128)} %state.1, f32[1,2048]{1,0:T(1,128)} %bitcast.5, bf16[64,128]{1,0:T(8,128)(2,1)} %w_query.1, bf16[64,128]{1,0:T(8,128)(2,1)} %w_forget.1, bf16[64,128]{1,0:T(8,128)(2,1)} %w_input.1, ...), custom_call_target="tpu_custom_call" | custom-call | tf_op jit(solution)/shard_map/layer/pallas_call | solution.py:546
  108.6 1.3 %copy.29 = bf16[48,256]{1,0:T(8,128)(2,1)} copy(bf16[48,256]{1,0:T(8,128)(2,1)} %get-tuple-element.4) | data formatting | bytes 49152
  110.0 3.9 %copy.30 = f32[48,1,128,128]{3,2,1,0:T(8,128)} copy(f32[48,1,128,128]{3,2,1,0:T(8,128)} %get-tuple-element.5) | data formatting | bytes 6291456

commit v3 on v2

--- a/solution.py
+++ b/solution.py
@@ -17,12 +17,17 @@
 SLOTS, PADDED = NE * CAP, NE * PAD
 ROWS = SEQ * NE // NT
 FF = 128
+OWN = SEQ // NT
+TILE = OWN * WIDTH // 128
 
 BF, F32 = jnp.bfloat16, jnp.float32
 Z_ORDER = (1, 7, 2, 6, 3, 5, 4)
 Y_ORDER = (1, 3, 2)
 X_ORDER = (1, 3, 2)
-SENDS, ARRIVALS, LOCALS = 119, 134, 20
+FAR_ORDER = (4, 3, 5, 2, 6, 1, 7, 0)
+SENDS, ARRIVALS, LOCALS = 140, 162, 19
+STRIPS = 6
+scope = jax.named_scope
 
 
 def cols_at(ref, index, width):
@@ -181,7 +186,7 @@
     dense_down,
     dense_mix,
     mixed,
-    new_state,
+    gates,
     tok,
     wz,
     dense_w,
@@ -199,13 +204,21 @@
     part_in,
     head_part,
     head_in,
-    cols,
+    rows,
+    flat,
+    tok_rows,
+    row_out,
+    row_in,
+    pack,
+    unpack,
+    order,
+    unit_rows,
+    dense_raw,
     resid_rows,
     slot_out,
     slot_in,
     chosen,
     chosen_in,
-    dense_rows,
     dense_in,
     dense_hidden,
     hidden,
@@ -222,9 +235,6 @@
     dispatch,
     squeeze,
     expand,
-    decay_t,
-    keygate_t,
-    value_f,
     resid,
     send_sem,
     recv_sem,
@@ -278,31 +288,25 @@
     for copy in load_dense:
         copy.wait()
     dense_relay, dense_rest = n.gather_tp(lambda t: dense_w.at[t])
-    load_down.wait()
-    down_rest = n.swap_tp(lambda t: cols_at(down_own, t, WIDE), lambda t: down_all.at[:, t])
-
-    lane = iota((SEQ, 128), 1)
-    named = [route_ids[:, k : k + 1] for k in range(TOPK)]
-    equal = [(lane == ids).astype(F32) for ids in named]
-    earlier = (iota((SEQ, SEQ), 1) < iota((SEQ, SEQ), 0)).astype(BF)
-    rank = dot(earlier, sum(equal).astype(BF))
-    places = []
-    for ids, same in zip(named, equal):
-        first = (ids // 2) * PAD + (ids % 2) * CAP
-        places.append(first.astype(F32) + jnp.sum(same * rank, axis=1, keepdims=True))
-    slot_lane = iota((SEQ, PADDED), 1).astype(F32)
-    total = jnp.zeros((SEQ, PADDED), F32)
-    table = jnp.full((SEQ, 128), -1.0, F32)
-    for k, place in enumerate(places):
-        total = total + jnp.where(slot_lane == place, route_weight[:, k : k + 1], 0.0)
-        table = jnp.where(lane == k, place, table)
-    combine[...] = total
-    table = table.T
-    slot_row = iota((PADDED, SEQ), 0).astype(F32)
-    picked = jnp.zeros((PADDED, SEQ), F32)
-    for k in range(TOPK):
-        picked = picked + (slot_row == table[k : k + 1, :]).astype(F32)
-    dispatch[...] = picked.astype(BF)
+
+    with scope("routes"):
+        expert_row = iota((128, SEQ), 0)
+        named = [route_ids[k : k + 1, :] for k in range(TOPK)]
+        equal = [(expert_row == ids).astype(F32) for ids in named]
+        earlier = (iota((SEQ, SEQ), 0) < iota((SEQ, SEQ), 1)).astype(BF)
+        rank = dot(sum(equal).astype(BF), earlier)
+        slot_row = iota((PADDED, SEQ), 0).astype(F32)
+        total = jnp.zeros((PADDED, SEQ), F32)
+        picked = jnp.zeros((PADDED, SEQ), F32)
+        for k in range(TOPK):
+            ids = named[k]
+            first = (ids // 2) * PAD + (ids % 2) * CAP
+            place = first.astype(F32) + jnp.sum(equal[k] * rank, axis=0, keepdims=True)
+            here = slot_row == place
+            total = total + jnp.where(here, route_weight[k : k + 1, :], 0.0)
+            picked = picked + here.astype(F32)
+        dispatch[...] = picked.astype(BF)
+        combine[...] = total.T
 
     def row_of(slot):
         inside = slot % PAD
@@ -312,6 +316,22 @@
 
     squeeze[...] = (iota((PAIR * SLOTS, PADDED), 0) == row_of(iota((1, PADDED), 1))).astype(F32).astype(BF)
     expand[...] = (iota((PADDED, PAIR * SLOTS), 1) == row_of(iota((PADDED, 1), 0))).astype(F32).astype(BF)
+
+    def packed_row(row):
+        inside = row % SEQ
+        return (inside // OWN) * TILE + (row // SEQ) * OWN + inside % OWN
+
+    def ordered_row(row):
+        inside = row % SEQ
+        return (inside // OWN) * SEQ + (row // SEQ) * OWN + inside % OWN
+
+    many, few = NT * TILE, NT * SEQ
+    pack[...] = (iota((many, many), 0) == packed_row(iota((1, many), 1))).astype(F32).astype(BF)
+    unpack[...] = (iota((many, many), 1) == packed_row(iota((many, 1), 0))).astype(F32).astype(BF)
+    order[...] = (iota((few, few), 0) == ordered_row(iota((1, few), 1))).astype(F32).astype(BF)
+    for k in range(WIDTH // 128):
+        flat[k * SEQ : (k + 1) * SEQ, :] = tok[:, k * 128 : (k + 1) * 128]
+    tok_rows[...] = dot(pack[...], flat[...]).astype(BF).reshape(NT, TILE, 128)
 
     for dx in X_ORDER:
         x = (n.x + dx) % NX
@@ -326,7 +346,6 @@
         x = (n.x + dx) % NX
         n.send(part_out.at[x], part_in.at[n.x], base_p + n.x, x=x)
     part_in[pl.ds(n.x, 1)] = part_out[pl.ds(n.x, 1)]
-    dense_relay()
     for dx in X_ORDER:
         x = (n.x + dx) % NX
         n.wait(part_in.at[x], base_p + x)
@@ -341,9 +360,7 @@
     decay = low + (1.0 - low) * forget_sig
     keygate = (1.0 - low) * (1.0 - forget_sig)
     mixed_q = (query * decay).T
-    decay_t[...] = decay.T
-    keygate_t[...] = keygate.T
-    value_f[...] = values
+    gates[0], gates[1], gates[2] = decay, keygate, values
     load_state.wait()
     for b in range(SEQ):
         readout[b : b + 1, :] = jnp.sum(mixed_q[:, b : b + 1] * held[b, 0], axis=0, keepdims=True)
@@ -351,54 +368,80 @@
     read = read * lax.rsqrt(jnp.mean(read * read, axis=-1, keepdims=True) + EPS)
     head_out = (read * head_gain[...] * jax.nn.silu(out_gate)).astype(BF)
     load_out.wait()
-    head_part[...] = dot(head_out, out_w[...]).astype(BF)
+    whole = dot(head_out, out_w[...]).astype(BF)
+    for k in range(WIDTH // 128):
+        flat[k * SEQ : (k + 1) * SEQ, :] = whole[:, k * 128 : (k + 1) * 128]
+    row_out[...] = dot(pack[...], flat[...]).astype(BF).reshape(NT, TILE, 128)
+    row_rest = n.swap_tp(lambda t: row_out.at[t], lambda t: row_in.at[t])
+    head_part[...] = whole
     head_rest = n.swap_tp(lambda t: cols_at(head_part, t, WIDE), lambda t: head_in.at[t])
+    row_in[pl.ds(n.t, 1)] = row_out[pl.ds(n.t, 1)]
     head_in[pl.ds(n.t, 1)] = cols_at(head_part, n.t, WIDE)[...][None]
+    row_rest()
+    own = tok_rows[pl.ds(n.t, 1)][0].astype(F32)
+    for t in range(NT):
+        own = own + row_in[t].astype(F32)
+    rows[pl.ds(n.e, 1)] = own.astype(BF)[None]
+
+    base_c = n.reserve(NE)
+    mine = rows.at[n.e]
+    for dz in Z_ORDER:
+        n.send(mine, mine, base_c + n.e, z=(n.z + dz) % NZ)
+    for dx in X_ORDER:
+        n.send(mine, mine, base_c + n.e, x=(n.x + dx) % NX)
     head_rest()
     own = cols_at(tok, n.t, WIDE)[...].astype(F32)
     for t in range(NT):
         own = own + head_in[t].astype(F32)
     resid[...] = own
     own_cols = own.astype(BF)
-    cols[pl.ds(n.e, 1)] = own_cols[None]
-
-    base_c = n.reserve(NE)
-    mine = cols.at[n.e]
-    for dz in Z_ORDER:
-        n.send(mine, mine, base_c + n.e, z=(n.z + dz) % NZ)
-    for dx in X_ORDER:
-        n.send(mine, mine, base_c + n.e, x=(n.x + dx) % NX)
-    cols_at(resid_rows, n.t, WIDE)[...] = own_cols
-    rows_relay, rows_rest = n.gather_tp(lambda t: cols_at(resid_rows, t, WIDE))
     slot_out[...] = dot(dispatch[...], own_cols).astype(BF).reshape(NE, PAD, WIDE)
     slots_rest = n.swap_ep(slot_out, slot_in)
     slot_in[pl.ds(n.e, 1)] = slot_out[pl.ds(n.e, 1)]
+    cols_at(resid_rows, n.t, WIDE)[...] = own_cols
+    rows_relay, rows_rest = n.gather_tp(lambda t: cols_at(resid_rows, t, WIDE))
+    load_down.wait()
+    down_rest = n.swap_tp(lambda t: cols_at(down_own, t, WIDE), lambda t: down_all.at[:, t])
     for dz in Z_ORDER:
         e = ((n.z + dz) % NZ) * NX + n.x
-        n.wait(cols.at[e], base_c + e)
+        n.wait(rows.at[e], base_c + e)
         for dx in X_ORDER:
-            n.send(cols.at[e], cols.at[e], base_c + e, x=(n.x + dx) % NX)
+            n.send(rows.at[e], rows.at[e], base_c + e, x=(n.x + dx) % NX)
     rows_relay()
+    dense_relay()
 
     slots_rest()
     picked_rows = dot(squeeze[...], slot_in[...].reshape(PADDED, WIDE)).astype(BF)
     cols_at(chosen, n.t, WIDE)[...] = picked_rows
     chosen_relay, chosen_rest = n.gather_tp(lambda t: cols_at(chosen, t, WIDE))
 
-    for b in range(SEQ):
-        held[b, 0] = decay_t[:, b : b + 1] * held[b, 0] + keygate_t[:, b : b + 1] * value_f[b : b + 1, :]
-    store_state = n.load(held, new_state)
-
     for dz in (0,) + Z_ORDER:
         for dx in X_ORDER:
             e = ((n.z + dz) % NZ) * NX + (n.x + dx) % NX
-            n.wait(cols.at[e], base_c + e)
-    per = NE // NT
-    dense_swap = n.swap_tp(
-        lambda t: cols.at[pl.ds(t * per, per)],
-        lambda t: dense_rows.at[:, :, pl.ds(pl.multiple_of(t * WIDE, WIDE), WIDE)],
-    )
-    dense_rows[:, :, pl.ds(pl.multiple_of(n.t * WIDE, WIDE), WIDE)] = cols[pl.ds(n.t * per, per)]
+            n.wait(rows.at[e], base_c + e)
+    gain = ffn_gain[...]
+    for g in range(NE // NT):
+        group = dot(unpack[...], rows[g * NT : (g + 1) * NT].reshape(NT * TILE, 128))
+        for k in range(WIDTH // 128):
+            dense_raw[:, k * 128 : (k + 1) * 128] = group[k * SEQ : (k + 1) * SEQ, :]
+        dense_in[g * SEQ : (g + 1) * SEQ, :] = scaled(dense_raw[...], gain).astype(BF)
+    dense_rest()
+    pre = dot(dense_in[...], dense_w[...].reshape(WIDTH, 2 * WIDE))
+    dense_hidden[pl.ds(n.t, 1)] = (jax.nn.silu(pre[:, :WIDE]) * pre[:, WIDE:]).astype(BF)[None]
+    units_relay, units_rest = n.gather_tp(lambda t: dense_hidden.at[t])
+
+    chosen_relay()
+    chosen_rest()
+    for copy in load_expert:
+        copy.wait()
+    for j in range(PAIR):
+        for i in range(4):
+            part = pl.ds(j * SLOTS + i * SEQ, SEQ)
+            chosen_in[part] = scaled(chosen[part], gain).astype(BF)
+        pre = dot(chosen_in[pl.ds(j * SLOTS, SLOTS)], expert_w[:, 2 * j * FF : 2 * (j + 1) * FF])
+        unit = (jax.nn.silu(pre[:, :FF]) * pre[:, FF:]).astype(BF)
+        cols_at(hidden, n.t, FF).at[pl.ds(j * SLOTS, SLOTS)][...] = unit
+    hidden_relay, hidden_rest = n.gather_tp(lambda t: cols_at(hidden, t, FF))
 
     rows_rest()
     for copy in load_shared:
@@ -410,30 +453,24 @@
     shared_rest = n.swap_tp(lambda t: cols_at(shared_part, t, WIDE), lambda t: shared_in.at[t])
     shared_in[pl.ds(n.t, 1)] = cols_at(shared_part, n.t, WIDE)[...][None]
 
-    chosen_relay()
-    chosen_rest()
-    for copy in load_expert:
-        copy.wait()
-    gain = ffn_gain[...]
-    for j in range(PAIR):
-        for i in range(4):
-            rows = pl.ds(j * SLOTS + i * SEQ, SEQ)
-            chosen_in[rows] = scaled(chosen[rows], gain).astype(BF)
-        pre = dot(chosen_in[pl.ds(j * SLOTS, SLOTS)], expert_w[:, 2 * j * FF : 2 * (j + 1) * FF])
-        unit = (jax.nn.silu(pre[:, :FF]) * pre[:, FF:]).astype(BF)
-        cols_at(hidden, n.t, FF).at[pl.ds(j * SLOTS, SLOTS)][...] = unit
-    hidden_relay, hidden_rest = n.gather_tp(lambda t: cols_at(hidden, t, FF))
-
-    dense_rest()
-    dense_swap()
-    for i in range(per):
-        dense_in[pl.ds(i * SEQ, SEQ)] = scaled(dense_rows[i], gain).astype(BF)
-    pre = dot(dense_in[...], dense_w[...].reshape(WIDTH, 2 * WIDE))
-    dense_hidden[pl.ds(n.t, 1)] = (jax.nn.silu(pre[:, :WIDE]) * pre[:, WIDE:]).astype(BF)[None]
-    units_relay, units_rest = n.gather_tp(lambda t: dense_hidden.at[t])
+    units_relay()
+    units_rest()
+    load_dense_d.wait()
+    scale = jax.nn.sigmoid(dense_mix[...])
+    for g in range(NE // NT):
+        for t in range(NT):
+            unit_rows[t * SEQ : (t + 1) * SEQ, :] = dense_hidden[t, g * SEQ : (g + 1) * SEQ, :]
+        inner = dot(order[...], unit_rows[...]).astype(BF)
+        block = dot(inner, dense_d[...]) * scale
+        sum_out[2 * g : 2 * g + 2] = block.astype(BF).reshape(2, NX, SEQ, WIDE)
+    base_x = n.reserve(NX * NZ)
+    for dz in FAR_ORDER:
+        z = (n.z + dz) % NZ
+        for dx in X_ORDER:
+            x = (n.x + dx) % NX
+            n.send(sum_out.at[z, x], sum_in.at[n.x, z], base_x + n.x * NZ + z, x=x)
 
     hidden_relay()
-    units_relay()
     down_rest()
     load_mine.wait()
     hidden_rest()
@@ -445,16 +482,19 @@
     back_rest = n.swap_ep(back_out, back_in)
     back_in[pl.ds(n.e, 1)] = back_out[pl.ds(n.e, 1)]
 
-    units_rest()
-    load_dense_d.wait()
-    scale = jax.nn.sigmoid(dense_mix[...])
-    for t in range(NT):
-        block = dot(dense_hidden[t], dense_d[...]) * scale
-        sum_out[t] = block.astype(BF).reshape(NX, SEQ, WIDE)
-    base_x = n.reserve(NX)
-    for dx in X_ORDER:
-        x = (n.x + dx) % NX
-        n.send(sum_out.at[:, x], sum_in.at[n.x], base_x + n.x, x=x)
+    base_z = n.reserve(NZ)
+    for dz in FAR_ORDER:
+        z = (n.z + dz) % NZ
+        block = sum_out[pl.ds(z, 1), n.x][0].astype(F32)
+        for dx in X_ORDER:
+            x = (n.x + dx) % NX
+            n.wait(sum_in.at[x, z], base_x + x * NZ + z)
+            block = block + sum_in[x, pl.ds(z, 1)][0].astype(F32)
+        if dz:
+            sum2_out[pl.ds(z, 1)] = block.astype(BF)[None]
+            n.send(sum2_out.at[z], sum2_in.at[n.z], base_z + n.z, z=z)
+        else:
+            sum2_in[pl.ds(n.z, 1)] = block.astype(BF)[None]
     back_rest()
     shared_rest()
     result = resid[...] + jnp.dot(
@@ -465,35 +505,42 @@
     )
     for t in range(NT):
         result = result + shared_in[t].astype(F32)
-    resid[...] = result
-    for dx in X_ORDER:
-        x = (n.x + dx) % NX
-        n.wait(sum_in.at[x], base_x + x)
-    for z in range(NZ):
-        block = sum_out[z, pl.ds(n.x, 1)][0].astype(F32)
-        for dx in X_ORDER:
-            block = block + sum_in[pl.ds((n.x + dx) % NX, 1), z][0].astype(F32)
-        sum2_out[z] = block.astype(BF)
-    base_z = n.reserve(NZ)
-    for dz in (4, 3, 5, 2, 6, 1, 7):
-        z = (n.z + dz) % NZ
-        n.send(sum2_out.at[z], sum2_in.at[n.z], base_z + n.z, z=z)
-    sum2_in[pl.ds(n.z, 1)] = sum2_out[pl.ds(n.z, 1)]
     for dz in Z_ORDER:
         z = (n.z + dz) % NZ
         n.wait(sum2_in.at[z], base_z + z)
-    result = resid[...]
     for z in range(NZ):
         result = result + sum2_in[z].astype(F32)
-    mixed[...] = result.astype(BF)
-    store_state.wait()
+    mixed[...] = result
     n.finish()
+
+
+def closing(result, gates, state, mixed, new_state, held, sem):
+    rows = SEQ // STRIPS
+    strips = [pl.ds(i * rows, rows) for i in range(STRIPS)]
+    loads = [pltpu.make_async_copy(state.at[r], held.at[r], sem.at[i]) for i, r in enumerate(strips)]
+    stores = [
+        pltpu.make_async_copy(held.at[r], new_state.at[r], sem.at[STRIPS + i]) for i, r in enumerate(strips)
+    ]
+    for copy in loads:
+        copy.start()
+    mixed[...] = result[...].astype(BF)
+    decay, keygate = gates[0].T, gates[1].T
+    for i in range(STRIPS):
+        loads[i].wait()
+        for b in range(i * rows, (i + 1) * rows):
+            held[b, 0] = decay[:, b : b + 1] * held[b, 0] + keygate[:, b : b + 1] * gates[2, b : b + 1, :]
+        stores[i].start()
+    for copy in stores:
+        copy.wait()
 
 
 def local(*args):
     args = list(args)
+    state = args[1]
     for i in (2, 7, 8, 10, 22):
         args[i] = args[i].reshape(1, -1)
+    for i in (11, 12):
+        args[i] = args[i].T
     vmem = pl.BlockSpec(memory_space=pltpu.VMEM)
     hbm = pl.BlockSpec(memory_space=pl.ANY)
     small = (2, 7, 8, 10, 11, 12, 22)
@@ -515,13 +562,21 @@
         ((NX, SEQ, 512), BF),
         ((SEQ, WIDTH), BF),
         ((NT, SEQ, WIDE), BF),
-        ((NE, SEQ, WIDE), BF),
+        ((NE, TILE, 128), BF),
+        ((NT * TILE, 128), BF),
+        ((NT, TILE, 128), BF),
+        ((NT, TILE, 128), BF),
+        ((NT, TILE, 128), BF),
+        ((NT * TILE, NT * TILE), BF),
+        ((NT * TILE, NT * TILE), BF),
+        ((NT * SEQ, NT * SEQ), BF),
+        ((NT * SEQ, WIDE), BF),
+        ((SEQ, WIDTH), F32),
         ((SEQ, WIDTH), BF),
         ((NE, PAD, WIDE), BF),
         ((NE, PAD, WIDE), BF),
         ((PAIR * SLOTS, WIDTH), BF),
         ((PAIR * SLOTS, WIDTH), BF),
-        ((NE // NT, SEQ, WIDTH), BF),
         ((ROWS, WIDTH), BF),
         ((NT, ROWS, WIDE), BF),
         ((PAIR * SLOTS, NT * FF), BF),
@@ -538,19 +593,16 @@
         ((PADDED, SEQ), BF),
         ((PAIR * SLOTS, PADDED), BF),
         ((PADDED, PAIR * SLOTS), BF),
-        ((HEAD, SEQ), F32),
-        ((HEAD, SEQ), F32),
-        ((SEQ, HEAD), F32),
         ((SEQ, WIDE), F32),
     ]
-    return pl.pallas_call(
+    result, gates = pl.pallas_call(
         layer,
         out_shape=[
-            jax.ShapeDtypeStruct((SEQ, WIDE), BF),
-            jax.ShapeDtypeStruct((SEQ, 1, HEAD, HEAD), F32),
+            jax.ShapeDtypeStruct((SEQ, WIDE), F32),
+            jax.ShapeDtypeStruct((3, SEQ, HEAD), F32),
         ],
         in_specs=[vmem if i in small else hbm for i in range(len(args))],
-        out_specs=[vmem, hbm],
+        out_specs=[vmem, vmem],
         scratch_shapes=[pltpu.VMEM(shape, kind) for shape, kind in scratch]
         + [
             pltpu.SemaphoreType.DMA((SENDS,)),
@@ -560,6 +612,20 @@
         compiler_params=pltpu.CompilerParams(collective_id=0, has_side_effects=True),
         name="layer",
     )(*args)
+    return pl.pallas_call(
+        closing,
+        out_shape=[
+            jax.ShapeDtypeStruct((SEQ, WIDE), BF),
+            jax.ShapeDtypeStruct((SEQ, 1, HEAD, HEAD), F32),
+        ],
+        in_specs=[vmem, vmem, hbm],
+        out_specs=[vmem, hbm],
+        scratch_shapes=[
+            pltpu.VMEM((SEQ, 1, HEAD, HEAD), F32),
+            pltpu.SemaphoreType.DMA((2 * STRIPS,)),
+        ],
+        name="closing",
+    )(result, gates, state)
 
 
 def solution(mesh):

time: 114 us -> 95.9 us (0.84)
  Pallas kernels: 105 us -> 95.1 us
  local copies, waits for them, and re-layouts: 8 us -> 0 us
    pallas_call x1 -> x2, Pallas kernels: 105 us -> 95.1 us  [the longest x1 89.6 us: local(): pl.pallas_call(layer, out_shape=[jax.ShapeDtypeStruct((SEQ, WIDE), F32),...]
    unnamed x4 -> x0, local copies, waits for them, and re-layouts: 8 us -> none
where the time goes in v3:
time: 95.9 us; the launch traced here: 95.8 us
  Pallas kernels  95.1 us (99%)
    pallas_call x1, Pallas kernels, local(): pl.pallas_call(layer, out_shape=[jax.ShapeDtypeStruct((SEQ, WIDE), F32),...  89.6 us
    pallas_call x1, Pallas kernels, local(): pl.pallas_call(closing, out_shape=[jax.ShapeDtypeStruct((SEQ, WIDE), BF),...  5.56 us

profile of v3, /device:TPU:1, one launch (start us, length us, event | category | flops | bytes accessed | tf_op | source)
XLA Modules:
  0.0 95.8 jit_solution(7043881312095464289)
XLA Ops:
  0.6 89.6 %layer.1 = (f32[48,256]{1,0:T(8,128)}, f32[3,48,128]{2,1,0:T(8,128)}) custom-call(bf16[48,2048]{1,0:T(8,128)(2,1)} %tokens.1, f32[48,1,128,128]{3,2,1,0:T(8,128)} %state.3, f32[1,2048]{1,0:T(1,128)} %bitcast.7, bf16[64,128]{1,0:T(8,128)(2,1)} %w_query.1, bf16[64,128]{1,0:T(8,128)(2,1)} %w_forget.1, bf16[64,128]{1,0:T(8,128)(2,1)} %w_input.1, ...), custom_call_target="tpu_custom_call" | custom-call | tf_op jit(solution)/shard_map/layer/pallas_call | solution.py:598
  90.2 5.6 %closing.1 = (bf16[48,256]{1,0:T(8,128)(2,1)}, f32[48,1,128,128]{3,2,1,0:T(8,128)}) custom-call(f32[48,256]{1,0:T(8,128)} %get-tuple-element.4.result, f32[3,48,128]{2,1,0:T(8,128)} %get-tuple-element.5.gates, f32[48,1,128,128]{3,2,1,0:T(8,128)} %state.3), custom_call_target="tpu_custom_call" | custom-call | tf_op jit(solution)/shard_map/closing/pallas_call | solution.py:615

commit v4 on v3

--- a/solution.py
+++ b/solution.py
@@ -25,8 +25,7 @@
 Y_ORDER = (1, 3, 2)
 X_ORDER = (1, 3, 2)
 FAR_ORDER = (4, 3, 5, 2, 6, 1, 7, 0)
-SENDS, ARRIVALS, LOCALS = 140, 162, 19
-STRIPS = 6
+SENDS, ARRIVALS, LOCALS = 18, 62, 19
 scope = jax.named_scope
 
 
@@ -83,10 +82,14 @@
             device_id_type=MESH,
         )
 
-    def send(self, src, dst, slot, **device):
-        copy = self.copy(src, dst, self.new_send(), slot, **device)
-        copy.start()
-        self.pending.append(copy)
+    def stage(self, total):
+        sent = self.new_send()
+        self.pending.append(self.copy(total, total, sent, 0, c=1 - self.c))
+
+        def send(src, dst, slot, **device):
+            self.copy(src, dst, sent, slot, **device).start()
+
+        return send
 
     def wait(self, dst, slot):
         self.copy(dst, dst, 0, slot, c=1 - self.c).wait_recv()
@@ -111,44 +114,56 @@
             pl.semaphore_signal(barrier, inc=1, device_id=peer, device_id_type=MESH)
         return lambda: pl.semaphore_wait(barrier, len(peers))
 
-    def gather_tp(self, view):
-        base = self.reserve(NT)
+    def gather_tp(self, view, seven, four):
+        base = self.reserve(7)
+        send = self.stage(seven)
+        up, down = (self.y + 1) % NY, (self.y + NY - 1) % NY
+        far = (self.y + 2) % NY
+
+        def half(y, i):
+            block = view(y * NC + self.c)
+            size = block.shape[0] // 2
+            return block.at[(pl.ds(i * size, size),) + (slice(None),) * (len(block.shape) - 1)]
+
+        for i in range(2):
+            send(half(self.y, i), half(self.y, i), base + i, y=up)
+            send(half(self.y, 1 - i), half(self.y, 1 - i), base + 2 + i, y=down)
         mine = view(self.t)
-        for dy in Y_ORDER:
-            self.send(mine, mine, base + self.t, y=(self.y + dy) % NY)
-        self.send(mine, mine, base + self.t, c=1 - self.c)
+        send(mine, mine, base + 6, c=1 - self.c)
+
+        def onward():
+            self.wait(half(down, 0), base)
+            send(half(down, 0), half(down, 0), base + 4, y=up)
+            self.wait(half(up, 1), base + 2)
+            send(half(up, 1), half(up, 1), base + 5, y=down)
 
         def relay():
-            for dy in Y_ORDER:
-                t = ((self.y + dy) % NY) * NC + self.c
-                block = view(t)
-                self.wait(block, base + t)
-                self.send(block, block, base + t, c=1 - self.c)
+            self.wait(half(down, 1), base + 1)
+            block = view(down * NC + self.c)
+            send(block, block, base + 6, c=1 - self.c)
+            self.wait(half(up, 0), base + 3)
+            block = view(up * NC + self.c)
+            send(block, block, base + 6, c=1 - self.c)
+            self.wait(half(far, 0), base + 4)
+            self.wait(half(far, 1), base + 5)
+            block = view(far * NC + self.c)
+            send(block, block, base + 6, c=1 - self.c)
 
         def rest():
-            for dy in (0,) + Y_ORDER:
-                t = ((self.y + dy) % NY) * NC + 1 - self.c
-                self.wait(view(t), base + t)
-
-        return relay, rest
-
-    def swap_tp(self, src_view, dst_view):
-        base = self.reserve(NT)
+            self.wait(four, base + 6)
+
+        return onward, relay, rest
+
+    def swap_tp(self, src_view, dst_view, seven):
+        base = self.reserve(1)
+        send = self.stage(seven)
         mine = dst_view(self.t)
-        others = []
         for dy in Y_ORDER + (0,):
             for dc in range(NC):
                 if dy or dc:
-                    others.append(((self.y + dy) % NY, (self.c + dc) % NC))
-        for y, c in others:
-            self.send(src_view(y * NC + c), mine, base + self.t, y=y, c=c)
-
-        def rest():
-            for y, c in others:
-                t = y * NC + c
-                self.wait(dst_view(t), base + t)
-
-        return rest
+                    y, c = (self.y + dy) % NY, (self.c + dc) % NC
+                    send(src_view(y * NC + c), mine, base, y=y, c=c)
+        return lambda: self.wait(seven, base)
 
     def swap_ep(self, src, dst):
         slot, sent = self.reserve(1), self.new_send()
@@ -186,13 +201,13 @@
     dense_down,
     dense_mix,
     mixed,
-    gates,
+    held,
     tok,
     wz,
     dense_w,
     down_own,
     down_all,
-    held,
+    gates,
     expert_w,
     shared_w,
     shared_d,
@@ -278,16 +293,21 @@
     met()
     for copy in load_w:
         copy.wait()
-    base_w = n.reserve(NZ)
-    for dz in Z_ORDER:
-        n.send(wz.at[n.z], wz.at[n.z], base_w + n.z, z=(n.z + dz) % NZ)
-    base_t = n.reserve(NX)
+    base_w = n.reserve(7)
+    send_w = n.stage(wz.at[pl.ds(0, 7)])
+    z_at = [(n.z + dz) % NZ for dz in range(NZ)]
+    for dz, slot in ((2, 0), (6, 1), (1, 2), (7, 2)):
+        send_w(wz.at[n.z], wz.at[n.z], base_w + slot, z=z_at[dz])
+    base_t = n.reserve(1)
+    send_t = n.stage(tok_in.at[pl.ds(0, 3)])
     for dx in X_ORDER:
         x = (n.x + dx) % NX
-        n.send(tok_out.at[x], tok_in.at[n.x], base_t + n.x, x=x)
+        send_t(tok_out.at[x], tok_in.at[n.x], base_t, x=x)
     for copy in load_dense:
         copy.wait()
-    dense_relay, dense_rest = n.gather_tp(lambda t: dense_w.at[t])
+    dense_onward, dense_relay, dense_rest = n.gather_tp(
+        lambda t: dense_w.at[t], dense_w.at[pl.ds(0, 7)], dense_w.at[pl.ds(0, 4)]
+    )
 
     with scope("routes"):
         expert_row = iota((128, SEQ), 0)
@@ -333,22 +353,31 @@
         flat[k * SEQ : (k + 1) * SEQ, :] = tok[:, k * 128 : (k + 1) * 128]
     tok_rows[...] = dot(pack[...], flat[...]).astype(BF).reshape(NT, TILE, 128)
 
+    for source, near, far, row, slot in ((6, 1, 2, 0, 0), (2, 7, 6, 32, 1)):
+        block = wz.at[z_at[source]]
+        n.wait(block, base_w + slot)
+        send_w(block, block, base_w + 3 + slot, z=z_at[near])
+        block = wz.at[z_at[source], pl.ds(row, 32)]
+        send_w(block, block, base_w + 5 + slot, z=z_at[far])
+    dense_onward()
+    load_down.wait()
+    down_rest = [
+        n.swap_tp(lambda t: cols_at(down_own.at[0], t, WIDE), lambda t: down_all.at[0, t], down_all.at[0, pl.ds(0, 7)])
+    ]
+    n.wait(tok_in.at[pl.ds(0, 3)], base_t)
+    n.wait(wz.at[pl.ds(0, 2)], base_w + 2)
+    for slot in range(2):
+        n.wait(wz.at[0], base_w + 3 + slot)
+        n.wait(wz.at[0, pl.ds(0, 32)], base_w + 5 + slot)
+    part = dot(tok_in[...].reshape(NX * SEQ, 512), wz[...].reshape(512, 512))
+    part_out[...] = part.astype(BF).reshape(NX, SEQ, 512)
+    base_p = n.reserve(1)
+    send_p = n.stage(part_in.at[pl.ds(0, 3)])
     for dx in X_ORDER:
         x = (n.x + dx) % NX
-        n.wait(tok_in.at[x], base_t + x)
-    for dz in Z_ORDER:
-        z = (n.z + dz) % NZ
-        n.wait(wz.at[z], base_w + z)
-    part = dot(tok_in[...].reshape(NX * SEQ, 512), wz[...].reshape(512, 512))
-    part_out[...] = part.astype(BF).reshape(NX, SEQ, 512)
-    base_p = n.reserve(NX)
-    for dx in X_ORDER:
-        x = (n.x + dx) % NX
-        n.send(part_out.at[x], part_in.at[n.x], base_p + n.x, x=x)
+        send_p(part_out.at[x], part_in.at[n.x], base_p, x=x)
     part_in[pl.ds(n.x, 1)] = part_out[pl.ds(n.x, 1)]
-    for dx in X_ORDER:
-        x = (n.x + dx) % NX
-        n.wait(part_in.at[x], base_p + x)
+    n.wait(part_in.at[pl.ds(0, 3)], base_p)
     projected = part_in[0].astype(F32)
     for x in range(1, NX):
         projected = projected + part_in[x].astype(F32)
@@ -360,7 +389,7 @@
     decay = low + (1.0 - low) * forget_sig
     keygate = (1.0 - low) * (1.0 - forget_sig)
     mixed_q = (query * decay).T
-    gates[0], gates[1], gates[2] = decay, keygate, values
+    gates[0, :, :], gates[1, :, :], gates[2, :, :] = decay, keygate, values
     load_state.wait()
     for b in range(SEQ):
         readout[b : b + 1, :] = jnp.sum(mixed_q[:, b : b + 1] * held[b, 0], axis=0, keepdims=True)
@@ -372,9 +401,9 @@
     for k in range(WIDTH // 128):
         flat[k * SEQ : (k + 1) * SEQ, :] = whole[:, k * 128 : (k + 1) * 128]
     row_out[...] = dot(pack[...], flat[...]).astype(BF).reshape(NT, TILE, 128)
-    row_rest = n.swap_tp(lambda t: row_out.at[t], lambda t: row_in.at[t])
+    row_rest = n.swap_tp(lambda t: row_out.at[t], lambda t: row_in.at[t], row_in.at[pl.ds(0, 7)])
     head_part[...] = whole
-    head_rest = n.swap_tp(lambda t: cols_at(head_part, t, WIDE), lambda t: head_in.at[t])
+    head_rest = n.swap_tp(lambda t: cols_at(head_part, t, WIDE), lambda t: head_in.at[t], head_in.at[pl.ds(0, 7)])
     row_in[pl.ds(n.t, 1)] = row_out[pl.ds(n.t, 1)]
     head_in[pl.ds(n.t, 1)] = cols_at(head_part, n.t, WIDE)[...][None]
     row_rest()
@@ -383,12 +412,13 @@
         own = own + row_in[t].astype(F32)
     rows[pl.ds(n.e, 1)] = own.astype(BF)[None]
 
-    base_c = n.reserve(NE)
+    base_c = n.reserve(NZ)
+    send_c = n.stage(rows.at[pl.ds(0, NE - 1)])
     mine = rows.at[n.e]
-    for dz in Z_ORDER:
-        n.send(mine, mine, base_c + n.e, z=(n.z + dz) % NZ)
+    for i, dz in enumerate(Z_ORDER):
+        send_c(mine, mine, base_c + i, z=z_at[dz])
     for dx in X_ORDER:
-        n.send(mine, mine, base_c + n.e, x=(n.x + dx) % NX)
+        send_c(mine, mine, base_c + 7, x=(n.x + dx) % NX)
     head_rest()
     own = cols_at(tok, n.t, WIDE)[...].astype(F32)
     for t in range(NT):
@@ -399,27 +429,38 @@
     slots_rest = n.swap_ep(slot_out, slot_in)
     slot_in[pl.ds(n.e, 1)] = slot_out[pl.ds(n.e, 1)]
     cols_at(resid_rows, n.t, WIDE)[...] = own_cols
-    rows_relay, rows_rest = n.gather_tp(lambda t: cols_at(resid_rows, t, WIDE))
-    load_down.wait()
-    down_rest = n.swap_tp(lambda t: cols_at(down_own, t, WIDE), lambda t: down_all.at[:, t])
-    for dz in Z_ORDER:
-        e = ((n.z + dz) % NZ) * NX + n.x
-        n.wait(rows.at[e], base_c + e)
+    rows_mine = cols_at(resid_rows, n.t, WIDE)
+    rows_seven = resid_rows.at[:, pl.ds(0, 7 * WIDE)]
+    rows_rest = n.swap_tp(lambda t: rows_mine, lambda t: cols_at(resid_rows, t, WIDE), rows_seven)
+    down_rest.append(
+        n.swap_tp(lambda t: cols_at(down_own.at[1], t, WIDE), lambda t: down_all.at[1, t], down_all.at[1, pl.ds(0, 7)])
+    )
+    dense_relay()
+    for i, dz in enumerate(Z_ORDER):
+        e = z_at[(NZ - dz) % NZ] * NX + n.x
+        n.wait(rows.at[e], base_c + i)
         for dx in X_ORDER:
-            n.send(rows.at[e], rows.at[e], base_c + e, x=(n.x + dx) % NX)
-    rows_relay()
-    dense_relay()
+            send_c(rows.at[e], rows.at[e], base_c + 7, x=(n.x + dx) % NX)
+
+    gain = ffn_gain[...]
+    rows_rest()
+    for copy in load_shared:
+        copy.wait()
+    shared_x = scaled(resid_rows[...], gain).astype(BF)
+    shared_pre = dot(shared_x, shared_w[...])
+    shared_hidden = (jax.nn.silu(shared_pre[:, :FF]) * shared_pre[:, FF:]).astype(BF)
+    shared_part[...] = dot(shared_hidden, shared_d[...]).astype(BF)
+    shared_rest = n.swap_tp(lambda t: cols_at(shared_part, t, WIDE), lambda t: shared_in.at[t], shared_in.at[pl.ds(0, 7)])
+    shared_in[pl.ds(n.t, 1)] = cols_at(shared_part, n.t, WIDE)[...][None]
 
     slots_rest()
     picked_rows = dot(squeeze[...], slot_in[...].reshape(PADDED, WIDE)).astype(BF)
     cols_at(chosen, n.t, WIDE)[...] = picked_rows
-    chosen_relay, chosen_rest = n.gather_tp(lambda t: cols_at(chosen, t, WIDE))
-
-    for dz in (0,) + Z_ORDER:
-        for dx in X_ORDER:
-            e = ((n.z + dz) % NZ) * NX + (n.x + dx) % NX
-            n.wait(rows.at[e], base_c + e)
-    gain = ffn_gain[...]
+    chosen_onward, chosen_relay, chosen_rest = n.gather_tp(
+        lambda t: cols_at(chosen, t, WIDE), chosen.at[:, pl.ds(0, 7 * WIDE)], chosen.at[:, pl.ds(0, 4 * WIDE)]
+    )
+
+    n.wait(rows.at[pl.ds(0, 24)], base_c + 7)
     for g in range(NE // NT):
         group = dot(unpack[...], rows[g * NT : (g + 1) * NT].reshape(NT * TILE, 128))
         for k in range(WIDTH // 128):
@@ -428,9 +469,17 @@
     dense_rest()
     pre = dot(dense_in[...], dense_w[...].reshape(WIDTH, 2 * WIDE))
     dense_hidden[pl.ds(n.t, 1)] = (jax.nn.silu(pre[:, :WIDE]) * pre[:, WIDE:]).astype(BF)[None]
-    units_relay, units_rest = n.gather_tp(lambda t: dense_hidden.at[t])
+    chosen_onward()
+    units_onward, units_relay, units_rest = n.gather_tp(
+        lambda t: dense_hidden.at[t], dense_hidden.at[pl.ds(0, 7)], dense_hidden.at[pl.ds(0, 4)]
+    )
+
+    decay, keygate = gates[0].T, gates[1].T
+    for b in range(SEQ):
+        held[b, 0] = decay[:, b : b + 1] * held[b, 0] + keygate[:, b : b + 1] * gates[2, b : b + 1, :]
 
     chosen_relay()
+    units_onward()
     chosen_rest()
     for copy in load_expert:
         copy.wait()
@@ -441,19 +490,12 @@
         pre = dot(chosen_in[pl.ds(j * SLOTS, SLOTS)], expert_w[:, 2 * j * FF : 2 * (j + 1) * FF])
         unit = (jax.nn.silu(pre[:, :FF]) * pre[:, FF:]).astype(BF)
         cols_at(hidden, n.t, FF).at[pl.ds(j * SLOTS, SLOTS)][...] = unit
-    hidden_relay, hidden_rest = n.gather_tp(lambda t: cols_at(hidden, t, FF))
-
-    rows_rest()
-    for copy in load_shared:
-        copy.wait()
-    shared_x = scaled(resid_rows[...], ffn_gain[...]).astype(BF)
-    shared_pre = dot(shared_x, shared_w[...])
-    shared_hidden = (jax.nn.silu(shared_pre[:, :FF]) * shared_pre[:, FF:]).astype(BF)
-    shared_part[...] = dot(shared_hidden, shared_d[...]).astype(BF)
-    shared_rest = n.swap_tp(lambda t: cols_at(shared_part, t, WIDE), lambda t: shared_in.at[t])
-    shared_in[pl.ds(n.t, 1)] = cols_at(shared_part, n.t, WIDE)[...][None]
+    hidden_onward, hidden_relay, hidden_rest = n.gather_tp(
+        lambda t: cols_at(hidden, t, FF), hidden.at[:, pl.ds(0, 7 * FF)], hidden.at[:, pl.ds(0, 4 * FF)]
+    )
 
     units_relay()
+    hidden_onward()
     units_rest()
     load_dense_d.wait()
     scale = jax.nn.sigmoid(dense_mix[...])
@@ -463,15 +505,16 @@
         inner = dot(order[...], unit_rows[...]).astype(BF)
         block = dot(inner, dense_d[...]) * scale
         sum_out[2 * g : 2 * g + 2] = block.astype(BF).reshape(2, NX, SEQ, WIDE)
-    base_x = n.reserve(NX * NZ)
-    for dz in FAR_ORDER:
-        z = (n.z + dz) % NZ
+    base_x = n.reserve(NZ)
+    send_x = n.stage(sum_in.at[pl.ds(0, 3)])
+    for i, dz in enumerate(FAR_ORDER):
         for dx in X_ORDER:
             x = (n.x + dx) % NX
-            n.send(sum_out.at[z, x], sum_in.at[n.x, z], base_x + n.x * NZ + z, x=x)
+            send_x(sum_out.at[z_at[dz], x], sum_in.at[n.x, z_at[dz]], base_x + i, x=x)
 
     hidden_relay()
-    down_rest()
+    for rest in down_rest:
+        rest()
     load_mine.wait()
     hidden_rest()
     outs = [
@@ -482,17 +525,17 @@
     back_rest = n.swap_ep(back_out, back_in)
     back_in[pl.ds(n.e, 1)] = back_out[pl.ds(n.e, 1)]
 
-    base_z = n.reserve(NZ)
-    for dz in FAR_ORDER:
-        z = (n.z + dz) % NZ
+    base_z = n.reserve(1)
+    send_z = n.stage(sum2_in.at[pl.ds(0, 7)])
+    for i, dz in enumerate(FAR_ORDER):
+        z = z_at[dz]
+        n.wait(sum_in.at[pl.ds(0, 3), z], base_x + i)
         block = sum_out[pl.ds(z, 1), n.x][0].astype(F32)
         for dx in X_ORDER:
-            x = (n.x + dx) % NX
-            n.wait(sum_in.at[x, z], base_x + x * NZ + z)
-            block = block + sum_in[x, pl.ds(z, 1)][0].astype(F32)
+            block = block + sum_in[(n.x + dx) % NX, pl.ds(z, 1)][0].astype(F32)
         if dz:
             sum2_out[pl.ds(z, 1)] = block.astype(BF)[None]
-            n.send(sum2_out.at[z], sum2_in.at[n.z], base_z + n.z, z=z)
+            send_z(sum2_out.at[z], sum2_in.at[n.z], base_z, z=z)
         else:
             sum2_in[pl.ds(n.z, 1)] = block.astype(BF)[None]
     back_rest()
@@ -505,38 +548,22 @@
     )
     for t in range(NT):
         result = result + shared_in[t].astype(F32)
-    for dz in Z_ORDER:
-        z = (n.z + dz) % NZ
-        n.wait(sum2_in.at[z], base_z + z)
+    n.wait(sum2_in.at[pl.ds(0, 7)], base_z)
     for z in range(NZ):
         result = result + sum2_in[z].astype(F32)
     mixed[...] = result
     n.finish()
 
 
-def closing(result, gates, state, mixed, new_state, held, sem):
-    rows = SEQ // STRIPS
-    strips = [pl.ds(i * rows, rows) for i in range(STRIPS)]
-    loads = [pltpu.make_async_copy(state.at[r], held.at[r], sem.at[i]) for i, r in enumerate(strips)]
-    stores = [
-        pltpu.make_async_copy(held.at[r], new_state.at[r], sem.at[STRIPS + i]) for i, r in enumerate(strips)
-    ]
-    for copy in loads:
-        copy.start()
+def closing(result, held, mixed, new_state, sem):
+    copy = pltpu.make_async_copy(held, new_state, sem)
+    copy.start()
     mixed[...] = result[...].astype(BF)
-    decay, keygate = gates[0].T, gates[1].T
-    for i in range(STRIPS):
-        loads[i].wait()
-        for b in range(i * rows, (i + 1) * rows):
-            held[b, 0] = decay[:, b : b + 1] * held[b, 0] + keygate[:, b : b + 1] * gates[2, b : b + 1, :]
-        stores[i].start()
-    for copy in stores:
-        copy.wait()
+    copy.wait()
 
 
 def local(*args):
     args = list(args)
-    state = args[1]
     for i in (2, 7, 8, 10, 22):
         args[i] = args[i].reshape(1, -1)
     for i in (11, 12):
@@ -550,7 +577,7 @@
         ((NT, WIDE, 2 * WIDE), BF),
         ((PAIR, FF, WIDTH), BF),
         ((PAIR, NT, FF, WIDE), BF),
-        ((SEQ, 1, HEAD, HEAD), F32),
+        ((3, SEQ, HEAD), F32),
         ((WIDTH, 2 * PAIR * FF), BF),
         ((WIDTH, 2 * FF), BF),
         ((FF, WIDTH), BF),
@@ -595,11 +622,11 @@
         ((PADDED, PAIR * SLOTS), BF),
         ((SEQ, WIDE), F32),
     ]
-    result, gates = pl.pallas_call(
+    result, held = pl.pallas_call(
         layer,
         out_shape=[
-            jax.ShapeDtypeStruct((SEQ, WIDE), F32),
-            jax.ShapeDtypeStruct((3, SEQ, HEAD), F32),
+            pltpu.VMEM((SEQ, WIDE), F32),
+            pltpu.VMEM((SEQ, 1, HEAD, HEAD), F32),
         ],
         in_specs=[vmem if i in small else hbm for i in range(len(args))],
         out_specs=[vmem, vmem],
@@ -618,14 +645,11 @@
             jax.ShapeDtypeStruct((SEQ, WIDE), BF),
             jax.ShapeDtypeStruct((SEQ, 1, HEAD, HEAD), F32),
         ],
-        in_specs=[vmem, vmem, hbm],
+        in_specs=[vmem, hbm],
         out_specs=[vmem, hbm],
-        scratch_shapes=[
-            pltpu.VMEM((SEQ, 1, HEAD, HEAD), F32),
-            pltpu.SemaphoreType.DMA((2 * STRIPS,)),
-        ],
+        scratch_shapes=[pltpu.SemaphoreType.DMA(())],
         name="closing",
-    )(result, gates, state)
+    )(pltpu.with_memory_space_constraint(result, pltpu.VMEM), pltpu.with_memory_space_constraint(held, pltpu.VMEM))
 
 
 def solution(mesh):

time: 95.9 us -> 83.3 us (0.87)
  Pallas kernels: 95.1 us -> 82.5 us
    pallas_call x1, Pallas kernels: 89.6 us -> 80.2 us  [local(): pl.pallas_call(layer, out_shape=[pltpu.VMEM((SEQ, WIDE), F32), pltpu.VMEM...]
    pallas_call x1, Pallas kernels: 5.56 us -> 2.28 us  [local(): pl.pallas_call(closing, out_shape=[jax.ShapeDtypeStruct((SEQ, WIDE), BF),...]
where the time goes in v4:
time: 83.3 us; the launch traced here: 83.1 us
  Pallas kernels  82.5 us (99%)
    pallas_call x1, Pallas kernels, local(): pl.pallas_call(layer, out_shape=[pltpu.VMEM((SEQ, WIDE), F32), pltpu.VMEM...  80.2 us
    pallas_call x1, Pallas kernels, local(): pl.pallas_call(closing, out_shape=[jax.ShapeDtypeStruct((SEQ, WIDE), BF),...  2.28 us

profile of v4, /device:TPU:1, one launch (start us, length us, event | category | flops | bytes accessed | tf_op | source)
XLA Modules:
  0.0 83.1 jit_solution(9837662454700251561)
XLA Ops:
  0.6 80.2 %layer.1 = (f32[48,256]{1,0:T(8,128)S(1)}, f32[48,1,128,128]{3,2,1,0:T(8,128)S(1)}) custom-call(bf16[48,2048]{1,0:T(8,128)(2,1)} %tokens.1, f32[48,1,128,128]{3,2,1,0:T(8,128)} %state.1, f32[1,2048]{1,0:T(1,128)} %bitcast.7, bf16[64,128]{1,0:T(8,128)(2,1)} %w_query.1, bf16[64,128]{1,0:T(8,128)(2,1)} %w_forget.1, bf16[64,128]{1,0:T(8,128)(2,1)} %w_input.1, ...), custom_call_target="tpu_custom_call" | custom-call | tf_op jit(solution)/shard_map/layer/pallas_call | solution.py:625
  80.9 2.3 %closing.1 = (bf16[48,256]{1,0:T(8,128)(2,1)}, f32[48,1,128,128]{3,2,1,0:T(8,128)}) custom-call(f32[48,256]{1,0:T(8,128)S(1)} %get-tuple-element.4.result, f32[48,1,128,128]{3,2,1,0:T(8,128)S(1)} %get-tuple-element.5.held), custom_call_target="tpu_custom_call" | custom-call | tf_op jit(solution)/shard_map/closing/pallas_call | solution.py:642

commit v5 on v4

--- a/solution.py
+++ b/solution.py
@@ -13,8 +13,9 @@
 MESH = pl.DeviceIdType.MESH
 EPS = 1e-06
 SEQ, WIDTH, HEAD, WIDE, TOPK = 48, 2048, 128, 256, 4
-PAIR, CAP, PAD = 2, 6, 16
-SLOTS, PADDED = NE * CAP, NE * PAD
+PAIR, CAP = 2, 6
+SLOTS, BOTH = NE * CAP, PAIR * CAP
+LINES = NE * 2 * BOTH
 ROWS = SEQ * NE // NT
 FF = 128
 OWN = SEQ // NT
@@ -25,7 +26,7 @@
 Y_ORDER = (1, 3, 2)
 X_ORDER = (1, 3, 2)
 FAR_ORDER = (4, 3, 5, 2, 6, 1, 7, 0)
-SENDS, ARRIVALS, LOCALS = 18, 62, 19
+SENDS, ARRIVALS, LOCALS = 18, 67, 19
 scope = jax.named_scope
 
 
@@ -114,8 +115,8 @@
             pl.semaphore_signal(barrier, inc=1, device_id=peer, device_id_type=MESH)
         return lambda: pl.semaphore_wait(barrier, len(peers))
 
-    def gather_tp(self, view, seven, four):
-        base = self.reserve(7)
+    def gather_tp(self, view, seven):
+        base = self.reserve(10)
         send = self.stage(seven)
         up, down = (self.y + 1) % NY, (self.y + NY - 1) % NY
         far = (self.y + 2) % NY
@@ -140,17 +141,18 @@
         def relay():
             self.wait(half(down, 1), base + 1)
             block = view(down * NC + self.c)
-            send(block, block, base + 6, c=1 - self.c)
+            send(block, block, base + 7, c=1 - self.c)
             self.wait(half(up, 0), base + 3)
             block = view(up * NC + self.c)
-            send(block, block, base + 6, c=1 - self.c)
+            send(block, block, base + 8, c=1 - self.c)
             self.wait(half(far, 0), base + 4)
             self.wait(half(far, 1), base + 5)
             block = view(far * NC + self.c)
-            send(block, block, base + 6, c=1 - self.c)
-
-        def rest():
-            self.wait(four, base + 6)
+            send(block, block, base + 9, c=1 - self.c)
+
+        def rest(only=range(4)):
+            for i in only:
+                self.wait(view((self.y, down, up, far)[i] * NC + 1 - self.c), base + 6 + i)
 
         return onward, relay, rest
 
@@ -227,7 +229,7 @@
     pack,
     unpack,
     order,
-    unit_rows,
+    regroup,
     dense_raw,
     resid_rows,
     slot_out,
@@ -250,6 +252,7 @@
     dispatch,
     squeeze,
     expand,
+    second,
     resid,
     send_sem,
     recv_sem,
@@ -306,7 +309,7 @@
     for copy in load_dense:
         copy.wait()
     dense_onward, dense_relay, dense_rest = n.gather_tp(
-        lambda t: dense_w.at[t], dense_w.at[pl.ds(0, 7)], dense_w.at[pl.ds(0, 4)]
+        lambda t: dense_w.at[t], dense_w.at[pl.ds(0, 7)]
     )
 
     with scope("routes"):
@@ -315,27 +318,38 @@
         equal = [(expert_row == ids).astype(F32) for ids in named]
         earlier = (iota((SEQ, SEQ), 0) < iota((SEQ, SEQ), 1)).astype(BF)
         rank = dot(sum(equal).astype(BF), earlier)
-        slot_row = iota((PADDED, SEQ), 0).astype(F32)
-        total = jnp.zeros((PADDED, SEQ), F32)
-        picked = jnp.zeros((PADDED, SEQ), F32)
+        line = iota((LINES, SEQ), 0).astype(F32)
+        halves = [jnp.zeros((LINES, SEQ), F32) for _ in range(2)]
+        picked = jnp.zeros((LINES, SEQ), F32)
         for k in range(TOPK):
             ids = named[k]
-            first = (ids // 2) * PAD + (ids % 2) * CAP
+            first = (ids // PAIR) * (2 * BOTH) + (ids % PAIR) * CAP
             place = first.astype(F32) + jnp.sum(equal[k] * rank, axis=0, keepdims=True)
-            here = slot_row == place
-            total = total + jnp.where(here, route_weight[k : k + 1, :], 0.0)
-            picked = picked + here.astype(F32)
+            for h in range(2):
+                here = line == place + h * BOTH
+                halves[h] = halves[h] + jnp.where(here, route_weight[k : k + 1, :], 0.0)
+                picked = picked + here.astype(F32)
         dispatch[...] = picked.astype(BF)
-        combine[...] = total.T
-
-    def row_of(slot):
-        inside = slot % PAD
-        second = (inside >= CAP).astype(jnp.int32)
-        row = second * SLOTS + (slot // PAD) * CAP + inside - second * CAP
-        return jnp.where(inside < PAIR * CAP, row, -1)
-
-    squeeze[...] = (iota((PAIR * SLOTS, PADDED), 0) == row_of(iota((1, PADDED), 1))).astype(F32).astype(BF)
-    expand[...] = (iota((PADDED, PAIR * SLOTS), 1) == row_of(iota((PADDED, 1), 0))).astype(F32).astype(BF)
+        for h in range(2):
+            combine[h, :, :] = halves[h].T
+
+    def row_of(place):
+        inside = place % BOTH
+        return (inside // CAP) * SLOTS + (place // (2 * BOTH)) * CAP + inside % CAP
+
+    def is_second(place):
+        return (place // BOTH) % 2
+
+    across, along = iota((1, LINES), 1), iota((LINES, 1), 0)
+    row = iota((PAIR * SLOTS, LINES), 0)
+    for h in range(2):
+        target = jnp.where(is_second(across) == h, row_of(across), -1)
+        squeeze[h, :, :] = (row == target).astype(F32).astype(BF)
+    expand[...] = (iota((LINES, PAIR * SLOTS), 1) == row_of(along)).astype(F32).astype(BF)
+    second[...] = jnp.broadcast_to(is_second(along), (LINES, 128)).astype(F32)
+
+    def in_lines(values):
+        return jnp.where(second[...] > 0.5, values[:, 128:], values[:, :128]).astype(BF).reshape(NE, 2 * BOTH, 128)
 
     def packed_row(row):
         inside = row % SEQ
@@ -344,11 +358,16 @@
     def ordered_row(row):
         inside = row % SEQ
         return (inside // OWN) * SEQ + (row // SEQ) * OWN + inside % OWN
+
+    def regrouped_row(row):
+        e = row // OWN
+        return (e % NX) * SEQ + (e // NX) * OWN + row % OWN
 
     many, few = NT * TILE, NT * SEQ
     pack[...] = (iota((many, many), 0) == packed_row(iota((1, many), 1))).astype(F32).astype(BF)
     unpack[...] = (iota((many, many), 1) == packed_row(iota((many, 1), 0))).astype(F32).astype(BF)
     order[...] = (iota((few, few), 0) == ordered_row(iota((1, few), 1))).astype(F32).astype(BF)
+    regroup[...] = (iota((ROWS, ROWS), 0) == regrouped_row(iota((1, ROWS), 1))).astype(F32).astype(BF)
     for k in range(WIDTH // 128):
         flat[k * SEQ : (k + 1) * SEQ, :] = tok[:, k * 128 : (k + 1) * 128]
     tok_rows[...] = dot(pack[...], flat[...]).astype(BF).reshape(NT, TILE, 128)
@@ -425,7 +444,7 @@
         own = own + head_in[t].astype(F32)
     resid[...] = own
     own_cols = own.astype(BF)
-    slot_out[...] = dot(dispatch[...], own_cols).astype(BF).reshape(NE, PAD, WIDE)
+    slot_out[...] = in_lines(dot(dispatch[...], own_cols))
     slots_rest = n.swap_ep(slot_out, slot_in)
     slot_in[pl.ds(n.e, 1)] = slot_out[pl.ds(n.e, 1)]
     cols_at(resid_rows, n.t, WIDE)[...] = own_cols
@@ -454,10 +473,11 @@
     shared_in[pl.ds(n.t, 1)] = cols_at(shared_part, n.t, WIDE)[...][None]
 
     slots_rest()
-    picked_rows = dot(squeeze[...], slot_in[...].reshape(PADDED, WIDE)).astype(BF)
-    cols_at(chosen, n.t, WIDE)[...] = picked_rows
+    lines = slot_in[...].reshape(LINES, 128)
+    picked_rows = jnp.concatenate([dot(squeeze[h], lines) for h in range(2)], axis=1)
+    cols_at(chosen, n.t, WIDE)[...] = picked_rows.astype(BF)
     chosen_onward, chosen_relay, chosen_rest = n.gather_tp(
-        lambda t: cols_at(chosen, t, WIDE), chosen.at[:, pl.ds(0, 7 * WIDE)], chosen.at[:, pl.ds(0, 4 * WIDE)]
+        lambda t: cols_at(chosen, t, WIDE), chosen.at[:, pl.ds(0, 7 * WIDE)]
     )
 
     n.wait(rows.at[pl.ds(0, 24)], base_c + 7)
@@ -471,13 +491,31 @@
     dense_hidden[pl.ds(n.t, 1)] = (jax.nn.silu(pre[:, :WIDE]) * pre[:, WIDE:]).astype(BF)[None]
     chosen_onward()
     units_onward, units_relay, units_rest = n.gather_tp(
-        lambda t: dense_hidden.at[t], dense_hidden.at[pl.ds(0, 7)], dense_hidden.at[pl.ds(0, 4)]
+        lambda t: dense_hidden.at[t], dense_hidden.at[pl.ds(0, 7)]
     )
+
+    load_dense_d.wait()
+    scale = jax.nn.sigmoid(dense_mix[...])
+    base_x = n.reserve(1)
+    send_x = n.stage(sum_in.at[pl.ds(0, 3)])
+
+    def emit(dy, same):
+        t = ((n.y + dy) % NY) * NC + (n.c if same else 1 - n.c)
+        inner = dot(regroup[...], dense_hidden[pl.ds(t, 1)][0]).astype(BF)
+        block = dot(inner, dense_d[...]) * scale
+        sum_out[pl.ds(t, 1)] = block.astype(BF).reshape(1, NX, SEQ, WIDE)
+        for dx in X_ORDER:
+            x = (n.x + dx) % NX
+            send_x(sum_out.at[t, x], sum_in.at[n.x, t], base_x, x=x)
+
+    emit(0, True)
 
     decay, keygate = gates[0].T, gates[1].T
     for b in range(SEQ):
         held[b, 0] = decay[:, b : b + 1] * held[b, 0] + keygate[:, b : b + 1] * gates[2, b : b + 1, :]
 
+    units_rest([0])
+    emit(0, False)
     chosen_relay()
     units_onward()
     chosen_rest()
@@ -491,26 +529,16 @@
         unit = (jax.nn.silu(pre[:, :FF]) * pre[:, FF:]).astype(BF)
         cols_at(hidden, n.t, FF).at[pl.ds(j * SLOTS, SLOTS)][...] = unit
     hidden_onward, hidden_relay, hidden_rest = n.gather_tp(
-        lambda t: cols_at(hidden, t, FF), hidden.at[:, pl.ds(0, 7 * FF)], hidden.at[:, pl.ds(0, 4 * FF)]
+        lambda t: cols_at(hidden, t, FF), hidden.at[:, pl.ds(0, 7 * FF)]
     )
 
     units_relay()
+    for dy in (3, 1, 2):
+        emit(dy, True)
     hidden_onward()
-    units_rest()
-    load_dense_d.wait()
-    scale = jax.nn.sigmoid(dense_mix[...])
-    for g in range(NE // NT):
-        for t in range(NT):
-            unit_rows[t * SEQ : (t + 1) * SEQ, :] = dense_hidden[t, g * SEQ : (g + 1) * SEQ, :]
-        inner = dot(order[...], unit_rows[...]).astype(BF)
-        block = dot(inner, dense_d[...]) * scale
-        sum_out[2 * g : 2 * g + 2] = block.astype(BF).reshape(2, NX, SEQ, WIDE)
-    base_x = n.reserve(NZ)
-    send_x = n.stage(sum_in.at[pl.ds(0, 3)])
-    for i, dz in enumerate(FAR_ORDER):
-        for dx in X_ORDER:
-            x = (n.x + dx) % NX
-            send_x(sum_out.at[z_at[dz], x], sum_in.at[n.x, z_at[dz]], base_x + i, x=x)
+    for i, dy in ((1, 3), (2, 1), (3, 2)):
+        units_rest([i])
+        emit(dy, False)
 
     hidden_relay()
     for rest in down_rest:
@@ -521,31 +549,27 @@
         dot(hidden[pl.ds(j * SLOTS, SLOTS)], down_all[j].reshape(NT * FF, WIDE)).astype(BF) for j in range(PAIR)
     ]
     spread = dot(expand[:, :SLOTS], outs[0]) + dot(expand[:, SLOTS:], outs[1])
-    back_out[...] = spread.astype(BF).reshape(NE, PAD, WIDE)
+    back_out[...] = in_lines(spread)
     back_rest = n.swap_ep(back_out, back_in)
     back_in[pl.ds(n.e, 1)] = back_out[pl.ds(n.e, 1)]
 
+    n.wait(sum_in.at[pl.ds(0, 3)], base_x)
+    block = sum_out[:, pl.ds(n.x, 1)].reshape(NT * SEQ, WIDE).astype(F32)
+    for dx in X_ORDER:
+        block = block + sum_in[pl.ds((n.x + dx) % NX, 1)].reshape(NT * SEQ, WIDE).astype(F32)
+    sum2_out[...] = dot(order[...], block.astype(BF)).astype(BF).reshape(NZ, SEQ, WIDE)
     base_z = n.reserve(1)
     send_z = n.stage(sum2_in.at[pl.ds(0, 7)])
-    for i, dz in enumerate(FAR_ORDER):
-        z = z_at[dz]
-        n.wait(sum_in.at[pl.ds(0, 3), z], base_x + i)
-        block = sum_out[pl.ds(z, 1), n.x][0].astype(F32)
-        for dx in X_ORDER:
-            block = block + sum_in[(n.x + dx) % NX, pl.ds(z, 1)][0].astype(F32)
-        if dz:
-            sum2_out[pl.ds(z, 1)] = block.astype(BF)[None]
-            send_z(sum2_out.at[z], sum2_in.at[n.z], base_z, z=z)
-        else:
-            sum2_in[pl.ds(n.z, 1)] = block.astype(BF)[None]
+    for dz in FAR_ORDER[:-1]:
+        send_z(sum2_out.at[z_at[dz]], sum2_in.at[n.z], base_z, z=z_at[dz])
+    sum2_in[pl.ds(n.z, 1)] = sum2_out[pl.ds(n.z, 1)]
     back_rest()
     shared_rest()
-    result = resid[...] + jnp.dot(
-        combine[...],
-        back_in[...].reshape(PADDED, WIDE).astype(F32),
-        preferred_element_type=F32,
-        precision=lax.Precision.HIGHEST,
-    )
+    lines = back_in[...].reshape(LINES, 128).astype(F32)
+    routed = [
+        jnp.dot(combine[h], lines, preferred_element_type=F32, precision=lax.Precision.HIGHEST) for h in range(2)
+    ]
+    result = resid[...] + jnp.concatenate(routed, axis=1)
     for t in range(NT):
         result = result + shared_in[t].astype(F32)
     n.wait(sum2_in.at[pl.ds(0, 7)], base_z)
@@ -597,11 +621,11 @@
         ((NT * TILE, NT * TILE), BF),
         ((NT * TILE, NT * TILE), BF),
         ((NT * SEQ, NT * SEQ), BF),
-        ((NT * SEQ, WIDE), BF),
+        ((ROWS, ROWS), BF),
         ((SEQ, WIDTH), F32),
         ((SEQ, WIDTH), BF),
-        ((NE, PAD, WIDE), BF),
-        ((NE, PAD, WIDE), BF),
+        ((NE, 2 * BOTH, 128), BF),
+        ((NE, 2 * BOTH, 128), BF),
         ((PAIR * SLOTS, WIDTH), BF),
         ((PAIR * SLOTS, WIDTH), BF),
         ((ROWS, WIDTH), BF),
@@ -609,17 +633,18 @@
         ((PAIR * SLOTS, NT * FF), BF),
         ((SEQ, WIDTH), BF),
         ((NT, SEQ, WIDE), BF),
-        ((NZ, NX, SEQ, WIDE), BF),
-        ((NX, NZ, SEQ, WIDE), BF),
+        ((NT, NX, SEQ, WIDE), BF),
+        ((NX, NT, SEQ, WIDE), BF),
         ((NZ, SEQ, WIDE), BF),
         ((NZ, SEQ, WIDE), BF),
-        ((NE, PAD, WIDE), BF),
-        ((NE, PAD, WIDE), BF),
+        ((NE, 2 * BOTH, 128), BF),
+        ((NE, 2 * BOTH, 128), BF),
         ((SEQ, HEAD), F32),
-        ((SEQ, PADDED), F32),
-        ((PADDED, SEQ), BF),
-        ((PAIR * SLOTS, PADDED), BF),
-        ((PADDED, PAIR * SLOTS), BF),
+        ((2, SEQ, LINES), F32),
+        ((LINES, SEQ), BF),
+        ((2, PAIR * SLOTS, LINES), BF),
+        ((LINES, PAIR * SLOTS), BF),
+        ((LINES, 128), F32),
         ((SEQ, WIDE), F32),
     ]
     result, held = pl.pallas_call(

time: 83.3 us -> 82 us (0.984)
  Pallas kernels: 82.5 us -> 81 us
    pallas_call x1, Pallas kernels: 80.2 us -> 78.7 us  [local(): pl.pallas_call(layer, out_shape=[pltpu.VMEM((SEQ, WIDE), F32), pltpu.VMEM...]
where the time goes in v5:
time: 82 us; the launch traced here: 81.8 us
  Pallas kernels  81 us (99%)
    pallas_call x1, Pallas kernels, local(): pl.pallas_call(layer, out_shape=[pltpu.VMEM((SEQ, WIDE), F32), pltpu.VMEM...  78.7 us
    pallas_call x1, Pallas kernels, local(): pl.pallas_call(closing, out_shape=[jax.ShapeDtypeStruct((SEQ, WIDE), BF),...  2.28 us

profile of v5, /device:TPU:1, one launch (start us, length us, event | category | flops | bytes accessed | tf_op | source)
XLA Modules:
  0.0 81.8 jit_solution(7813523305857189041)
XLA Ops:
  0.6 78.7 %layer.1 = (f32[48,256]{1,0:T(8,128)S(1)}, f32[48,1,128,128]{3,2,1,0:T(8,128)S(1)}) custom-call(bf16[48,2048]{1,0:T(8,128)(2,1)} %tokens.1, f32[48,1,128,128]{3,2,1,0:T(8,128)} %state.1, f32[1,2048]{1,0:T(1,128)} %bitcast.7, bf16[64,128]{1,0:T(8,128)(2,1)} %w_query.1, bf16[64,128]{1,0:T(8,128)(2,1)} %w_forget.1, bf16[64,128]{1,0:T(8,128)(2,1)} %w_input.1, ...), custom_call_target="tpu_custom_call" | custom-call | tf_op jit(solution)/shard_map/layer/pallas_call | solution.py:650
  79.4 2.3 %closing.1 = (bf16[48,256]{1,0:T(8,128)(2,1)}, f32[48,1,128,128]{3,2,1,0:T(8,128)}) custom-call(f32[48,256]{1,0:T(8,128)S(1)} %get-tuple-element.4.result, f32[48,1,128,128]{3,2,1,0:T(8,128)S(1)} %get-tuple-element.5.held), custom_call_target="tpu_custom_call" | custom-call | tf_op jit(solution)/shard_map/closing/pallas_call | solution.py:667

commit v6 on v5

--- a/solution.py
+++ b/solution.py
@@ -26,7 +26,7 @@
 Y_ORDER = (1, 3, 2)
 X_ORDER = (1, 3, 2)
 FAR_ORDER = (4, 3, 5, 2, 6, 1, 7, 0)
-SENDS, ARRIVALS, LOCALS = 18, 67, 19
+SENDS, ARRIVALS, LOCALS = 21, 70, 19
 scope = jax.named_scope
 
 
@@ -237,7 +237,6 @@
     chosen,
     chosen_in,
     dense_in,
-    dense_hidden,
     hidden,
     shared_part,
     shared_in,
@@ -245,6 +244,10 @@
     sum_in,
     sum2_out,
     sum2_in,
+    swap_out,
+    swap_in,
+    pad_lines,
+    take_lines,
     back_out,
     back_in,
     readout,
@@ -283,7 +286,7 @@
         for j in range(PAIR)
         for i, w in enumerate((expert_gate, expert_up))
     ]
-    load_dense_d = n.load(dense_down, dense_d)
+    load_dense_d = n.load(dense_down, cols_at(dense_d, n.t, WIDE))
 
     load_tok.wait()
     normed = scaled(tok[...], norm_gain[...]).astype(BF)
@@ -310,6 +313,10 @@
         copy.wait()
     dense_onward, dense_relay, dense_rest = n.gather_tp(
         lambda t: dense_w.at[t], dense_w.at[pl.ds(0, 7)]
+    )
+    load_dense_d.wait()
+    last_onward, last_relay, last_rest = n.gather_tp(
+        lambda t: cols_at(dense_d, t, WIDE), dense_d.at[:, pl.ds(0, 7 * WIDE)]
     )
 
     with scope("routes"):
@@ -367,6 +374,12 @@
     pack[...] = (iota((many, many), 0) == packed_row(iota((1, many), 1))).astype(F32).astype(BF)
     unpack[...] = (iota((many, many), 1) == packed_row(iota((many, 1), 0))).astype(F32).astype(BF)
     order[...] = (iota((few, few), 0) == ordered_row(iota((1, few), 1))).astype(F32).astype(BF)
+    line = iota((1, TILE), 1)
+    pad_lines[...] = (iota((NT * 16, TILE), 0) == (line // 12) * 16 + line % 12).astype(F32).astype(BF)
+    token = iota((SEQ, 1), 0)
+    for h in range(2):
+        source = (token // OWN) * 16 + h * OWN + token % OWN
+        take_lines[h, :, :] = (iota((SEQ, NT * 16), 1) == source).astype(F32).astype(BF)
     regroup[...] = (iota((ROWS, ROWS), 0) == regrouped_row(iota((1, ROWS), 1))).astype(F32).astype(BF)
     for k in range(WIDTH // 128):
         flat[k * SEQ : (k + 1) * SEQ, :] = tok[:, k * 128 : (k + 1) * 128]
@@ -379,10 +392,6 @@
         block = wz.at[z_at[source], pl.ds(row, 32)]
         send_w(block, block, base_w + 5 + slot, z=z_at[far])
     dense_onward()
-    load_down.wait()
-    down_rest = [
-        n.swap_tp(lambda t: cols_at(down_own.at[0], t, WIDE), lambda t: down_all.at[0, t], down_all.at[0, pl.ds(0, 7)])
-    ]
     n.wait(tok_in.at[pl.ds(0, 3)], base_t)
     n.wait(wz.at[pl.ds(0, 2)], base_w + 2)
     for slot in range(2):
@@ -417,20 +426,30 @@
     head_out = (read * head_gain[...] * jax.nn.silu(out_gate)).astype(BF)
     load_out.wait()
     whole = dot(head_out, out_w[...]).astype(BF)
+    head_part[...] = whole
+    head_rest = n.swap_tp(lambda t: cols_at(head_part, t, WIDE), lambda t: head_in.at[t], head_in.at[pl.ds(0, 7)])
     for k in range(WIDTH // 128):
         flat[k * SEQ : (k + 1) * SEQ, :] = whole[:, k * 128 : (k + 1) * 128]
     row_out[...] = dot(pack[...], flat[...]).astype(BF).reshape(NT, TILE, 128)
     row_rest = n.swap_tp(lambda t: row_out.at[t], lambda t: row_in.at[t], row_in.at[pl.ds(0, 7)])
-    head_part[...] = whole
-    head_rest = n.swap_tp(lambda t: cols_at(head_part, t, WIDE), lambda t: head_in.at[t], head_in.at[pl.ds(0, 7)])
     row_in[pl.ds(n.t, 1)] = row_out[pl.ds(n.t, 1)]
     head_in[pl.ds(n.t, 1)] = cols_at(head_part, n.t, WIDE)[...][None]
+    last_onward()
+    head_rest()
+    own = cols_at(tok, n.t, WIDE)[...].astype(F32)
+    for t in range(NT):
+        own = own + head_in[t].astype(F32)
+    own_cols = own.astype(BF)
+    slot_out[...] = in_lines(dot(dispatch[...], own_cols))
+    slots_rest = n.swap_ep(slot_out, slot_in)
+    slot_in[pl.ds(n.e, 1)] = slot_out[pl.ds(n.e, 1)]
+    resid[...] = own
+
     row_rest()
     own = tok_rows[pl.ds(n.t, 1)][0].astype(F32)
     for t in range(NT):
         own = own + row_in[t].astype(F32)
     rows[pl.ds(n.e, 1)] = own.astype(BF)[None]
-
     base_c = n.reserve(NZ)
     send_c = n.stage(rows.at[pl.ds(0, NE - 1)])
     mine = rows.at[n.e]
@@ -438,28 +457,37 @@
         send_c(mine, mine, base_c + i, z=z_at[dz])
     for dx in X_ORDER:
         send_c(mine, mine, base_c + 7, x=(n.x + dx) % NX)
-    head_rest()
-    own = cols_at(tok, n.t, WIDE)[...].astype(F32)
-    for t in range(NT):
-        own = own + head_in[t].astype(F32)
-    resid[...] = own
-    own_cols = own.astype(BF)
-    slot_out[...] = in_lines(dot(dispatch[...], own_cols))
-    slots_rest = n.swap_ep(slot_out, slot_in)
-    slot_in[pl.ds(n.e, 1)] = slot_out[pl.ds(n.e, 1)]
     cols_at(resid_rows, n.t, WIDE)[...] = own_cols
     rows_mine = cols_at(resid_rows, n.t, WIDE)
     rows_seven = resid_rows.at[:, pl.ds(0, 7 * WIDE)]
     rows_rest = n.swap_tp(lambda t: rows_mine, lambda t: cols_at(resid_rows, t, WIDE), rows_seven)
-    down_rest.append(
-        n.swap_tp(lambda t: cols_at(down_own.at[1], t, WIDE), lambda t: down_all.at[1, t], down_all.at[1, pl.ds(0, 7)])
+    load_down.wait()
+
+    def swap_down(j):
+        here = down_all.at[j]
+        return n.swap_tp(lambda t: cols_at(down_own.at[j], t, WIDE), lambda t: here.at[t], here.at[pl.ds(0, 7)])
+
+    down_rest = [swap_down(0)]
+    dense_relay()
+    last_relay()
+
+    def pass_on(order):
+        for i in order:
+            e = z_at[(NZ - Z_ORDER[i]) % NZ] * NX + n.x
+            n.wait(rows.at[e], base_c + i)
+            for dx in X_ORDER:
+                send_c(rows.at[e], rows.at[e], base_c + 7, x=(n.x + dx) % NX)
+
+    pass_on(range(2))
+
+    slots_rest()
+    lines = slot_in[...].reshape(LINES, 128)
+    picked_rows = jnp.concatenate([dot(squeeze[h], lines) for h in range(2)], axis=1)
+    cols_at(chosen, n.t, WIDE)[...] = picked_rows.astype(BF)
+    chosen_onward, chosen_relay, chosen_rest = n.gather_tp(
+        lambda t: cols_at(chosen, t, WIDE), chosen.at[:, pl.ds(0, 7 * WIDE)]
     )
-    dense_relay()
-    for i, dz in enumerate(Z_ORDER):
-        e = z_at[(NZ - dz) % NZ] * NX + n.x
-        n.wait(rows.at[e], base_c + i)
-        for dx in X_ORDER:
-            send_c(rows.at[e], rows.at[e], base_c + 7, x=(n.x + dx) % NX)
+    pass_on(range(2, 7))
 
     gain = ffn_gain[...]
     rows_rest()
@@ -469,18 +497,11 @@
     shared_pre = dot(shared_x, shared_w[...])
     shared_hidden = (jax.nn.silu(shared_pre[:, :FF]) * shared_pre[:, FF:]).astype(BF)
     shared_part[...] = dot(shared_hidden, shared_d[...]).astype(BF)
-    shared_rest = n.swap_tp(lambda t: cols_at(shared_part, t, WIDE), lambda t: shared_in.at[t], shared_in.at[pl.ds(0, 7)])
-    shared_in[pl.ds(n.t, 1)] = cols_at(shared_part, n.t, WIDE)[...][None]
-
-    slots_rest()
-    lines = slot_in[...].reshape(LINES, 128)
-    picked_rows = jnp.concatenate([dot(squeeze[h], lines) for h in range(2)], axis=1)
-    cols_at(chosen, n.t, WIDE)[...] = picked_rows.astype(BF)
-    chosen_onward, chosen_relay, chosen_rest = n.gather_tp(
-        lambda t: cols_at(chosen, t, WIDE), chosen.at[:, pl.ds(0, 7 * WIDE)]
-    )
+    chosen_onward()
+    down_rest.append(swap_down(1))
 
     n.wait(rows.at[pl.ds(0, 24)], base_c + 7)
+    chosen_relay()
     for g in range(NE // NT):
         group = dot(unpack[...], rows[g * NT : (g + 1) * NT].reshape(NT * TILE, 128))
         for k in range(WIDTH // 128):
@@ -488,36 +509,17 @@
         dense_in[g * SEQ : (g + 1) * SEQ, :] = scaled(dense_raw[...], gain).astype(BF)
     dense_rest()
     pre = dot(dense_in[...], dense_w[...].reshape(WIDTH, 2 * WIDE))
-    dense_hidden[pl.ds(n.t, 1)] = (jax.nn.silu(pre[:, :WIDE]) * pre[:, WIDE:]).astype(BF)[None]
-    chosen_onward()
-    units_onward, units_relay, units_rest = n.gather_tp(
-        lambda t: dense_hidden.at[t], dense_hidden.at[pl.ds(0, 7)]
-    )
-
-    load_dense_d.wait()
-    scale = jax.nn.sigmoid(dense_mix[...])
-    base_x = n.reserve(1)
-    send_x = n.stage(sum_in.at[pl.ds(0, 3)])
-
-    def emit(dy, same):
-        t = ((n.y + dy) % NY) * NC + (n.c if same else 1 - n.c)
-        inner = dot(regroup[...], dense_hidden[pl.ds(t, 1)][0]).astype(BF)
-        block = dot(inner, dense_d[...]) * scale
-        sum_out[pl.ds(t, 1)] = block.astype(BF).reshape(1, NX, SEQ, WIDE)
+    units = (jax.nn.silu(pre[:, :WIDE]) * pre[:, WIDE:]).astype(BF)
+    inner = dot(regroup[...], units).astype(BF)
+    last_rest()
+    base_x = n.reserve(2)
+    for h in range(2):
+        block = dot(inner, dense_d[:, h * 1024 : (h + 1) * 1024])
+        sum_out[h, :, :, :] = block.astype(BF).reshape(NX, SEQ, 1024)
+        send_x = n.stage(sum_in.at[h, pl.ds(0, 3)])
         for dx in X_ORDER:
             x = (n.x + dx) % NX
-            send_x(sum_out.at[t, x], sum_in.at[n.x, t], base_x, x=x)
-
-    emit(0, True)
-
-    decay, keygate = gates[0].T, gates[1].T
-    for b in range(SEQ):
-        held[b, 0] = decay[:, b : b + 1] * held[b, 0] + keygate[:, b : b + 1] * gates[2, b : b + 1, :]
-
-    units_rest([0])
-    emit(0, False)
-    chosen_relay()
-    units_onward()
+            send_x(sum_out.at[h, x], sum_in.at[h, n.x], base_x + h, x=x)
     chosen_rest()
     for copy in load_expert:
         copy.wait()
@@ -532,15 +534,33 @@
         lambda t: cols_at(hidden, t, FF), hidden.at[:, pl.ds(0, 7 * FF)]
     )
 
-    units_relay()
-    for dy in (3, 1, 2):
-        emit(dy, True)
+    decay, keygate = gates[0].T, gates[1].T
+    for b in range(SEQ):
+        held[b, 0] = decay[:, b : b + 1] * held[b, 0] + keygate[:, b : b + 1] * gates[2, b : b + 1, :]
+
+    base_z = n.reserve(2)
+
+    def sum_over_x(h):
+        n.wait(sum_in.at[h, pl.ds(0, 3)], base_x + h)
+        block = sum_out[h, pl.ds(n.x, 1)][0].astype(F32)
+        for dx in X_ORDER:
+            block = block + sum_in[h, pl.ds((n.x + dx) % NX, 1)][0].astype(F32)
+        block = block.astype(BF)
+        for k in range(8):
+            flat[k * SEQ : (k + 1) * SEQ, :] = block[:, k * 128 : (k + 1) * 128]
+        sum2_out[h, :, :, :] = dot(order[...], flat[: 8 * SEQ]).astype(BF).reshape(NZ, SEQ, 128)
+        send_z = n.stage(sum2_in.at[h, pl.ds(0, 7)])
+        for dz in FAR_ORDER[:-1]:
+            send_z(sum2_out.at[h, z_at[dz]], sum2_in.at[h, n.z], base_z + h, z=z_at[dz])
+        sum2_in[h, pl.ds(n.z, 1)] = sum2_out[h, pl.ds(n.z, 1)]
+
     hidden_onward()
-    for i, dy in ((1, 3), (2, 1), (3, 2)):
-        units_rest([i])
-        emit(dy, False)
-
+    sum_over_x(0)
     hidden_relay()
+    sum_over_x(1)
+
+    shared_rest = n.swap_tp(lambda t: cols_at(shared_part, t, WIDE), lambda t: shared_in.at[t], shared_in.at[pl.ds(0, 7)])
+    shared_in[pl.ds(n.t, 1)] = cols_at(shared_part, n.t, WIDE)[...][None]
     for rest in down_rest:
         rest()
     load_mine.wait()
@@ -553,16 +573,17 @@
     back_rest = n.swap_ep(back_out, back_in)
     back_in[pl.ds(n.e, 1)] = back_out[pl.ds(n.e, 1)]
 
-    n.wait(sum_in.at[pl.ds(0, 3)], base_x)
-    block = sum_out[:, pl.ds(n.x, 1)].reshape(NT * SEQ, WIDE).astype(F32)
-    for dx in X_ORDER:
-        block = block + sum_in[pl.ds((n.x + dx) % NX, 1)].reshape(NT * SEQ, WIDE).astype(F32)
-    sum2_out[...] = dot(order[...], block.astype(BF)).astype(BF).reshape(NZ, SEQ, WIDE)
-    base_z = n.reserve(1)
-    send_z = n.stage(sum2_in.at[pl.ds(0, 7)])
-    for dz in FAR_ORDER[:-1]:
-        send_z(sum2_out.at[z_at[dz]], sum2_in.at[n.z], base_z, z=z_at[dz])
-    sum2_in[pl.ds(n.z, 1)] = sum2_out[pl.ds(n.z, 1)]
+    own_lines = []
+    for h in range(2):
+        n.wait(sum2_in.at[h, pl.ds(0, 7)], base_z + h)
+        acc = sum2_in[h, 0].astype(F32)
+        for z in range(1, NZ):
+            acc = acc + sum2_in[h, z].astype(F32)
+        own_lines.append(acc)
+    own_lines = jnp.concatenate(own_lines, axis=0).astype(BF)
+    swap_out[...] = dot(pad_lines[...], own_lines).astype(BF).reshape(NT, 16, 128)
+    swap_rest = n.swap_tp(lambda t: swap_out.at[t], lambda t: swap_in.at[t], swap_in.at[pl.ds(0, 7)])
+    swap_in[pl.ds(n.t, 1)] = swap_out[pl.ds(n.t, 1)]
     back_rest()
     shared_rest()
     lines = back_in[...].reshape(LINES, 128).astype(F32)
@@ -572,9 +593,10 @@
     result = resid[...] + jnp.concatenate(routed, axis=1)
     for t in range(NT):
         result = result + shared_in[t].astype(F32)
-    n.wait(sum2_in.at[pl.ds(0, 7)], base_z)
-    for z in range(NZ):
-        result = result + sum2_in[z].astype(F32)
+    swap_rest()
+    lines = swap_in[...].reshape(NT * 16, 128)
+    dense_out = jnp.concatenate([dot(take_lines[h], lines) for h in range(2)], axis=1)
+    result = result + dense_out * jax.nn.sigmoid(dense_mix[...])
     mixed[...] = result
     n.finish()
 
@@ -606,7 +628,7 @@
         ((WIDTH, 2 * FF), BF),
         ((FF, WIDTH), BF),
         ((HEAD, WIDTH), BF),
-        ((WIDE, WIDE), BF),
+        ((WIDE, WIDTH), BF),
         ((NX, SEQ, 512), BF),
         ((NX, SEQ, 512), BF),
         ((NX, SEQ, 512), BF),
@@ -629,14 +651,17 @@
         ((PAIR * SLOTS, WIDTH), BF),
         ((PAIR * SLOTS, WIDTH), BF),
         ((ROWS, WIDTH), BF),
-        ((NT, ROWS, WIDE), BF),
         ((PAIR * SLOTS, NT * FF), BF),
         ((SEQ, WIDTH), BF),
         ((NT, SEQ, WIDE), BF),
-        ((NT, NX, SEQ, WIDE), BF),
-        ((NX, NT, SEQ, WIDE), BF),
-        ((NZ, SEQ, WIDE), BF),
-        ((NZ, SEQ, WIDE), BF),
+        ((2, NX, SEQ, 1024), BF),
+        ((2, NX, SEQ, 1024), BF),
+        ((2, NZ, SEQ, 128), BF),
+        ((2, NZ, SEQ, 128), BF),
+        ((NT, 16, 128), BF),
+        ((NT, 16, 128), BF),
+        ((NT * 16, TILE), BF),
+        ((2, SEQ, NT * 16), BF),
         ((NE, 2 * BOTH, 128), BF),
         ((NE, 2 * BOTH, 128), BF),
         ((SEQ, HEAD), F32),

time: 82 us -> 79.4 us (0.968)
  Pallas kernels: 81 us -> 78.7 us
    pallas_call x1, Pallas kernels: 78.7 us -> 76.4 us  [local(): pl.pallas_call(layer, out_shape=[pltpu.VMEM((SEQ, WIDE), F32), pltpu.VMEM...]
where the time goes in v6:
time: 79.4 us; the launch traced here: 79.3 us
  Pallas kernels  78.7 us (99%)
    pallas_call x1, Pallas kernels, local(): pl.pallas_call(layer, out_shape=[pltpu.VMEM((SEQ, WIDE), F32), pltpu.VMEM...  76.4 us
    pallas_call x1, Pallas kernels, local(): pl.pallas_call(closing, out_shape=[jax.ShapeDtypeStruct((SEQ, WIDE), BF),...  2.28 us

profile of v6, /device:TPU:1, one launch (start us, length us, event | category | flops | bytes accessed | tf_op | source)
XLA Modules:
  0.0 79.3 jit_solution(3424753174821894727)
XLA Ops:
  0.6 76.4 %layer.1 = (f32[48,256]{1,0:T(8,128)S(1)}, f32[48,1,128,128]{3,2,1,0:T(8,128)S(1)}) custom-call(bf16[48,2048]{1,0:T(8,128)(2,1)} %tokens.1, f32[48,1,128,128]{3,2,1,0:T(8,128)} %state.1, f32[1,2048]{1,0:T(1,128)} %bitcast.7, bf16[64,128]{1,0:T(8,128)(2,1)} %w_query.1, bf16[64,128]{1,0:T(8,128)(2,1)} %w_forget.1, bf16[64,128]{1,0:T(8,128)(2,1)} %w_input.1, ...), custom_call_target="tpu_custom_call" | custom-call | tf_op jit(solution)/shard_map/layer/pallas_call | solution.py:675
  77.0 2.3 %closing.1 = (bf16[48,256]{1,0:T(8,128)(2,1)}, f32[48,1,128,128]{3,2,1,0:T(8,128)}) custom-call(f32[48,256]{1,0:T(8,128)S(1)} %get-tuple-element.4.result, f32[48,1,128,128]{3,2,1,0:T(8,128)S(1)} %get-tuple-element.5.held), custom_call_target="tpu_custom_call" | custom-call | tf_op jit(solution)/shard_map/closing/pallas_call | solution.py:692

commit v7 on v6

--- a/solution.py
+++ b/solution.py
@@ -26,7 +26,7 @@
 Y_ORDER = (1, 3, 2)
 X_ORDER = (1, 3, 2)
 FAR_ORDER = (4, 3, 5, 2, 6, 1, 7, 0)
-SENDS, ARRIVALS, LOCALS = 21, 70, 19
+SENDS, ARRIVALS, LOCALS = 25, 74, 19
 scope = jax.named_scope
 
 
@@ -103,11 +103,11 @@
     def greet(self):
         barrier = pltpu.get_barrier_semaphore()
         peers = []
-        for dz in range(NZ):
-            for dx in range(NX):
+        for dz in FAR_ORDER:
+            for dx in (2, 1, 3, 0):
                 if dz or dx:
                     peers.append(dict(z=(self.z + dz) % NZ, x=(self.x + dx) % NX))
-        for dy in range(NY):
+        for dy in (2, 1, 3, 0):
             for dc in range(NC):
                 if dy or dc:
                     peers.append(dict(y=(self.y + dy) % NY, c=(self.c + dc) % NC))
@@ -228,7 +228,6 @@
     row_in,
     pack,
     unpack,
-    order,
     regroup,
     dense_raw,
     resid_rows,
@@ -244,6 +243,11 @@
     sum_in,
     sum2_out,
     sum2_in,
+    zq_out,
+    zq_in,
+    xq_out,
+    xq_in,
+    quarter,
     swap_out,
     swap_in,
     pad_lines,
@@ -338,7 +342,11 @@
                 picked = picked + here.astype(F32)
         dispatch[...] = picked.astype(BF)
         for h in range(2):
-            combine[h, :, :] = halves[h].T
+            rest = halves[h].T
+            for i in range(3):
+                piece = rest.astype(BF)
+                combine[h, i * SEQ : (i + 1) * SEQ, :] = piece
+                rest = rest - piece.astype(F32)
 
     def row_of(place):
         inside = place % BOTH
@@ -362,18 +370,18 @@
         inside = row % SEQ
         return (inside // OWN) * TILE + (row // SEQ) * OWN + inside % OWN
 
-    def ordered_row(row):
+    def quarter_row(row):
         inside = row % SEQ
-        return (inside // OWN) * SEQ + (row // SEQ) * OWN + inside % OWN
+        return (inside // OWN) * 4 * OWN + (row // SEQ) * OWN + inside % OWN
 
     def regrouped_row(row):
         e = row // OWN
         return (e % NX) * SEQ + (e // NX) * OWN + row % OWN
 
-    many, few = NT * TILE, NT * SEQ
+    many = NT * TILE
     pack[...] = (iota((many, many), 0) == packed_row(iota((1, many), 1))).astype(F32).astype(BF)
     unpack[...] = (iota((many, many), 1) == packed_row(iota((many, 1), 0))).astype(F32).astype(BF)
-    order[...] = (iota((few, few), 0) == ordered_row(iota((1, few), 1))).astype(F32).astype(BF)
+    quarter[...] = (iota((ROWS, ROWS), 0) == quarter_row(iota((1, ROWS), 1))).astype(F32).astype(BF)
     line = iota((1, TILE), 1)
     pad_lines[...] = (iota((NT * 16, TILE), 0) == (line // 12) * 16 + line % 12).astype(F32).astype(BF)
     token = iota((SEQ, 1), 0)
@@ -500,26 +508,7 @@
     chosen_onward()
     down_rest.append(swap_down(1))
 
-    n.wait(rows.at[pl.ds(0, 24)], base_c + 7)
     chosen_relay()
-    for g in range(NE // NT):
-        group = dot(unpack[...], rows[g * NT : (g + 1) * NT].reshape(NT * TILE, 128))
-        for k in range(WIDTH // 128):
-            dense_raw[:, k * 128 : (k + 1) * 128] = group[k * SEQ : (k + 1) * SEQ, :]
-        dense_in[g * SEQ : (g + 1) * SEQ, :] = scaled(dense_raw[...], gain).astype(BF)
-    dense_rest()
-    pre = dot(dense_in[...], dense_w[...].reshape(WIDTH, 2 * WIDE))
-    units = (jax.nn.silu(pre[:, :WIDE]) * pre[:, WIDE:]).astype(BF)
-    inner = dot(regroup[...], units).astype(BF)
-    last_rest()
-    base_x = n.reserve(2)
-    for h in range(2):
-        block = dot(inner, dense_d[:, h * 1024 : (h + 1) * 1024])
-        sum_out[h, :, :, :] = block.astype(BF).reshape(NX, SEQ, 1024)
-        send_x = n.stage(sum_in.at[h, pl.ds(0, 3)])
-        for dx in X_ORDER:
-            x = (n.x + dx) % NX
-            send_x(sum_out.at[h, x], sum_in.at[h, n.x], base_x + h, x=x)
     chosen_rest()
     for copy in load_expert:
         copy.wait()
@@ -534,30 +523,68 @@
         lambda t: cols_at(hidden, t, FF), hidden.at[:, pl.ds(0, 7 * FF)]
     )
 
-    decay, keygate = gates[0].T, gates[1].T
-    for b in range(SEQ):
-        held[b, 0] = decay[:, b : b + 1] * held[b, 0] + keygate[:, b : b + 1] * gates[2, b : b + 1, :]
-
-    base_z = n.reserve(2)
-
-    def sum_over_x(h):
-        n.wait(sum_in.at[h, pl.ds(0, 3)], base_x + h)
-        block = sum_out[h, pl.ds(n.x, 1)][0].astype(F32)
+    n.wait(rows.at[pl.ds(0, 24)], base_c + 7)
+    for g in range(NE // NT):
+        group = dot(unpack[...], rows[g * NT : (g + 1) * NT].reshape(NT * TILE, 128))
+        for k in range(WIDTH // 128):
+            dense_raw[:, k * 128 : (k + 1) * 128] = group[k * SEQ : (k + 1) * SEQ, :]
+        dense_in[g * SEQ : (g + 1) * SEQ, :] = scaled(dense_raw[...], gain).astype(BF)
+    dense_rest()
+    pre = dot(dense_in[...], dense_w[...].reshape(WIDTH, 2 * WIDE))
+    units = (jax.nn.silu(pre[:, :WIDE]) * pre[:, WIDE:]).astype(BF)
+    inner = dot(regroup[...], units).astype(BF)
+    last_rest()
+    def to_lines(block):
+        for k in range(4):
+            flat[k * SEQ : (k + 1) * SEQ, :] = block[:, k * 128 : (k + 1) * 128]
+        return dot(quarter[...], flat[:ROWS]).astype(BF).reshape(NZ, 4 * OWN, 128)
+
+    block = dot(inner, dense_d[:, 3 * 512 :]).astype(BF)
+    for x in range(NX):
+        zq_out[:, x] = to_lines(block[x * SEQ : (x + 1) * SEQ])
+    base_zq = n.reserve(1)
+    send_zq = n.stage(zq_in.at[pl.ds(0, 7)])
+    for dz in FAR_ORDER[:-1]:
+        send_zq(zq_out.at[z_at[dz]], zq_in.at[n.z], base_zq, z=z_at[dz])
+    zq_in[pl.ds(n.z, 1)] = zq_out[pl.ds(n.z, 1)]
+    base_x = n.reserve(3)
+    for q in range(3):
+        block = dot(inner, dense_d[:, q * 512 : (q + 1) * 512])
+        sum_out[q, :, :, :] = block.astype(BF).reshape(NX, SEQ, 512)
+        send_x = n.stage(sum_in.at[q, pl.ds(0, 3)])
         for dx in X_ORDER:
-            block = block + sum_in[h, pl.ds((n.x + dx) % NX, 1)][0].astype(F32)
-        block = block.astype(BF)
-        for k in range(8):
-            flat[k * SEQ : (k + 1) * SEQ, :] = block[:, k * 128 : (k + 1) * 128]
-        sum2_out[h, :, :, :] = dot(order[...], flat[: 8 * SEQ]).astype(BF).reshape(NZ, SEQ, 128)
-        send_z = n.stage(sum2_in.at[h, pl.ds(0, 7)])
+            x = (n.x + dx) % NX
+            send_x(sum_out.at[q, x], sum_in.at[q, n.x], base_x + q, x=x)
+
+    base_z = n.reserve(3)
+
+    def sum_over_x(q):
+        n.wait(sum_in.at[q, pl.ds(0, 3)], base_x + q)
+        block = sum_out[q, pl.ds(n.x, 1)][0].astype(F32)
+        for dx in X_ORDER:
+            block = block + sum_in[q, pl.ds((n.x + dx) % NX, 1)][0].astype(F32)
+        sum2_out[q, :, :, :] = to_lines(block.astype(BF))
+        send_z = n.stage(sum2_in.at[q, pl.ds(0, 7)])
         for dz in FAR_ORDER[:-1]:
-            send_z(sum2_out.at[h, z_at[dz]], sum2_in.at[h, n.z], base_z + h, z=z_at[dz])
-        sum2_in[h, pl.ds(n.z, 1)] = sum2_out[h, pl.ds(n.z, 1)]
+            send_z(sum2_out.at[q, z_at[dz]], sum2_in.at[q, n.z], base_z + q, z=z_at[dz])
+        sum2_in[q, pl.ds(n.z, 1)] = sum2_out[q, pl.ds(n.z, 1)]
 
     hidden_onward()
+    hidden_relay()
     sum_over_x(0)
-    hidden_relay()
     sum_over_x(1)
+    n.wait(zq_in.at[pl.ds(0, 7)], base_zq)
+    acc = zq_in[0].astype(F32)
+    for z in range(1, NZ):
+        acc = acc + zq_in[z].astype(F32)
+    xq_out[...] = acc.astype(BF)
+    base_xq = n.reserve(1)
+    send_xq = n.stage(xq_in.at[pl.ds(0, 3)])
+    for dx in X_ORDER:
+        x = (n.x + dx) % NX
+        send_xq(xq_out.at[x], xq_in.at[n.x], base_xq, x=x)
+    xq_in[pl.ds(n.x, 1)] = xq_out[pl.ds(n.x, 1)]
+    sum_over_x(2)
 
     shared_rest = n.swap_tp(lambda t: cols_at(shared_part, t, WIDE), lambda t: shared_in.at[t], shared_in.at[pl.ds(0, 7)])
     shared_in[pl.ds(n.t, 1)] = cols_at(shared_part, n.t, WIDE)[...][None]
@@ -573,30 +600,40 @@
     back_rest = n.swap_ep(back_out, back_in)
     back_in[pl.ds(n.e, 1)] = back_out[pl.ds(n.e, 1)]
 
+    decay, keygate = gates[0].T, gates[1].T
+    for b in range(SEQ):
+        held[b, 0] = decay[:, b : b + 1] * held[b, 0] + keygate[:, b : b + 1] * gates[2, b : b + 1, :]
+
     own_lines = []
-    for h in range(2):
-        n.wait(sum2_in.at[h, pl.ds(0, 7)], base_z + h)
-        acc = sum2_in[h, 0].astype(F32)
+    for q in range(3):
+        n.wait(sum2_in.at[q, pl.ds(0, 7)], base_z + q)
+        acc = sum2_in[q, 0].astype(F32)
         for z in range(1, NZ):
-            acc = acc + sum2_in[h, z].astype(F32)
+            acc = acc + sum2_in[q, z].astype(F32)
         own_lines.append(acc)
+    n.wait(xq_in.at[pl.ds(0, 3)], base_xq)
+    acc = xq_in[0].astype(F32)
+    for x in range(1, NX):
+        acc = acc + xq_in[x].astype(F32)
+    own_lines.append(acc)
     own_lines = jnp.concatenate(own_lines, axis=0).astype(BF)
     swap_out[...] = dot(pad_lines[...], own_lines).astype(BF).reshape(NT, 16, 128)
     swap_rest = n.swap_tp(lambda t: swap_out.at[t], lambda t: swap_in.at[t], swap_in.at[pl.ds(0, 7)])
     swap_in[pl.ds(n.t, 1)] = swap_out[pl.ds(n.t, 1)]
-    back_rest()
     shared_rest()
-    lines = back_in[...].reshape(LINES, 128).astype(F32)
-    routed = [
-        jnp.dot(combine[h], lines, preferred_element_type=F32, precision=lax.Precision.HIGHEST) for h in range(2)
-    ]
-    result = resid[...] + jnp.concatenate(routed, axis=1)
+    result = resid[...]
     for t in range(NT):
         result = result + shared_in[t].astype(F32)
     swap_rest()
     lines = swap_in[...].reshape(NT * 16, 128)
     dense_out = jnp.concatenate([dot(take_lines[h], lines) for h in range(2)], axis=1)
     result = result + dense_out * jax.nn.sigmoid(dense_mix[...])
+    back_rest()
+    lines = back_in[...].reshape(LINES, 128)
+    both = dot(combine[...].reshape(6 * SEQ, LINES), lines)
+    parts = [both[i * SEQ : (i + 1) * SEQ] for i in range(6)]
+    routed = [parts[3 * h] + (parts[3 * h + 1] + parts[3 * h + 2]) for h in range(2)]
+    result = result + jnp.concatenate(routed, axis=1)
     mixed[...] = result
     n.finish()
 
@@ -642,7 +679,6 @@
         ((NT, TILE, 128), BF),
         ((NT * TILE, NT * TILE), BF),
         ((NT * TILE, NT * TILE), BF),
-        ((NT * SEQ, NT * SEQ), BF),
         ((ROWS, ROWS), BF),
         ((SEQ, WIDTH), F32),
         ((SEQ, WIDTH), BF),
@@ -654,10 +690,15 @@
         ((PAIR * SLOTS, NT * FF), BF),
         ((SEQ, WIDTH), BF),
         ((NT, SEQ, WIDE), BF),
-        ((2, NX, SEQ, 1024), BF),
-        ((2, NX, SEQ, 1024), BF),
-        ((2, NZ, SEQ, 128), BF),
-        ((2, NZ, SEQ, 128), BF),
+        ((3, NX, SEQ, 512), BF),
+        ((3, NX, SEQ, 512), BF),
+        ((3, NZ, 4 * OWN, 128), BF),
+        ((3, NZ, 4 * OWN, 128), BF),
+        ((NZ, NX, 4 * OWN, 128), BF),
+        ((NZ, NX, 4 * OWN, 128), BF),
+        ((NX, 4 * OWN, 128), BF),
+        ((NX, 4 * OWN, 128), BF),
+        ((ROWS, ROWS), BF),
         ((NT, 16, 128), BF),
         ((NT, 16, 128), BF),
         ((NT * 16, TILE), BF),
@@ -665,7 +706,7 @@
         ((NE, 2 * BOTH, 128), BF),
         ((NE, 2 * BOTH, 128), BF),
         ((SEQ, HEAD), F32),
-        ((2, SEQ, LINES), F32),
+        ((2, 3 * SEQ, LINES), BF),
         ((LINES, SEQ), BF),
         ((2, PAIR * SLOTS, LINES), BF),
         ((LINES, PAIR * SLOTS), BF),

time: 79.4 us -> 78.8 us (level)
  Pallas kernels: 78.7 us -> 77.8 us
    pallas_call x1, Pallas kernels: 76.4 us -> 75.6 us  [local(): pl.pallas_call(layer, out_shape=[pltpu.VMEM((SEQ, WIDE), F32), pltpu.VMEM...]
where the time goes in v7:
time: 78.8 us; the launch traced here: 78.6 us
  Pallas kernels  77.8 us (99%)
  between operations  0.81 us (1%)
    pallas_call x1, Pallas kernels, local(): pl.pallas_call(layer, out_shape=[pltpu.VMEM((SEQ, WIDE), F32), pltpu.VMEM...  75.6 us
    pallas_call x1, Pallas kernels, local(): pl.pallas_call(closing, out_shape=[jax.ShapeDtypeStruct((SEQ, WIDE), BF),...  2.28 us

profile of v7, /device:TPU:1, one launch (start us, length us, event | category | flops | bytes accessed | tf_op | source)
XLA Modules:
  0.0 78.6 jit_solution(10362715595966999981)
XLA Ops:
  0.6 75.6 %layer.1 = (f32[48,256]{1,0:T(8,128)S(1)}, f32[48,1,128,128]{3,2,1,0:T(8,128)S(1)}) custom-call(bf16[48,2048]{1,0:T(8,128)(2,1)} %tokens.1, f32[48,1,128,128]{3,2,1,0:T(8,128)} %state.1, f32[1,2048]{1,0:T(1,128)} %bitcast.7, bf16[64,128]{1,0:T(8,128)(2,1)} %w_query.1, bf16[64,128]{1,0:T(8,128)(2,1)} %w_forget.1, bf16[64,128]{1,0:T(8,128)(2,1)} %w_input.1, ...), custom_call_target="tpu_custom_call" | custom-call | tf_op jit(solution)/shard_map/layer/pallas_call | solution.py:716
  76.2 2.3 %closing.1 = (bf16[48,256]{1,0:T(8,128)(2,1)}, f32[48,1,128,128]{3,2,1,0:T(8,128)}) custom-call(f32[48,256]{1,0:T(8,128)S(1)} %get-tuple-element.4.result, f32[48,1,128,128]{3,2,1,0:T(8,128)S(1)} %get-tuple-element.5.held), custom_call_target="tpu_custom_call" | custom-call | tf_op jit(solution)/shard_map/closing/pallas_call | solution.py:733

commit v8 on v7

--- a/solution.py
+++ b/solution.py
@@ -490,7 +490,8 @@
 
     slots_rest()
     lines = slot_in[...].reshape(LINES, 128)
-    picked_rows = jnp.concatenate([dot(squeeze[h], lines) for h in range(2)], axis=1)
+    both = dot(squeeze[...].reshape(2 * PAIR * SLOTS, LINES), lines)
+    picked_rows = jnp.concatenate([both[: PAIR * SLOTS], both[PAIR * SLOTS :]], axis=1)
     cols_at(chosen, n.t, WIDE)[...] = picked_rows.astype(BF)
     chosen_onward, chosen_relay, chosen_rest = n.gather_tp(
         lambda t: cols_at(chosen, t, WIDE), chosen.at[:, pl.ds(0, 7 * WIDE)]
@@ -584,8 +585,6 @@
         x = (n.x + dx) % NX
         send_xq(xq_out.at[x], xq_in.at[n.x], base_xq, x=x)
     xq_in[pl.ds(n.x, 1)] = xq_out[pl.ds(n.x, 1)]
-    sum_over_x(2)
-
     shared_rest = n.swap_tp(lambda t: cols_at(shared_part, t, WIDE), lambda t: shared_in.at[t], shared_in.at[pl.ds(0, 7)])
     shared_in[pl.ds(n.t, 1)] = cols_at(shared_part, n.t, WIDE)[...][None]
     for rest in down_rest:
@@ -597,6 +596,7 @@
     ]
     spread = dot(expand[:, :SLOTS], outs[0]) + dot(expand[:, SLOTS:], outs[1])
     back_out[...] = in_lines(spread)
+    sum_over_x(2)
     back_rest = n.swap_ep(back_out, back_in)
     back_in[pl.ds(n.e, 1)] = back_out[pl.ds(n.e, 1)]
 

time: 78.8 us -> 79 us (level)
  no operation moved by 1% of the time
where the time goes in v8:
time: 79 us; the launch traced here: 78.8 us
  Pallas kernels  78 us (99%)
  between operations  0.81 us (1%)
    pallas_call x1, Pallas kernels, local(): pl.pallas_call(layer, out_shape=[pltpu.VMEM((SEQ, WIDE), F32), pltpu.VMEM...  75.7 us
    pallas_call x1, Pallas kernels, local(): pl.pallas_call(closing, out_shape=[jax.ShapeDtypeStruct((SEQ, WIDE), BF),...  2.28 us

profile of v8, /device:TPU:1, one launch (start us, length us, event | category | flops | bytes accessed | tf_op | source)
XLA Modules:
  0.0 78.8 jit_solution(17233194170912388103)
XLA Ops:
  0.6 75.7 %layer.1 = (f32[48,256]{1,0:T(8,128)S(1)}, f32[48,1,128,128]{3,2,1,0:T(8,128)S(1)}) custom-call(bf16[48,2048]{1,0:T(8,128)(2,1)} %tokens.1, f32[48,1,128,128]{3,2,1,0:T(8,128)} %state.1, f32[1,2048]{1,0:T(1,128)} %bitcast.7, bf16[64,128]{1,0:T(8,128)(2,1)} %w_query.1, bf16[64,128]{1,0:T(8,128)(2,1)} %w_forget.1, bf16[64,128]{1,0:T(8,128)(2,1)} %w_input.1, ...), custom_call_target="tpu_custom_call" | custom-call | tf_op jit(solution)/shard_map/layer/pallas_call | solution.py:716
  76.4 2.3 %closing.1 = (bf16[48,256]{1,0:T(8,128)(2,1)}, f32[48,1,128,128]{3,2,1,0:T(8,128)}) custom-call(f32[48,256]{1,0:T(8,128)S(1)} %get-tuple-element.4.result, f32[48,1,128,128]{3,2,1,0:T(8,128)S(1)} %get-tuple-element.5.held), custom_call_target="tpu_custom_call" | custom-call | tf_op jit(solution)/shard_map/closing/pallas_call | solution.py:733
